TPU v7x, 512 devices: a whole 4x4x16 slice. The times are simulated.
512 devices in a mesh: sp: 128 (over z, x, core), tp: 4 (over y).
Axes of the slice: x: 4, y: 4, z: 16, core: 2. Of those that a mesh axis runs over, the one named last changes fastest.
Arguments:
- tokens: bfloat16 [16384, 2048], P(('sp', 'tp')), may hold values from -6 to 6
- input_norm_gain: float32 [2048], replicated, may hold values from 0.1 to 1.9
- convolution_value_weight: bfloat16 [2048, 1024], P('sp', 'tp'), may hold values from -0.125 to 0.125
- convolution_gate_weight: bfloat16 [2048, 1024], P('sp', 'tp'), may hold values from -0.125 to 0.125
- depthwise_filter_taps: float32 [31, 1024], P(None, 'tp'), may hold values from -4 to 4
- channel_norm_gain: float32 [1024], P('tp'), may hold values from 0.1 to 1.9
- channel_norm_bias: float32 [1024], P('tp'), may hold values from -3 to 3
- query_projection_weight: bfloat16 [2048, 1024], P('sp', 'tp'), may hold values from -0.125 to 0.125
- forget_gate_weight: bfloat16 [2048, 1024], P('sp', 'tp'), may hold values from -0.125 to 0.125
- recurrence_value_weight: bfloat16 [2048, 1024], P('sp', 'tp'), may hold values from -0.125 to 0.125
- output_gate_weight: bfloat16 [2048, 1024], P('sp', 'tp'), may hold values from -0.125 to 0.125
- forget_floor_margin: float32 [1024], P('tp'), may hold values from 6.1035156e-06 to 0.1
- decay_jump_terms: float32 [8, 16384], P('tp', 'sp'), may hold values from -0.7 to 0
- head_norm_gain: float32 [1024], P('tp'), may hold values from 0.1 to 1.9
- convolution_output_weight: bfloat16 [1024, 2048], P('tp', 'sp'), may hold values from -0.125 to 0.125
- recurrence_output_weight: bfloat16 [1024, 2048], P('tp', 'sp'), may hold values from -0.125 to 0.125
Outputs:
- mixed: bfloat16 [16384, 2048], P(('sp', 'tp'))
All inputs are finite; a program needn't handle non-finite values.
Results may differ from a plain program's by a relative error of at most 0.015.
Values may be sent and summed in bfloat16 or wider, within the bound.
No kernel may reach another device: no remote copies, remote signals or barrier semaphores. Data moves between devices by JAX's collectives and lax.ppermute only.
A program may use at most 64 MiB of HBM per device.

v0:
```python
import jax
import jax.numpy as jnp
from jax import lax
from jax.sharding import Mesh
from jax.sharding import PartitionSpec as P

CONV_CH = 1024
HG_DK = 128
HG_DV = 128
HG_BLOCK = 64
SP = ("sp_0", "sp_1", "sp_2")
SP_TP = ("sp_0", "sp_1", "sp_2", "tp")


norm_eps = 1e-06
layer_eps = 1e-05


def rows_first(arrays, axis, dims):
    turned = [jnp.moveaxis(a, dim, 0) for a, dim in zip(arrays, dims)]
    both = jnp.concatenate([t.reshape(len(t), -1) for t in turned], axis=1)
    out, at, outs = (lax.all_gather(both, axis, axis=0, tiled=True), 0, [])
    for t, dim in zip(turned, dims):
        section = out[:, at : at + t[0].size].reshape(-1, *t.shape[1:])
        outs.append(jnp.moveaxis(section, 0, dim))
        at += t[0].size
    return tuple(outs)


def joined_along(blocks, dim):
    shape = list(blocks.shape[1:])
    shape[dim] *= blocks.shape[0]
    return jnp.moveaxis(blocks, 0, dim).reshape(shape)


def sent_to_all(x, axis):
    copies = jnp.broadcast_to(x, (lax.axis_size(axis), *x.shape))
    return lax.all_to_all(copies, axis, split_axis=0, concat_axis=0, tiled=True)


def gather_directly(x, axis, dim):
    return joined_along(sent_to_all(x, axis), dim)


def passed_along(value, axis, steps):
    count = lax.axis_size(axis)
    initial, last = (max(0, -steps), min(count, count - steps))
    return lax.ppermute(value, axis, [(source, source + steps) for source in range(initial, last)])


def filled_with(x, identity):
    return jax.tree.map(
        lambda part, zero: jnp.zeros_like(part) + jnp.asarray(zero, part.dtype), x, identity
    )


def entering(x, axes, combine, identity):
    before = start = filled_with(x, identity)
    running = x
    for axis in reversed(axes):
        size, mine = (lax.axis_size(axis), lax.axis_index(axis))
        pieces = jax.tree.map(
            lambda part, kind: lax.all_gather(part.astype(kind), axis),
            running,
            (jnp.bfloat16, jnp.bfloat16),
        )
        inside, running = (start, start)
        for k in range(size):
            passed = k < mine
            running = combine(
                running, jax.tree.map(lambda part, own: part[k].astype(own.dtype), pieces, x)
            )
            inside = jax.tree.map(lambda new, old: jnp.where(passed, new, old), running, inside)
        before = combine(inside, before)
    return before


def of_everyone(x, axis):
    return sent_to_all(x, axis).sum(axis=0)


def together(arrays, axis):
    flat, at, outs = (jnp.concatenate([a.reshape(-1) for a in arrays]), 0, [])
    running = of_everyone(flat, axis)
    for a in arrays:
        outs.append(running[at : at + a.size].reshape(a.shape))
        at += a.size
    return tuple(outs)


def in_blocks(x, dim, size):
    shape = x.shape
    blocks = x.reshape(*shape[:dim], size, shape[dim] // size, *shape[dim + 1 :])
    return jnp.moveaxis(blocks, dim, 0)


def sent_and_summed(x, axis, dim):
    blocks = in_blocks(x, dim, lax.axis_size(axis))
    arrived = lax.all_to_all(blocks, axis, split_axis=0, concat_axis=0, tiled=True)
    return arrived.astype(jnp.float32).sum(axis=0)


def convolve(gated, kernel):
    return lax.conv_general_dilated(
        gated[None],
        kernel[:, None, :],
        (1,),
        "VALID",
        dimension_numbers=("NWC", "WIO", "NWC"),
        feature_group_count=gated.shape[1],
    )[0]


def channel_norm(values, first_sum, second_sum, gain, bias):
    mean_value = first_sum[:, None] / CONV_CH
    variance = second_sum[:, None] / CONV_CH - mean_value * mean_value
    shifted = (values - mean_value) * lax.rsqrt(variance + layer_eps) * gain + bias
    return jax.nn.silu(shifted).astype(jnp.bfloat16)


def gate_factors(query_projected, forget_projected, forget_floor_margin, decay_jump_rows):
    row_total_count = query_projected.shape[0]
    head_total_count = decay_jump_rows.shape[1]
    query_rows = jax.nn.silu(query_projected.astype(jnp.float32))
    log_forget_gate = jnp.logaddexp(
        jnp.log1p(-forget_floor_margin),
        jnp.log(forget_floor_margin) + jax.nn.log_sigmoid(forget_projected.astype(jnp.float32)),
    )
    key_gate_values = -jnp.expm1(log_forget_gate)
    log_decay_running = (
        log_forget_gate.reshape(row_total_count, head_total_count, -1) + decay_jump_rows[:, :, None]
    )
    return (
        query_rows.reshape(row_total_count, head_total_count, -1),
        key_gate_values.reshape(row_total_count, head_total_count, -1),
        log_decay_running,
    )


def finish(recurrent, gain, outgate_proj):
    row_total_count = recurrent.shape[0]
    scaled = recurrent * lax.rsqrt(
        jnp.mean(recurrent * recurrent, axis=2, keepdims=True) + norm_eps
    )
    gated_out = (
        scaled.reshape(row_total_count, -1) * gain * jax.nn.silu(outgate_proj.astype(jnp.float32))
    )
    return gated_out.astype(jnp.bfloat16)


def combine_states(first_part, second_part):
    return (
        first_part[0] + second_part[0],
        jnp.exp(second_part[0])[:, :, None] * first_part[1] + second_part[1],
    )


def carry_step(recurrence_state, block_parts):
    decay_end, contribution = block_parts
    return (jnp.exp(decay_end)[:, :, None] * recurrence_state + contribution, recurrence_state)


def per_device(
    tokens,
    input_norm_gain,
    convolution_value_weight,
    convolution_gate_weight,
    depthwise_filter_taps,
    channel_norm_gain,
    channel_norm_bias,
    query_projection_weight,
    forget_gate_weight,
    recurrence_value_weight,
    output_gate_weight,
    forget_floor_margin,
    decay_jump_terms,
    head_norm_gain,
    convolution_output_weight,
    recurrence_output_weight,
):
    features = tokens.astype(jnp.float32)
    normed = (
        features
        * lax.rsqrt(jnp.mean(features * features, axis=1, keepdims=True) + norm_eps)
        * input_norm_gain
    ).astype(jnp.bfloat16)
    gathered = rows_first(
        (
            convolution_value_weight,
            convolution_gate_weight,
            query_projection_weight,
            forget_gate_weight,
            recurrence_value_weight,
            output_gate_weight,
            convolution_output_weight,
            recurrence_output_weight,
        ),
        SP,
        (0, 0, 0, 0, 0, 0, 1, 1),
    )
    projection_weights = gathered[:6]
    conv_columns = gathered[6]
    rec_columns = gathered[7]

    def project(row_piece):
        return jnp.concatenate(
            [
                jnp.dot(row_piece, weight, preferred_element_type=jnp.float32).astype(jnp.bfloat16)
                for weight in projection_weights
            ],
            axis=1,
        )

    projected = project(gather_directly(normed, "tp", 0))
    offsets = []
    position = 0
    for weight in projection_weights[:-1]:
        position = position + weight.shape[1]
        offsets.append(position)
    value_proj, gate_proj, query_projected, forget_projected, input_proj, outgate_proj = jnp.split(
        projected, offsets, axis=1
    )
    row_total_count = value_proj.shape[0]
    rim_rows = depthwise_filter_taps.shape[0] - 1
    tail_value, tail_gate = passed_along(
        (value_proj[row_total_count - rim_rows :], gate_proj[row_total_count - rim_rows :]), SP, 1
    )
    value_ext = jnp.concatenate([tail_value, value_proj], axis=0)
    gate_ext = jnp.concatenate([tail_gate, gate_proj], axis=0)
    gated = value_ext.astype(jnp.float32) * jax.nn.sigmoid(gate_ext.astype(jnp.float32))
    convolved = convolve(gated, depthwise_filter_taps).astype(jnp.bfloat16)
    device_heads = decay_jump_terms.shape[0]
    query_rows, key_gate_values, log_decay_running = gate_factors(
        query_projected, forget_projected, forget_floor_margin, decay_jump_terms.T
    )
    input_rows = input_proj.astype(jnp.float32).reshape(row_total_count, device_heads, -1)
    block_count = row_total_count // HG_BLOCK

    def to_blocks(array):
        return array.reshape(block_count, HG_BLOCK, device_heads, -1).transpose(0, 2, 1, 3)

    block_queries = to_blocks(query_rows)
    block_keys = to_blocks(key_gate_values)
    block_inputs = to_blocks(input_rows)
    cumulative = jnp.cumsum(to_blocks(log_decay_running), axis=2)
    final_decay = cumulative[:, :, -1, :]
    query_rows_scaled = block_queries * jnp.exp(cumulative)
    scaled_keys = block_keys * jnp.exp(-cumulative)
    final_keys = block_keys * jnp.exp(final_decay[:, :, None, :] - cumulative)
    attention_scores = jnp.einsum("nhtk,nhsk->nhts", query_rows_scaled, scaled_keys)
    causal = jnp.arange(HG_BLOCK)[:, None] >= jnp.arange(HG_BLOCK)[None, :]
    attention_scores = jnp.where(causal[None, None], attention_scores, 0.0)
    inner = jnp.einsum("nhts,nhsv->nhtv", attention_scores, block_inputs)
    contributions = jnp.einsum("nhsk,nhsv->nhkv", final_keys, block_inputs)
    initial = jnp.zeros((device_heads, HG_DK, HG_DV), jnp.float32)
    local_state, block_starts = lax.scan(carry_step, initial, (final_decay, contributions))
    device_decay = jnp.sum(final_decay, axis=0)
    before_blocks = jnp.cumsum(final_decay, axis=0) - final_decay
    incoming = entering(
        (device_decay, local_state),
        SP,
        combine_states,
        (jnp.zeros_like(device_decay), jnp.zeros_like(local_state)),
    )
    starts = block_starts + jnp.exp(before_blocks)[:, :, :, None] * incoming[1][None]
    recurrent = inner + jnp.einsum("nhtk,nhkv->nhtv", query_rows_scaled, starts)
    recurrent = recurrent.transpose(0, 2, 1, 3).reshape(row_total_count, device_heads, -1)
    rec_out = finish(recurrent, head_norm_gain, outgate_proj)
    values = convolved.astype(jnp.float32)
    totals = together((jnp.sum(values, axis=1), jnp.sum(values * values, axis=1)), "tp")
    conv_out = channel_norm(values, totals[0], totals[1], channel_norm_gain, channel_norm_bias)
    conv_part = lax.slice_in_dim(
        conv_out, 0, row_total_count // lax.axis_size("tp") * lax.axis_size("tp"), axis=0
    )
    summed = sent_and_summed(
        (
            jnp.dot(conv_part, conv_columns, preferred_element_type=jnp.float32)
            + jnp.dot(rec_out, rec_columns, preferred_element_type=jnp.float32)
        ).astype(jnp.bfloat16),
        "tp",
        0,
    )
    return summed.astype(jnp.bfloat16)


def solution(mesh):
    split = Mesh(mesh.devices.reshape(16, 4, 2, mesh.shape["tp"]), ("sp_0", "sp_1", "sp_2", "tp"))
    return jax.shard_map(
        per_device,
        mesh=split,
        in_specs=(
            P(SP_TP, None),
            P(),
            P(SP, "tp"),
            P(SP, "tp"),
            P(None, "tp"),
            P("tp"),
            P("tp"),
            P(SP, "tp"),
            P(SP, "tp"),
            P(SP, "tp"),
            P(SP, "tp"),
            P("tp"),
            P("tp", SP),
            P("tp"),
            P("tp", SP),
            P("tp", SP),
        ),
        out_specs=P(SP_TP, None),
        check_vma=False,
    )
```

profile of v0, /device:TPU:6, one launch (start us, length us, event | category | flops | bytes accessed | tf_op | source)
XLA Modules:
  0.0 284.3 jit_solution(15545226052518464159)
XLA Ops:
  12.8 1.0 fusion.18
  15.8 4.5 %all-to-all-start = ((bf16[4,32,2048]{2,1,0:T(8,128)(2,1)}), bf16[4,32,2048]{2,1,0:T(8,128)(2,1)S(1)}, u32[]{:S(2)}, u32[]{:S(2)}) async-start(bf16[4,32,2048]{2,1,0:T(8,128)(2,1)} %broadcast_in_dim.27), calls=%async_computation | async-start | bytes 1048576 | tf_op jit(solution)/shard_map/all_to_all | solution.py:38
  21.7 8.0 %all-to-all-done = bf16[4,32,2048]{2,1,0:T(8,128)(2,1)S(1)} async-done(((bf16[4,32,2048]{2,1,0:T(8,128)(2,1)}), bf16[4,32,2048]{2,1,0:T(8,128)(2,1)S(1)}, u32[]{:S(2)}, u32[]{:S(2)}) %all-to-all-start) | async-done | bytes 524320 | tf_op jit(solution)/shard_map/all_to_all | solution.py:38
  29.7 132.8 %all-gather.6.cloned.1.call-done = bf16[2048,2048]{1,0:T(8,128)(2,1)} async-done(((bf16[16,2048]{1,0:T(8,128)(2,1)}), bf16[2048,2048]{1,0:T(8,128)(2,1)}) %all-gather.6.cloned.1.call-update) | async-done | bytes 8388624 | tf_op jit(solution)/shard_map/all_gather | solution.py:22
  162.5 1.7 exponential-minus-one_negate_fusion
  164.7 1.5 convolution_convert_fusion.2
  166.9 1.9 all-gather.1
  168.8 1.8 all-gather.2
  170.8 12.3 %all_gather.35 = bf16[4,2,128,128]{3,2,1,0:T(8,128)(2,1)S(1)} all-gather(bf16[1,2,128,128]{3,2,1,0:T(8,128)(2,1)S(1)} %fusion.63), channel_id=1, replica_groups=mesh['sp_0'=16,'sp_1'=4,'sp_2'=2,'tp'=4] {'sp_1'}, dimensions={0}, use_global_device_ids=true | all-gather | bytes 327680 | tf_op jit(solution)/shard_map/all_gather | solution.py:63
  183.0 8.5 %all_gather.31 = bf16[4,2,128]{2,1,0:T(2,128)(2,1)S(1)} all-gather(bf16[1,2,128]{2,1,0:T(2,128)(2,1)S(1)} %get-tuple-element.87), channel_id=1, replica_groups=mesh['sp_0'=16,'sp_1'=4,'sp_2'=2,'tp'=4] {'sp_1'}, dimensions={0}, use_global_device_ids=true | all-gather | bytes 2560 | tf_op jit(solution)/shard_map/all_gather | solution.py:63
  192.4 1.6 divide_multiply_fusion.1
  194.0 1.5 convolution_convert_fusion.6
  195.6 1.9 collective-permute-start
  197.5 1.5 convolution_convert_fusion.5
  199.1 4.9 %collective-permute-start.1 = (bf16[30,256]{1,0:T(8,128)(2,1)S(1)}, bf16[30,256]{1,0:T(8,128)(2,1)S(1)}, u32[]{:S(2)}, u32[]{:S(2)}) collective-permute-start(bf16[30,256]{1,0:T(8,128)(2,1)S(1)} %slice.237), channel_id=1, source_target_pairs={{0,4},{4,8},{8,12},{12,16},{16,20},{20,24},{24,28},{28,32},{32,36}... | collective-permute-start | bytes 46088 | tf_op jit(solution)/shard_map/ppermute | solution.py:48
  203.9 26.1 %all_gather.32 = bf16[16,2,128]{2,1,0:T(2,128)(2,1)S(1)} all-gather(bf16[1,2,128]{2,1,0:T(2,128)(2,1)S(1)} %get-tuple-element.83), channel_id=1, replica_groups=mesh['sp_0'=16,'sp_1'=4,'sp_2'=2,'tp'=4] {'sp_0'}, dimensions={0}, use_global_device_ids=true | all-gather | bytes 8704 | tf_op jit(solution)/shard_map/all_gather | solution.py:63
  230.4 2.2 fusion.97
  233.3 4.3 %all-to-all-start.1 = ((f32[4,1,256]{2,1,0:T(1,128)}), f32[4,1,256]{2,1,0:T(1,128)S(1)}, u32[]{:S(2)}, u32[]{:S(2)}) async-start(f32[4,1,256]{2,1,0:T(1,128)} %broadcast_in_dim.29), calls=%async_computation.1 | async-start | bytes 8192 | tf_op jit(solution)/shard_map/all_to_all | solution.py:38
  237.6 5.3 %all-to-all-done.1 = f32[4,1,256]{2,1,0:T(1,128)S(1)} async-done(((f32[4,1,256]{2,1,0:T(1,128)}), f32[4,1,256]{2,1,0:T(1,128)S(1)}, u32[]{:S(2)}, u32[]{:S(2)}) %all-to-all-start.1) | async-done | bytes 4128 | tf_op jit(solution)/shard_map/all_to_all | solution.py:38
  243.0 1.7 fusion.14
  244.7 14.4 %all-gather.8.cloned.1.call-done = bf16[16,2,128,128]{3,2,1,0:T(8,128)(2,1)} async-done(((bf16[1,2,128,128]{3,2,1,0:T(8,128)(2,1)}), bf16[16,2,128,128]{3,2,1,0:T(8,128)(2,1)}) %all-gather.8.cloned.1.call-update) | async-done | bytes 1048592 | tf_op jit(solution)/shard_map/all_gather | solution.py:63
  259.1 2.1 fusion.38
  262.1 2.5 fusion
  264.5 12.2 %all_to_all.16 = bf16[4,32,2048]{2,1,0:T(8,128)(2,1)S(1)} all-to-all(bf16[4,32,2048]{2,1,0:T(8,128)(2,1)S(1)} %bitcast.162), channel_id=1, replica_groups=mesh['sp_0'=16,'sp_1'=4,'sp_2'=2,'tp'=4] {'tp'}, dimensions={0} | all-to-all | bytes 1048576 | tf_op jit(solution)/shard_map/all_to_all | solution.py:99
  (71 shorter events, 14.7 us)
Async XLA Ops:
  6.5 223.9 %copy-start = (f32[31,256]{1,0:T(8,128)S(1)}, f32[31,256]{1,0:T(8,128)}, u32[]{:S(2)}) copy-start(f32[31,256]{1,0:T(8,128)} %param.22) | copy-start | bytes 95236
  6.5 156.0 %all-gather.6.cloned.1.call-start = ((), (), s32[]{:S(2)}) async-start(), calls=%async_computation.3 | async-start | bytes 8454144 | tf_op jit(solution)/shard_map/all_gather | solution.py:22
  12.1 0.6 copy-start.1
  15.8 13.9 %all-to-all-start = ((bf16[4,32,2048]{2,1,0:T(8,128)(2,1)}), bf16[4,32,2048]{2,1,0:T(8,128)(2,1)S(1)}, u32[]{:S(2)}, u32[]{:S(2)}) async-start(bf16[4,32,2048]{2,1,0:T(8,128)(2,1)} %broadcast_in_dim.27), calls=%async_computation | async-start | bytes 1048576 | tf_op jit(solution)/shard_map/all_to_all | solution.py:38
  20.2 238.9 %all-gather.8.cloned.1.call-start = ((), (), s32[]{:S(2)}) async-start(), calls=%async_computation.4 | async-start | bytes 1114112 | tf_op jit(solution)/shard_map/all_gather | solution.py:63
  166.2 76.7 %copy-start.2 = (f32[256]{0:T(256)S(1)}, f32[256]{0:T(256)}, u32[]{:S(2)}) copy-start(f32[256]{0:T(256)} %param.24) | copy-start | bytes 3076
  166.2 76.7 %copy-start.3 = (f32[256]{0:T(256)S(1)}, f32[256]{0:T(256)}, u32[]{:S(2)}) copy-start(f32[256]{0:T(256)} %param.23) | copy-start | bytes 3076
  170.8 91.3 %copy-start.4 = (f32[256]{0:T(256)S(1)}, f32[256]{0:T(256)}, u32[]{:S(2)}) copy-start(f32[256]{0:T(256)} %param.31) | copy-start | bytes 3076
  195.6 34.7 %collective-permute-start = (bf16[30,256]{1,0:T(8,128)(2,1)S(1)}, bf16[30,256]{1,0:T(8,128)(2,1)S(1)}, u32[]{:S(2)}, u32[]{:S(2)}) collective-permute-start(bf16[30,256]{1,0:T(8,128)(2,1)S(1)} %slice.235), channel_id=1, source_target_pairs={{0,4},{4,8},{8,12},{12,16},{16,20},{20,24},{24,28},{28,32},{32,36}... | collective-permute-start | bytes 46088 | tf_op jit(solution)/shard_map/ppermute | solution.py:48
  199.1 31.3 %collective-permute-start.1 = (bf16[30,256]{1,0:T(8,128)(2,1)S(1)}, bf16[30,256]{1,0:T(8,128)(2,1)S(1)}, u32[]{:S(2)}, u32[]{:S(2)}) collective-permute-start(bf16[30,256]{1,0:T(8,128)(2,1)S(1)} %slice.237), channel_id=1, source_target_pairs={{0,4},{4,8},{8,12},{12,16},{16,20},{20,24},{24,28},{28,32},{32,36}... | collective-permute-start | bytes 46088 | tf_op jit(solution)/shard_map/ppermute | solution.py:48
  233.3 9.6 %all-to-all-start.1 = ((f32[4,1,256]{2,1,0:T(1,128)}), f32[4,1,256]{2,1,0:T(1,128)S(1)}, u32[]{:S(2)}, u32[]{:S(2)}) async-start(f32[4,1,256]{2,1,0:T(1,128)} %broadcast_in_dim.29), calls=%async_computation.1 | async-start | bytes 8192 | tf_op jit(solution)/shard_map/all_to_all | solution.py:38
Sparse Core Ops, SparseCore 0:
  12.9 149.5 all-gather.5
  192.5 66.5 all-gather.7
where the time goes:
time: 285 us; the launch traced here: 284 us
  waiting for transfers between devices  161 us (56%)
  blocking collectives  62.7 us (22%)
  starting transfers between devices  15.5 us (5%)
  matrix products  15.2 us (5%)
  between operations  13.7 us (5%)
  local copies, waits for them, and re-layouts  9.17 us (3%)
  other arithmetic  7.39 us (3%)
    all_gather x1, waiting for transfers between devices, rows_first(): out, at, outs = (lax.all_gather(both, axis, axis=0, tiled=True), 0, [])  133 us
    all_gather x5, blocking collectives, entering(): lax.all_gather(part.astype(kind), axis)  50.5 us
    all_gather x1, waiting for transfers between devices, entering(): lax.all_gather(part.astype(kind), axis)  14.4 us
    all_to_all x2, waiting for transfers between devices, sent_to_all(): return lax.all_to_all(copies, axis, split_axis=0, concat_axis=0, tiled=True)  13.3 us
    all_to_all x1, blocking collectives, sent_and_summed(): lax.all_to_all(blocks, axis, split_axis=0, concat_axis=0, tiled=True)  12.2 us
    all_to_all x2, starting transfers between devices, sent_to_all(): return lax.all_to_all(copies, axis, split_axis=0, concat_axis=0, tiled=True)  8.75 us
    dot_general x5, matrix products, project(): jnp.dot(row_piece, weight, preferred_element_type=jnp.float32)  7.87 us
    ppermute x2, starting transfers between devices, passed_along(): lax.ppermute(value, axis, [(source, source + steps) for source in range(i...  6.78 us
  transfers between devices with their start and end apart: 6, of which 4 were waited for; matrix products, arithmetic and copies ran while one was open for 5% of the time, Pallas kernels for 0%

commit v1 on v0

v1 whole, which is shorter than its diff:
```python
import jax
import jax.numpy as jnp
from jax import lax
from jax.experimental import pallas as pl
from jax.experimental.pallas import tpu as pltpu
from jax.sharding import Mesh
from jax.sharding import PartitionSpec as P

Z, X, C, Y = "sp_0", "sp_1", "sp_2", "tp"
SP = (Z, X, C)
SP_TP = (Z, X, C, Y)
NZ, NX, NC, NY = 16, 4, 2, 4
CONV_CH = 1024
CH = 128
ROWS = 256
OWN = 32
BLOCK = 64
TAPS = 31
HALO = 32
STATE_ROWS = 40
norm_eps = 1e-06
layer_eps = 1e-05
HIGH = lax.Precision.HIGHEST
bf16 = jnp.bfloat16
f32 = jnp.float32

VMEM = pl.BlockSpec(memory_space=pltpu.VMEM)
SMEM = pl.BlockSpec(memory_space=pltpu.SMEM)


def kernel_call(body, out, specs, scratch=(), name=None):
    return pl.pallas_call(
        body,
        out_shape=out,
        in_specs=specs,
        out_specs=jax.tree.map(lambda _: VMEM, out),
        scratch_shapes=scratch,
        name=name,
    )


def shape(dims, dtype):
    return jax.ShapeDtypeStruct(dims, dtype)


def matmul(a, b, dims, precision=None):
    return lax.dot_general(
        a, b, (dims, ((), ())), precision=precision, preferred_element_type=f32
    )


def sigmoid(v):
    return 1.0 / (1.0 + jnp.exp(-v))


def silu(v):
    return v * sigmoid(v)


def lane_groups(shape_of):
    return lax.broadcasted_iota(jnp.int32, shape_of, 1) // 32


def own_half(value, core):
    return jnp.where(core == 0, value[:, :CH], value[:, CH:])


def norm_body(tokens, gain, out):
    features = tokens[...].astype(f32)
    normed = (
        features
        * lax.rsqrt(jnp.mean(features * features, axis=1, keepdims=True) + norm_eps)
        * gain[...]
    )
    group = lane_groups((OWN, CH))
    for x in range(NX):
        for j in range(NZ // 4):
            piece = jnp.zeros((OWN, CH), f32)
            for i in range(4):
                at = (4 * j + i) * CH
                source = normed[:, at : at + CH]
                turned = pltpu.roll(source, (32 * (i - x)) % CH, 1) if i != x else source
                piece = jnp.where(group == i, turned, piece)
            to = (x * 4 + j) * CH
            out[:, to : to + CH] = piece.astype(bf16)


def in_order(value):
    pieces = [
        value[(y * NC + c) * OWN : (y * NC + c + 1) * OWN] for c in range(NC) for y in range(NY)
    ]
    return jnp.concatenate(pieces, axis=0)


def local_body(core, projected, margin, jump, inner, decayed, packed):
    c = core[0]
    bound = own_half(margin[...], c)
    both = in_order(projected[...]).astype(f32)
    queries = silu(both[:, :CH])
    keys = bound * sigmoid(-both[:, CH : 2 * CH])
    log_forget = jnp.log1p(-keys)
    inputs = both[:, 2 * CH :].astype(bf16)
    row = lax.broadcasted_iota(jnp.int32, (BLOCK, BLOCK), 0)
    col = lax.broadcasted_iota(jnp.int32, (BLOCK, BLOCK), 1)
    causal = row >= col
    lower = jnp.where(causal, 1.0, 0.0)
    state = jnp.zeros((CH, CH), f32)
    before = jnp.zeros((1, CH), f32)
    for n in range(ROWS // BLOCK):
        at = slice(n * BLOCK, (n + 1) * BLOCK)
        jumps = jump[:, n * BLOCK : (n + 1) * BLOCK]
        jumped = jnp.sum(jnp.where(causal, jumps, 0.0), axis=1, keepdims=True)
        running = matmul(lower, log_forget[at], ((1,), (0,)), HIGH) + jumped
        final = running[BLOCK - 1 : BLOCK]
        scaled = queries[at] * jnp.exp(running)
        scaled_keys = (keys[at] * jnp.exp(-running)).astype(bf16)
        final_keys = (keys[at] * jnp.exp(final - running)).astype(bf16)
        scores = matmul(scaled.astype(bf16), scaled_keys, ((1,), (1,)))
        scores = jnp.where(causal, scores, 0.0).astype(bf16)
        inner[at] = matmul(scores, inputs[at], ((1,), (0,))) + matmul(
            scaled.astype(bf16), state.astype(bf16), ((1,), (1,))
        )
        decayed[at] = (scaled * jnp.exp(before)).astype(bf16)
        state = state * jnp.exp(final) + matmul(inputs[at], final_keys, ((0,), (0,)))
        before = before + final
    high = before.astype(bf16)
    low = (before - high.astype(f32)).astype(bf16)
    first = lax.broadcasted_iota(jnp.int32, (8, CH), 0)
    tail = jnp.where(first == 0, high.astype(f32), jnp.where(first == 1, low.astype(f32), 0.0))
    for x in range(NX):
        packed[x, :OWN] = state[x * OWN : (x + 1) * OWN].astype(bf16)
        packed[x, OWN:] = tail.astype(bf16)


def unpacked(block):
    wide = block.astype(f32)
    return wide[OWN : OWN + 1] + wide[OWN + 1 : OWN + 2], wide[:OWN]


def slab_body(parts, total):
    state = jnp.zeros((OWN, CH), f32)
    decay = jnp.zeros((1, CH), f32)
    for x in range(NX):
        step, add = unpacked(parts[x])
        state = state * jnp.exp(step) + add
        decay = decay + step
    high = decay.astype(bf16).astype(f32)
    low = decay - high
    first = lax.broadcasted_iota(jnp.int32, (8, CH), 0)
    total[:OWN] = state.astype(bf16)
    total[OWN:] = jnp.where(first == 0, high, jnp.where(first == 1, low, 0.0)).astype(bf16)


def prefix_body(place, slabs, parts, starts):
    mine = place[0]
    state = jnp.zeros((OWN, CH), f32)
    for z in range(NZ):
        step, add = unpacked(slabs[z])
        state = jnp.where(z < mine, state * jnp.exp(step) + add, state)
    for x in range(NX):
        starts[x] = state.astype(bf16)
        step, add = unpacked(parts[x])
        state = state * jnp.exp(step) + add


def finish_body(core, inner, decayed, start, gain, outgate, out):
    recurrent = inner[...] + matmul(decayed[...], start[...], ((1,), (1,)))
    scale = lax.rsqrt(jnp.mean(recurrent * recurrent, axis=1, keepdims=True) + norm_eps)
    gate = silu(in_order(outgate[...]).astype(f32))
    out[...] = (recurrent * scale * own_half(gain[...], core[0]) * gate).astype(bf16)


def conv_body(core, projected, halo, taps, out, sums, gated):
    rim = halo[...].astype(f32)
    gated[:HALO] = rim[:, :CH] * sigmoid(rim[:, CH:])
    both = in_order(projected[...]).astype(f32)
    gated[HALO:] = both[:, :CH] * sigmoid(both[:, CH:])
    own_taps = own_half(taps[...], core[0])
    for n in range(ROWS // BLOCK):
        total = jnp.zeros((BLOCK, CH), f32)
        for j in range(TAPS):
            at = n * BLOCK + HALO - TAPS + 1 + j
            total = total + gated[at : at + BLOCK] * own_taps[j : j + 1]
        out[n * BLOCK : (n + 1) * BLOCK] = total.astype(bf16)
    values = out[...].astype(f32)
    ones = jnp.ones((8, CH), f32)
    first_sum = matmul(ones, values, ((1,), (1,)), HIGH)
    second_sum = matmul(ones, values * values, ((1,), (1,)), HIGH)
    row = lax.broadcasted_iota(jnp.int32, (8, ROWS), 0)
    both_sums = jnp.where(row == 0, first_sum, second_sum)
    for k in range(NC * NY):
        sums[k] = both_sums


def channel_body(core, values, sums, gain, bias, out):
    total = sums[0]
    for k in range(1, NC * NY):
        total = total + sums[k]
    row = lax.broadcasted_iota(jnp.int32, (8, CH), 0)
    pick_first = jnp.where(row == 0, 1.0 / CONV_CH, 0.0)
    pick_second = jnp.where(row == 1, 1.0 / CONV_CH, 0.0)
    mean = matmul(total, pick_first, ((0,), (0,)), HIGH)
    variance = matmul(total, pick_second, ((0,), (0,)), HIGH) - mean * mean
    shifted = (values[...].astype(f32) - mean) * lax.rsqrt(variance + layer_eps)
    out[...] = silu(
        shifted * own_half(gain[...], core[0]) + own_half(bias[...], core[0])
    ).astype(bf16)


def last_body(parts, out):
    total = parts[0].astype(f32)
    for y in range(1, NY):
        total = total + parts[y].astype(f32)
    group = lane_groups((OWN, CH))
    for z in range(NZ):
        piece = jnp.zeros((OWN, CH), f32)
        for x in range(NX):
            at = (x * 4 + z // 4) * CH
            source = total[:, at : at + CH]
            shift = (32 * (x - z % 4)) % CH
            turned = pltpu.roll(source, shift, 1) if shift else source
            piece = jnp.where(group == x, turned, piece)
        out[:, z * CH : (z + 1) * CH] = piece.astype(bf16)


def exchanged(x, axes):
    return lax.all_to_all(x, axes, split_axis=0, concat_axis=0, tiled=True)


def to_everyone(x, axes):
    return exchanged(jnp.broadcast_to(x, (lax.axis_size(axes), *x.shape)), axes)


def per_device(
    tokens,
    input_norm_gain,
    convolution_value_weight,
    convolution_gate_weight,
    depthwise_filter_taps,
    channel_norm_gain,
    channel_norm_bias,
    query_projection_weight,
    forget_gate_weight,
    recurrence_value_weight,
    output_gate_weight,
    forget_floor_margin,
    decay_jump_terms,
    head_norm_gain,
    convolution_output_weight,
    recurrence_output_weight,
):
    core = lax.axis_index(C).astype(jnp.int32).reshape(1)
    place = lax.axis_index(Z).astype(jnp.int32).reshape(1)
    width = tokens.shape[1]

    normed = kernel_call(norm_body, shape((OWN, width), bf16), [VMEM, VMEM], name="norm")(
        tokens, input_norm_gain.reshape(1, width)
    )

    weights = (
        query_projection_weight,
        forget_gate_weight,
        recurrence_value_weight,
        convolution_value_weight,
        convolution_gate_weight,
        output_gate_weight,
        convolution_output_weight.T,
        recurrence_output_weight.T,
    )
    jump_high = decay_jump_terms.astype(bf16)
    jump_low = (decay_jump_terms - jump_high.astype(f32)).astype(bf16)
    payload = []
    for c in range(NC):
        half = jnp.concatenate([w[:, c * CH : (c + 1) * CH] for w in weights], axis=1)
        jumps = jnp.concatenate([jump_high[c], jump_low[c]])
        payload.append(
            jnp.concatenate(
                [
                    normed,
                    jnp.concatenate([half[:8], half[8:]], axis=1),
                    jnp.broadcast_to(jnp.tile(jumps, 8), (8, width)),
                ],
                axis=0,
            )
        )
    arrived = exchanged(jnp.stack(payload), C)

    jumps = arrived[:, 40, : 2 * CH].astype(f32)
    jump = (jumps[:, :CH] + jumps[:, CH:]).reshape(1, ROWS)
    pair = arrived[:, 32:40]
    shard = jnp.concatenate([pair[:, :, :1024], pair[:, :, 1024:]], axis=1).reshape(32, 1024)
    rows = to_everyone(arrived[:, :32].reshape(2 * OWN, width), Y).reshape(ROWS, width)

    along = lax.all_gather(shard[:, :768], Z, axis=0, tiled=True)
    rec_weight = to_everyone(along[:, :384], X).reshape(width, 384)
    conv_weight = to_everyone(along[:, 384:768], X).reshape(width, 384)
    out_weight = to_everyone(
        to_everyone(shard[:, 768:], Z).reshape(512, 256), X
    ).reshape(width, 256)

    rec_projected = jnp.dot(rows, rec_weight, preferred_element_type=f32).astype(bf16)
    margin = forget_floor_margin.reshape(1, 2 * CH)
    inner, decayed, packed = kernel_call(
        local_body,
        (shape((ROWS, CH), f32), shape((ROWS, CH), bf16), shape((NX, STATE_ROWS, CH), bf16)),
        [SMEM, VMEM, VMEM, VMEM],
        name="local",
    )(core, rec_projected, margin, jump)
    parts = exchanged(packed, X)
    total = kernel_call(slab_body, shape((STATE_ROWS, CH), bf16), [VMEM], name="slab")(parts)
    slabs = to_everyone(total, Z)
    starts = kernel_call(
        prefix_body, shape((NX, OWN, CH), bf16), [SMEM, VMEM, VMEM], name="prefix"
    )(place, slabs, parts)
    start = exchanged(starts, X).reshape(CH, CH)

    conv_projected = jnp.dot(rows, conv_weight, preferred_element_type=f32).astype(bf16)
    value_gate = conv_projected[:, : 2 * CH]
    chips = NZ * NX
    halo = lax.ppermute(
        value_gate[ROWS - HALO :], (Z, X), [(k, k + 1) for k in range(chips - 1)]
    )
    convolved, sums = kernel_call(
        conv_body,
        (shape((ROWS, CH), bf16), shape((NC * NY, 8, ROWS), f32)),
        [SMEM, VMEM, VMEM, VMEM],
        [pltpu.VMEM((HALO + ROWS, CH), f32)],
        name="conv",
    )(core, value_gate, halo, depthwise_filter_taps)
    all_sums = exchanged(sums, (C, Y))
    conv_out = kernel_call(
        channel_body, shape((ROWS, CH), bf16), [SMEM, VMEM, VMEM, VMEM, VMEM], name="channel"
    )(
        core,
        convolved,
        all_sums,
        channel_norm_gain.reshape(1, 2 * CH),
        channel_norm_bias.reshape(1, 2 * CH),
    )
    rec_out = kernel_call(
        finish_body, shape((ROWS, CH), bf16), [SMEM, VMEM, VMEM, VMEM, VMEM, VMEM], name="finish"
    )(core, inner, decayed, start, head_norm_gain.reshape(1, 2 * CH), conv_projected[:, 2 * CH :])

    both = jnp.concatenate([conv_out, rec_out], axis=1)
    partial = matmul(both, out_weight, ((1,), (1,))).astype(bf16).reshape(NC, ROWS // NC, width)
    pair_sum = exchanged(partial, C).astype(f32).sum(axis=0).astype(bf16)
    pieces = exchanged(pair_sum.reshape(NY, OWN, width), Y)
    return kernel_call(last_body, shape((OWN, width), bf16), [VMEM], name="last")(pieces)


def solution(mesh):
    split = Mesh(mesh.devices.reshape(NZ, NX, NC, mesh.shape["tp"]), SP_TP)
    return jax.shard_map(
        per_device,
        mesh=split,
        in_specs=(
            P(SP_TP, None),
            P(),
            P(SP, "tp"),
            P(SP, "tp"),
            P(None, "tp"),
            P("tp"),
            P("tp"),
            P(SP, "tp"),
            P(SP, "tp"),
            P(SP, "tp"),
            P(SP, "tp"),
            P("tp"),
            P("tp", SP),
            P("tp"),
            P("tp", SP),
            P("tp", SP),
        ),
        out_specs=P(SP_TP, None),
        check_vma=False,
    )
```

time: 285 us -> 211 us (0.74)
  waiting for transfers between devices: 161 us -> 45.2 us
  starting transfers between devices: 15.5 us -> 43.6 us
  blocking collectives: 62.7 us -> 80.8 us
  Pallas kernels: 0 us -> 15.6 us
  between operations: 13.7 us -> 0.21 us
  matrix products: 15.2 us -> 4.66 us
  local copies, waits for them, and re-layouts: 9.17 us -> 14.8 us
  other arithmetic: 7.39 us -> 2.66 us
    all_gather x2 -> x0, waiting for transfers between devices: 147 us -> none  [the longest x1 133 us: rows_first(): out, at, outs = (lax.all_gather(both, axis, axis=0, tiled=True), 0, [])]
    all_to_all x2 -> x7, waiting for transfers between devices: 13.3 us -> 44.5 us  [exchanged(): return lax.all_to_all(x, axes, split_axis=0, concat_axis=0, tiled=True)]
    all_to_all x2 -> x7, starting transfers between devices: 8.75 us -> 38.3 us  [exchanged(): return lax.all_to_all(x, axes, split_axis=0, concat_axis=0, tiled=True)]
    all_to_all x1 -> x5, blocking collectives: 12.2 us -> 40.7 us  [exchanged(): return lax.all_to_all(x, axes, split_axis=0, concat_axis=0, tiled=True)]
    pallas_call x0 -> x8, Pallas kernels: none -> 15.6 us  [the longest x1 2.86 us: per_device(): kernel_call(local_body, (shape((ROWS, CH), f32), shape((ROWS, CH), bf16),...]
    all_gather x5 -> x1, blocking collectives: 50.5 us -> 40.1 us  [per_device(): along = lax.all_gather(shard[:, :768], Z, axis=0, tiled=True)]
    dot_general x10 -> x3, matrix products: 13 us -> 4.66 us  [the longest x1 2.62 us: per_device(): jnp.dot(rows, rec_weight, preferred_element_type=f32).astype(bf16)]
    broadcast_in_dim x2 -> x8, local copies, waits for them, and re-layouts: 1.49 us -> 6.98 us  [the longest x6 6.97 us: to_everyone(): return exchanged(jnp.broadcast_to(x, (lax.axis_size(axes), *x.shape)), axes)]
  transfers between devices with their start and end apart: 6 -> 8, of which waited for: 4 -> 7; matrix products, arithmetic and copies ran while one was open for 5% -> 3% of each run, Pallas kernels for 0% -> 6%
where the time goes in v1:
time: 211 us; the launch traced here: 208 us
  blocking collectives  80.8 us (38%)
  waiting for transfers between devices  45.2 us (21%)
  starting transfers between devices  43.6 us (21%)
  Pallas kernels  15.6 us (7%)
  local copies, waits for them, and re-layouts  14.8 us (7%)
  matrix products  4.66 us (2%)
  other arithmetic  2.66 us (1%)
    all_to_all x7, waiting for transfers between devices, exchanged(): return lax.all_to_all(x, axes, split_axis=0, concat_axis=0, tiled=True)  44.5 us
    all_to_all x5, blocking collectives, exchanged(): return lax.all_to_all(x, axes, split_axis=0, concat_axis=0, tiled=True)  40.7 us
    all_gather x1, blocking collectives, per_device(): along = lax.all_gather(shard[:, :768], Z, axis=0, tiled=True)  40.1 us
    all_to_all x7, starting transfers between devices, exchanged(): return lax.all_to_all(x, axes, split_axis=0, concat_axis=0, tiled=True)  38.3 us
    broadcast_in_dim x6, local copies, waits for them, and re-layouts, to_everyone(): return exchanged(jnp.broadcast_to(x, (lax.axis_size(axes), *x.shape)), axes)  6.97 us
    unnamed x22, local copies, waits for them, and re-layouts  5.69 us
    ppermute x1, starting transfers between devices, per_device(): lax.ppermute(value_gate[ROWS - HALO:], (Z, X), [(k, k + 1) for k in range...  5.34 us
  transfers between devices with their start and end apart: 8, of which 7 were waited for; matrix products, arithmetic and copies ran while one was open for 3% of the time, Pallas kernels for 6%

profile of v1, /device:TPU:6, one launch (start us, length us, event | category | flops | bytes accessed | tf_op | source)
XLA Modules:
  0.0 207.6 jit_solution(13803365608265986019)
XLA Ops:
  9.4 4.0 %all_to_all.60 = bf16[2,48,2048]{2,1,0:T(8,128)(2,1)S(1)} all-to-all(bf16[2,48,2048]{2,1,0:T(8,128)(2,1)S(1)} %pad_maximum_fusion), channel_id=1, replica_groups=mesh['sp_0'=16,'sp_1'=4,'sp_2'=2,'tp'=4] {'sp_2'}, dimensions={0} | all-to-all | bytes 786432 | tf_op jit(solution)/shard_map/all_to_all | solution.py:227
  14.6 4.5 %all-to-all-start.1 = ((bf16[4,64,2048]{2,1,0:T(8,128)(2,1)}), bf16[4,64,2048]{2,1,0:T(8,128)(2,1)S(1)}, u32[]{:S(2)}, u32[]{:S(2)}) async-start(bf16[4,64,2048]{2,1,0:T(8,128)(2,1)} %broadcast_in_dim.26), calls=%async_computation.1 | async-start | bytes 2097152 | tf_op jit(solution)/shard_map/all_to_all | solution.py:227
  19.1 40.1 %all_gather.3 = bf16[512,768]{1,0:T(8,128)(2,1)S(1)} all-gather(bf16[32,768]{1,0:T(8,128)(2,1)S(1)} %slice.163), channel_id=1, replica_groups=mesh['sp_0'=16,'sp_1'=4,'sp_2'=2,'tp'=4] {'sp_0'}, dimensions={0}, use_global_device_ids=true | all-gather | bytes 835584 | tf_op jit(solution)/shard_map/all_gather | solution.py:294
  60.8 4.8 %all-to-all-start.4 = ((bf16[4,512,384]{2,1,0:T(8,128)(2,1)}), bf16[4,512,384]{2,1,0:T(8,128)(2,1)S(1)}, u32[]{:S(2)}, u32[]{:S(2)}) async-start(bf16[4,512,384]{2,1,0:T(8,128)(2,1)} %broadcast_in_dim.28), calls=%async_computation.4 | async-start | bytes 3145728 | tf_op jit(solution)/shard_map/all_to_all | solution.py:227
  65.5 11.8 %all-to-all-done.4 = bf16[4,512,384]{2,1,0:T(8,128)(2,1)S(1)} async-done(((bf16[4,512,384]{2,1,0:T(8,128)(2,1)}), bf16[4,512,384]{2,1,0:T(8,128)(2,1)S(1)}, u32[]{:S(2)}, u32[]{:S(2)}) %all-to-all-start.4) | async-done | bytes 1572896 | tf_op jit(solution)/shard_map/all_to_all | solution.py:227
  78.0 7.8 %all-to-all-start.8 = ((bf16[16,32,256]{2,1,0:T(8,128)(2,1)}), bf16[16,32,256]{2,1,0:T(8,128)(2,1)S(1)}, u32[]{:S(2)}, u32[]{:S(2)}) async-start(bf16[16,32,256]{2,1,0:T(8,128)(2,1)} %broadcast_in_dim.30), calls=%async_computation.8 | async-start | bytes 524288 | tf_op jit(solution)/shard_map/all_to_all | solution.py:227
  86.5 2.6 %convolution_convert_fusion.1.projected = bf16[256,384]{1,0:T(8,128)(2,1)} fusion(bf16[256,2048]{1,0:T(8,128)(2,1)} %bitcast.53, bf16[2048,384]{1,0:T(8,128)(2,1)S(1)} %bitcast.49), kind=kOutput, calls=%fused_computation.1 | convolution fusion | flops 402751488 | bytes 2818048 | tf_op jit(solution)/shard_map/dot_general | solution.py:301
  89.1 2.9 %local.1 = (f32[256,128]{1,0:T(8,128)}, bf16[256,128]{1,0:T(8,128)(2,1)}, bf16[4,40,128]{2,1,0:T(8,128)(2,1)}) custom-call(s32[1]{0:T(128)} %bitcast.core, bf16[256,384]{1,0:T(8,128)(2,1)} %convolution_convert_fusion.1.projected, f32[1,256]{1,0:T(1,128)} %bitcast.65, f32[1,256]{1,0:T(1,128)} %bitcast.64), custom_call_target="tpu_custom_call" | custom-call | tf_op jit(solution)/shard_map/local/pallas_call | solution.py:303
  92.0 7.7 %all-to-all-done.8 = bf16[16,32,256]{2,1,0:T(8,128)(2,1)S(1)} async-done(((bf16[16,32,256]{2,1,0:T(8,128)(2,1)}), bf16[16,32,256]{2,1,0:T(8,128)(2,1)S(1)}, u32[]{:S(2)}, u32[]{:S(2)}) %all-to-all-start.8) | async-done | bytes 262176 | tf_op jit(solution)/shard_map/all_to_all | solution.py:227
  99.7 9.5 %all_to_all.61.parts = bf16[4,40,128]{2,1,0:T(8,128)(2,1)} all-to-all(bf16[4,40,128]{2,1,0:T(8,128)(2,1)} %get-tuple-element.14), channel_id=1, replica_groups=mesh['sp_0'=16,'sp_1'=4,'sp_2'=2,'tp'=4] {'sp_1'}, dimensions={0} | all-to-all | bytes 81920 | tf_op jit(solution)/shard_map/all_to_all | solution.py:227
  110.5 5.7 %all-to-all-start.2 = ((bf16[4,512,384]{2,1,0:T(8,128)(2,1)}), bf16[4,512,384]{2,1,0:T(8,128)(2,1)S(1)}, u32[]{:S(2)}, u32[]{:S(2)}) async-start(bf16[4,512,384]{2,1,0:T(8,128)(2,1)} %broadcast_in_dim.27), calls=%async_computation.2 | async-start | bytes 3145728 | tf_op jit(solution)/shard_map/all_to_all | solution.py:227
  117.6 10.2 %all-to-all-done.2 = bf16[4,512,384]{2,1,0:T(8,128)(2,1)S(1)} async-done(((bf16[4,512,384]{2,1,0:T(8,128)(2,1)}), bf16[4,512,384]{2,1,0:T(8,128)(2,1)S(1)}, u32[]{:S(2)}, u32[]{:S(2)}) %all-to-all-start.2) | async-done | bytes 1572896 | tf_op jit(solution)/shard_map/all_to_all | solution.py:227
  129.3 6.2 %all-to-all-start.6 = ((bf16[16,40,128]{2,1,0:T(8,128)(2,1)}), bf16[16,40,128]{2,1,0:T(8,128)(2,1)S(1)}, u32[]{:S(2)}, u32[]{:S(2)}) async-start(bf16[16,40,128]{2,1,0:T(8,128)(2,1)} %broadcast_in_dim.29), calls=%async_computation.6 | async-start | bytes 327680 | tf_op jit(solution)/shard_map/all_to_all | solution.py:227
  136.2 5.3 %collective-permute-start = (bf16[32,256]{1,0:T(8,128)(2,1)S(1)}, bf16[32,256]{1,0:T(8,128)(2,1)S(1)}, u32[]{:S(2)}, u32[]{:S(2)}) collective-permute-start(bf16[32,256]{1,0:T(8,128)(2,1)S(1)} %slice.166), channel_id=1, source_target_pairs={{0,8},{8,16},{16,24},{24,32},{32,40},{40,48},{48,56},{56,64},{64,7... | collective-permute-start | bytes 49160 | tf_op jit(solution)/shard_map/ppermute | solution.py:320
  143.5 2.2 %conv.1 = (bf16[256,128]{1,0:T(8,128)(2,1)}, f32[8,8,256]{2,1,0:T(8,128)}) custom-call(s32[1]{0:T(128)} %bitcast.core, bf16[256,256]{1,0:T(8,128)(2,1)} %slice.165.projected, bf16[32,256]{1,0:T(8,128)(2,1)} %copy-done.4, f32[31,256]{1,0:T(8,128)} %taps.1), custom_call_target="tpu_custom_call" | custom-call | tf_op jit(solution)/shard_map/conv/pallas_call | solution.py:323
  145.7 3.0 %all-to-all-done.6.slabs = bf16[16,40,128]{2,1,0:T(8,128)(2,1)S(1)} async-done(((bf16[16,40,128]{2,1,0:T(8,128)(2,1)}), bf16[16,40,128]{2,1,0:T(8,128)(2,1)S(1)}, u32[]{:S(2)}, u32[]{:S(2)}) %all-to-all-start.6) | async-done | bytes 163872 | tf_op jit(solution)/shard_map/all_to_all | solution.py:227
  148.8 3.8 %all-to-all-start.3 = ((f32[8,8,256]{2,1,0:T(8,128)}), f32[8,8,256]{2,1,0:T(8,128)S(1)}, u32[]{:S(2)}, u32[]{:S(2)}) async-start(f32[8,8,256]{2,1,0:T(8,128)} %get-tuple-element.11), calls=%async_computation.3 | async-start | bytes 131072 | tf_op jit(solution)/shard_map/all_to_all | solution.py:227
  154.1 3.8 %all-to-all-done.3.sums = f32[8,8,256]{2,1,0:T(8,128)S(1)} async-done(((f32[8,8,256]{2,1,0:T(8,128)}), f32[8,8,256]{2,1,0:T(8,128)S(1)}, u32[]{:S(2)}, u32[]{:S(2)}) %all-to-all-start.3) | async-done | bytes 65568 | tf_op jit(solution)/shard_map/all_to_all | solution.py:227
  157.9 9.4 %all_to_all.62 = bf16[4,32,128]{2,1,0:T(8,128)(2,1)} all-to-all(bf16[4,32,128]{2,1,0:T(8,128)(2,1)} %prefix.1), channel_id=1, replica_groups=mesh['sp_0'=16,'sp_1'=4,'sp_2'=2,'tp'=4] {'sp_1'}, dimensions={0} | all-to-all | bytes 65536 | tf_op jit(solution)/shard_map/all_to_all | solution.py:227
  168.3 5.6 %all-to-all-start.9 = ((bf16[4,512,256]{2,1,0:T(8,128)(2,1)}), bf16[4,512,256]{2,1,0:T(8,128)(2,1)S(1)}, u32[]{:S(2)}, u32[]{:S(2)}) async-start(bf16[4,512,256]{2,1,0:T(8,128)(2,1)} %broadcast_in_dim.31), calls=%async_computation.9 | async-start | bytes 2097152 | tf_op jit(solution)/shard_map/all_to_all | solution.py:227
  174.5 2.0 channel.1
  178.3 8.0 %all-to-all-done.9 = bf16[4,512,256]{2,1,0:T(8,128)(2,1)S(1)} async-done(((bf16[4,512,256]{2,1,0:T(8,128)(2,1)}), bf16[4,512,256]{2,1,0:T(8,128)(2,1)S(1)}, u32[]{:S(2)}, u32[]{:S(2)}) %all-to-all-start.9) | async-done | bytes 1048608 | tf_op jit(solution)/shard_map/all_to_all | solution.py:227
  187.7 4.6 %all_to_all.63 = bf16[2,128,2048]{2,1,0:T(8,128)(2,1)S(1)} all-to-all(bf16[2,128,2048]{2,1,0:T(8,128)(2,1)S(1)} %bitcast.47), channel_id=1, replica_groups=mesh['sp_0'=16,'sp_1'=4,'sp_2'=2,'tp'=4] {'sp_2'}, dimensions={0} | all-to-all | bytes 2097152 | tf_op jit(solution)/shard_map/all_to_all | solution.py:227
  192.6 13.1 %all_to_all.64.parts = bf16[4,32,2048]{2,1,0:T(8,128)(2,1)} all-to-all(bf16[4,32,2048]{2,1,0:T(8,128)(2,1)S(1)} %bitcast.48), channel_id=1, replica_groups=mesh['sp_0'=16,'sp_1'=4,'sp_2'=2,'tp'=4] {'tp'}, dimensions={0} | all-to-all | bytes 1048576 | tf_op jit(solution)/shard_map/all_to_all | solution.py:227
  (59 shorter events, 28.8 us)
Async XLA Ops:
  14.6 44.7 %all-to-all-start.1 = ((bf16[4,64,2048]{2,1,0:T(8,128)(2,1)}), bf16[4,64,2048]{2,1,0:T(8,128)(2,1)S(1)}, u32[]{:S(2)}, u32[]{:S(2)}) async-start(bf16[4,64,2048]{2,1,0:T(8,128)(2,1)} %broadcast_in_dim.26), calls=%async_computation.1 | async-start | bytes 2097152 | tf_op jit(solution)/shard_map/all_to_all | solution.py:227
  59.3 1.5 copy-start
  60.8 16.5 %all-to-all-start.4 = ((bf16[4,512,384]{2,1,0:T(8,128)(2,1)}), bf16[4,512,384]{2,1,0:T(8,128)(2,1)S(1)}, u32[]{:S(2)}, u32[]{:S(2)}) async-start(bf16[4,512,384]{2,1,0:T(8,128)(2,1)} %broadcast_in_dim.28), calls=%async_computation.4 | async-start | bytes 3145728 | tf_op jit(solution)/shard_map/all_to_all | solution.py:227
  78.0 21.6 %all-to-all-start.8 = ((bf16[16,32,256]{2,1,0:T(8,128)(2,1)}), bf16[16,32,256]{2,1,0:T(8,128)(2,1)S(1)}, u32[]{:S(2)}, u32[]{:S(2)}) async-start(bf16[16,32,256]{2,1,0:T(8,128)(2,1)} %broadcast_in_dim.30), calls=%async_computation.8 | async-start | bytes 524288 | tf_op jit(solution)/shard_map/all_to_all | solution.py:227
  110.5 24.9 %copy-start.1 = (bf16[4,64,2048]{2,1,0:T(8,128)(2,1)S(1)}, bf16[4,64,2048]{2,1,0:T(8,128)(2,1)}, u32[]{:S(2)}) copy-start(bf16[4,64,2048]{2,1,0:T(8,128)(2,1)} %copy-done) | copy-start | bytes 3145732
  110.5 17.4 %all-to-all-start.2 = ((bf16[4,512,384]{2,1,0:T(8,128)(2,1)}), bf16[4,512,384]{2,1,0:T(8,128)(2,1)S(1)}, u32[]{:S(2)}, u32[]{:S(2)}) async-start(bf16[4,512,384]{2,1,0:T(8,128)(2,1)} %broadcast_in_dim.27), calls=%async_computation.2 | async-start | bytes 3145728 | tf_op jit(solution)/shard_map/all_to_all | solution.py:227
  129.3 19.5 %all-to-all-start.6 = ((bf16[16,40,128]{2,1,0:T(8,128)(2,1)}), bf16[16,40,128]{2,1,0:T(8,128)(2,1)S(1)}, u32[]{:S(2)}, u32[]{:S(2)}) async-start(bf16[16,40,128]{2,1,0:T(8,128)(2,1)} %broadcast_in_dim.29), calls=%async_computation.6 | async-start | bytes 327680 | tf_op jit(solution)/shard_map/all_to_all | solution.py:227
  136.2 6.8 %collective-permute-start = (bf16[32,256]{1,0:T(8,128)(2,1)S(1)}, bf16[32,256]{1,0:T(8,128)(2,1)S(1)}, u32[]{:S(2)}, u32[]{:S(2)}) collective-permute-start(bf16[32,256]{1,0:T(8,128)(2,1)S(1)} %slice.166), channel_id=1, source_target_pairs={{0,8},{8,16},{16,24},{24,32},{32,40},{40,48},{48,56},{56,64},{64,7... | collective-permute-start | bytes 49160 | tf_op jit(solution)/shard_map/ppermute | solution.py:320
  142.9 0.6 copy-start.4
  148.8 3.8 %copy-start.2 = (bf16[16,40,128]{2,1,0:T(8,128)(2,1)}, bf16[16,40,128]{2,1,0:T(8,128)(2,1)S(1)}, u32[]{:S(2)}) copy-start(bf16[16,40,128]{2,1,0:T(8,128)(2,1)S(1)} %all-to-all-done.6.slabs) | copy-start | bytes 491524
  148.8 9.1 %all-to-all-start.3 = ((f32[8,8,256]{2,1,0:T(8,128)}), f32[8,8,256]{2,1,0:T(8,128)S(1)}, u32[]{:S(2)}, u32[]{:S(2)}) async-start(f32[8,8,256]{2,1,0:T(8,128)} %get-tuple-element.11), calls=%async_computation.3 | async-start | bytes 131072 | tf_op jit(solution)/shard_map/all_to_all | solution.py:227
  157.9 10.4 %copy-start.3 = (f32[8,8,256]{2,1,0:T(8,128)}, f32[8,8,256]{2,1,0:T(8,128)S(1)}, u32[]{:S(2)}) copy-start(f32[8,8,256]{2,1,0:T(8,128)S(1)} %all-to-all-done.3.sums) | copy-start | bytes 196612
  168.3 18.0 %all-to-all-start.9 = ((bf16[4,512,256]{2,1,0:T(8,128)(2,1)}), bf16[4,512,256]{2,1,0:T(8,128)(2,1)S(1)}, u32[]{:S(2)}, u32[]{:S(2)}) async-start(bf16[4,512,256]{2,1,0:T(8,128)(2,1)} %broadcast_in_dim.31), calls=%async_computation.9 | async-start | bytes 2097152 | tf_op jit(solution)/shard_map/all_to_all | solution.py:227

commit v2 on v1

v2 whole, which is shorter than its diff:
```python
import jax
import jax.numpy as jnp
from jax import lax
from jax.experimental import pallas as pl
from jax.experimental.pallas import tpu as pltpu
from jax.sharding import Mesh
from jax.sharding import PartitionSpec as P


ZH, ZL, X, C, Y = "sp_0", "sp_1", "sp_2", "sp_3", "tp"
SP = (ZH, ZL, X, C)
SP_TP = (ZH, ZL, X, C, Y)
NZ, NQ, NX, NC, NY = 16, 4, 4, 2, 4
CONV_CH = 1024
CH = 128
ROWS = 256
OWN = 32
BLOCK = 64
TAPS = 31
HALO = 32
STATE_ROWS = 136
PAIR = 64
norm_eps = 1e-06
layer_eps = 1e-05
HIGH = lax.Precision.HIGHEST
bf16 = jnp.bfloat16
f32 = jnp.float32

VMEM = pl.BlockSpec(memory_space=pltpu.VMEM)
SMEM = pl.BlockSpec(memory_space=pltpu.SMEM)


def kernel_call(body, out, specs, scratch=()):
    return pl.pallas_call(
        body,
        out_shape=out,
        in_specs=specs,
        out_specs=jax.tree.map(lambda _: VMEM, out),
        scratch_shapes=scratch,
    )


def shape(dims, dtype):
    return jax.ShapeDtypeStruct(dims, dtype)


def matmul(a, b, dims, precision=None):
    return lax.dot_general(
        a, b, (dims, ((), ())), precision=precision, preferred_element_type=f32
    )


def sigmoid(v):
    return 1.0 / (1.0 + jnp.exp(-v))


def silu(v):
    return v * sigmoid(v)


def lane_groups(shape_of):
    return lax.broadcasted_iota(jnp.int32, shape_of, 1) // 32


def own_half(value, core):
    return jnp.where(core == 0, value[:, :CH], value[:, CH:])


def prepare_body(tokens, gain, query, forget, value, left, gate, outgate, conv_out, rec_out, jump, out):
    features = tokens[...].astype(f32)
    normed = (
        features
        * lax.rsqrt(jnp.mean(features * features, axis=1, keepdims=True) + norm_eps)
        * gain[...]
    )
    group = lane_groups((OWN, CH))
    for x in range(NX):
        for j in range(NZ // 4):
            piece = jnp.zeros((OWN, CH), f32)
            for i in range(4):
                at = (4 * j + i) * CH
                source = normed[:, at : at + CH]
                turned = pltpu.roll(source, (32 * (i - x)) % CH, 1) if i != x else source
                piece = jnp.where(group == i, turned, piece)
            to = (x * 4 + j) * CH
            for c in range(NC):
                out[c, :OWN, to : to + CH] = piece.astype(bf16)
    side = 2 * CH
    same = (
        lax.broadcasted_iota(jnp.int32, (side, side), 0)
        == lax.broadcasted_iota(jnp.int32, (side, side), 1)
    )
    identity = jnp.where(same, 1.0, 0.0).astype(bf16)
    blocks = [w[...].astype(f32) for w in (query, forget, value, left, gate, outgate)]
    blocks += [matmul(w[...], identity, ((0,), (0,))) for w in (conv_out, rec_out)]
    for c in range(NC):
        for k, block in enumerate(blocks):
            half = block[:, c * CH : (c + 1) * CH].astype(bf16)
            out[c, OWN : OWN + 8, k * CH : (k + 1) * CH] = half[:8]
            out[c, OWN : OWN + 8, (8 + k) * CH : (9 + k) * CH] = half[8:]
        row = jnp.broadcast_to(jump[c : c + 1], (8, CH))
        high = row.astype(bf16)
        out[c, OWN + 8 :, :CH] = high
        out[c, OWN + 8 :, CH : 2 * CH] = (row - high.astype(f32)).astype(bf16)
        out[c, OWN + 8 :, 2 * CH :] = jnp.zeros((8, 14 * CH), bf16)


def in_order(ref, y):
    pieces = []
    for c in range(NC):
        for k in range(NY):
            slot = lax.rem(k - y + NY, NY)
            at = pl.multiple_of(slot * PAIR + c * OWN, OWN)
            pieces.append(ref[pl.ds(at, OWN)])
    return jnp.concatenate(pieces, axis=0)


def local_body(place, own, next_one, across, last_one, weight, margin, jump, inner, decayed, packed, projected):
    c = place[3]
    for k, piece in enumerate((own, next_one, across, last_one)):
        projected[k * PAIR : (k + 1) * PAIR] = matmul(piece[...], weight[...], ((1,), (0,)))
    bound = own_half(margin[...], c)
    both = in_order(projected, place[4]).astype(bf16).astype(f32)
    queries = silu(both[:, :CH])
    keys = bound * sigmoid(-both[:, CH : 2 * CH])
    log_forget = jnp.log1p(-keys)
    inputs = both[:, 2 * CH :].astype(bf16)
    row = lax.broadcasted_iota(jnp.int32, (BLOCK, BLOCK), 0)
    col = lax.broadcasted_iota(jnp.int32, (BLOCK, BLOCK), 1)
    causal = row >= col
    lower = jnp.where(causal, 1.0, 0.0)
    state = jnp.zeros((CH, CH), f32)
    before = jnp.zeros((1, CH), f32)
    for n in range(ROWS // BLOCK):
        at = slice(n * BLOCK, (n + 1) * BLOCK)
        jumps = jump[:, n * BLOCK : (n + 1) * BLOCK]
        jumped = jnp.sum(jnp.where(causal, jumps, 0.0), axis=1, keepdims=True)
        running = matmul(lower, log_forget[at], ((1,), (0,)), HIGH) + jumped
        final = running[BLOCK - 1 : BLOCK]
        scaled = queries[at] * jnp.exp(running)
        scaled_keys = (keys[at] * jnp.exp(-running)).astype(bf16)
        final_keys = (keys[at] * jnp.exp(final - running)).astype(bf16)
        scores = matmul(scaled.astype(bf16), scaled_keys, ((1,), (1,)))
        scores = jnp.where(causal, scores, 0.0).astype(bf16)
        inner[at] = matmul(scores, inputs[at], ((1,), (0,))) + matmul(
            scaled.astype(bf16), state.astype(bf16), ((1,), (1,))
        )
        decayed[at] = (scaled * jnp.exp(before)).astype(bf16)
        state = state * jnp.exp(final) + matmul(inputs[at], final_keys, ((0,), (0,)))
        before = before + final
    pack(packed, state, before)


def pack(ref, state, decay):
    high = decay.astype(bf16).astype(f32)
    low = decay - high
    first = lax.broadcasted_iota(jnp.int32, (8, CH), 0)
    ref[:CH] = state.astype(bf16)
    ref[CH:] = jnp.where(first == 0, high, jnp.where(first == 1, low, 0.0)).astype(bf16)


def unpacked(block):
    wide = block.astype(f32)
    return wide[CH : CH + 1] + wide[CH + 1 : CH + 2], wide[:CH]


def total_body(parts, total):
    state = jnp.zeros((CH, CH), f32)
    decay = jnp.zeros((1, CH), f32)
    for k in range(NQ):
        step, add = unpacked(parts[k])
        state = state * jnp.exp(step) + add
        decay = decay + step
    pack(total, state, decay)


def finish_body(place, quads, slabs, chips, inner, decayed, gain, outgate, out):
    state = jnp.zeros((CH, CH), f32)
    for level, parts in enumerate((quads, slabs, chips)):
        for k in range(NQ):
            step, add = unpacked(parts[k])
            state = jnp.where(k < place[level], state * jnp.exp(step) + add, state)
    recurrent = inner[...] + matmul(decayed[...], state.astype(bf16), ((1,), (1,)))
    scale = lax.rsqrt(jnp.mean(recurrent * recurrent, axis=1, keepdims=True) + norm_eps)
    gate = silu(outgate[...].astype(f32))
    out[...] = (recurrent * scale * own_half(gain[...], place[3]) * gate).astype(bf16)


def project_body(place, own, next_one, across, last_one, weight, value_gate, outgate, tail, projected):
    for k, piece in enumerate((own, next_one, across, last_one)):
        projected[k * PAIR : (k + 1) * PAIR] = matmul(piece[...], weight[...], ((1,), (0,)))
    ordered = in_order(projected, place[4]).astype(bf16)
    value_gate[...] = ordered[:, : 2 * CH]
    outgate[...] = ordered[:, 2 * CH :]
    tail[...] = ordered[ROWS - HALO :, : 2 * CH]


def conv_body(place, projected, halo, taps, out, sums, gated):
    rim = halo[...].astype(f32)
    gated[:HALO] = rim[:, :CH] * sigmoid(rim[:, CH:])
    both = projected[...].astype(f32)
    gated[HALO:] = both[:, :CH] * sigmoid(both[:, CH:])
    own_taps = own_half(taps[...], place[3])
    for n in range(ROWS // BLOCK):
        total = jnp.zeros((BLOCK, CH), f32)
        for j in range(TAPS):
            at = n * BLOCK + HALO - TAPS + 1 + j
            total = total + gated[at : at + BLOCK] * own_taps[j : j + 1]
        out[n * BLOCK : (n + 1) * BLOCK] = total.astype(bf16)
    values = out[...].astype(f32)
    ones = jnp.ones((8, CH), f32)
    first_sum = matmul(ones, values, ((1,), (1,)), HIGH)
    second_sum = matmul(ones, values * values, ((1,), (1,)), HIGH)
    row = lax.broadcasted_iota(jnp.int32, (8, ROWS), 0)
    sums[...] = jnp.where(row == 0, first_sum, second_sum)


def channel_body(place, values, sums, gain, bias, out):
    total = sums[0]
    for k in range(1, NC * NY):
        total = total + sums[k]
    row = lax.broadcasted_iota(jnp.int32, (8, CH), 0)
    pick_first = jnp.where(row == 0, 1.0 / CONV_CH, 0.0)
    pick_second = jnp.where(row == 1, 1.0 / CONV_CH, 0.0)
    mean = matmul(total, pick_first, ((0,), (0,)), HIGH)
    variance = matmul(total, pick_second, ((0,), (0,)), HIGH) - mean * mean
    shifted = (values[...].astype(f32) - mean) * lax.rsqrt(variance + layer_eps)
    out[...] = silu(
        shifted * own_half(gain[...], place[3]) + own_half(bias[...], place[3])
    ).astype(bf16)


def output_body(place, conv_out, rec_out, own, next_one, across, last_one, out):
    both = jnp.concatenate([conv_out[...], rec_out[...]], axis=1)
    step = own.shape[0]
    for k, piece in enumerate((own, next_one, across, last_one)):
        result = matmul(both, piece[...], ((1,), (1,))).astype(bf16)
        at = pl.multiple_of(lax.rem(place[2] + k, NX) * step, step)
        for c in range(NC):
            out[c, :, pl.ds(at, step)] = result[c * (ROWS // NC) : (c + 1) * (ROWS // NC)]


def last_body(parts, out):
    total = parts[0].astype(f32)
    for y in range(1, NY):
        total = total + parts[y].astype(f32)
    group = lane_groups((OWN, CH))
    for z in range(NZ):
        piece = jnp.zeros((OWN, CH), f32)
        for x in range(NX):
            at = (x * 4 + z // 4) * CH
            source = total[:, at : at + CH]
            shift = (32 * (x - z % 4)) % CH
            turned = pltpu.roll(source, shift, 1) if shift else source
            piece = jnp.where(group == x, turned, piece)
        out[:, z * CH : (z + 1) * CH] = piece.astype(bf16)


def exchanged(x, axes):
    return lax.all_to_all(x, axes, split_axis=0, concat_axis=0, tiled=True)


def to_everyone(x, axes):
    copies = jnp.broadcast_to(x, (lax.axis_size(axes), *x.shape))
    return exchanged(copies, axes)


def shifted(x, axis):
    count = lax.axis_size(axis)
    pieces = []
    for steps in range(1, count):
        pieces.append(
            lax.ppermute(x, axis, [((k + steps) % count, k) for k in range(count)])
        )
    return pieces


def per_device(
    tokens,
    input_norm_gain,
    convolution_value_weight,
    convolution_gate_weight,
    depthwise_filter_taps,
    channel_norm_gain,
    channel_norm_bias,
    query_projection_weight,
    forget_gate_weight,
    recurrence_value_weight,
    output_gate_weight,
    forget_floor_margin,
    decay_jump_terms,
    head_norm_gain,
    convolution_output_weight,
    recurrence_output_weight,
):
    place = jnp.stack([lax.axis_index(a) for a in SP_TP]).astype(jnp.int32)
    width = tokens.shape[1]

    payload = kernel_call(prepare_body, shape((NC, 48, width), bf16), [VMEM] * 11)(
        tokens,
        input_norm_gain.reshape(1, width),
        query_projection_weight,
        forget_gate_weight,
        recurrence_value_weight,
        convolution_value_weight,
        convolution_gate_weight,
        output_gate_weight,
        convolution_output_weight,
        recurrence_output_weight,
        decay_jump_terms,
    )
    arrived = exchanged(payload, C)
    jumps = arrived[:, 40, : 2 * CH].astype(f32)
    jump = (jumps[:, :CH] + jumps[:, CH:]).reshape(1, ROWS)
    pair = arrived[:, 32:40]
    shard = jnp.concatenate([pair[:, :, :1024], pair[:, :, 1024:]], axis=1).reshape(32, 1024)
    own = arrived[:, :32].reshape(PAIR, width)
    rows = (own, *shifted(own, Y))

    out_along = to_everyone(shard[:, 768:], (ZH, ZL)).reshape(512, 256)
    along = lax.all_gather(shard[:, :768], (ZH, ZL), axis=0, tiled=True)
    rec_weight = to_everyone(along[:, :384], X).reshape(width, 384)
    conv_weight = to_everyone(along[:, 384:768], X).reshape(width, 384)

    margin = forget_floor_margin.reshape(1, 2 * CH)
    inner, decayed, packed = kernel_call(
        local_body,
        (shape((ROWS, CH), f32), shape((ROWS, CH), bf16), shape((STATE_ROWS, CH), bf16)),
        [SMEM] + [VMEM] * 7,
        [pltpu.VMEM((ROWS, 3 * CH), f32)],
    )(place, *rows, rec_weight, margin, jump)
    chips = lax.all_gather(packed, X, axis=0)

    def total_of(parts):
        return kernel_call(total_body, shape((STATE_ROWS, CH), bf16), [VMEM])(parts)

    slabs = to_everyone(total_of(chips), ZL)
    quads = to_everyone(total_of(slabs), ZH)

    out_pieces = (out_along, *shifted(out_along, X))

    value_gate, outgate, tail = kernel_call(
        project_body,
        (shape((ROWS, 2 * CH), bf16), shape((ROWS, CH), bf16), shape((HALO, 2 * CH), bf16)),
        [SMEM] + [VMEM] * 5,
        [pltpu.VMEM((ROWS, 3 * CH), f32)],
    )(place, *rows, conv_weight)
    blocks = NZ * NX
    halo = lax.ppermute(tail, (ZH, ZL, X), [(k, k + 1) for k in range(blocks - 1)])
    convolved, sums = kernel_call(
        conv_body,
        (shape((ROWS, CH), bf16), shape((8, ROWS), f32)),
        [SMEM, VMEM, VMEM, VMEM],
        [pltpu.VMEM((HALO + ROWS, CH), f32)],
    )(place, value_gate, halo, depthwise_filter_taps)
    all_sums = lax.all_gather(sums, (C, Y), axis=0)
    conv_out = kernel_call(channel_body, shape((ROWS, CH), bf16), [SMEM, VMEM, VMEM, VMEM, VMEM])(
        place,
        convolved,
        all_sums,
        channel_norm_gain.reshape(1, 2 * CH),
        channel_norm_bias.reshape(1, 2 * CH),
    )
    rec_out = kernel_call(
        finish_body, shape((ROWS, CH), bf16), [SMEM] + [VMEM] * 7
    )(place, quads, slabs, chips, inner, decayed, head_norm_gain.reshape(1, 2 * CH), outgate)

    partial = kernel_call(
        output_body, shape((NC, ROWS // NC, width), bf16), [SMEM] + [VMEM] * 6
    )(place, conv_out, rec_out, *out_pieces)
    pair_sum = exchanged(partial, C).astype(f32).sum(axis=0).astype(bf16)
    pieces = exchanged(pair_sum.reshape(NY, OWN, width), Y)
    return kernel_call(last_body, shape((OWN, width), bf16), [VMEM])(pieces)


def solution(mesh):
    split = Mesh(mesh.devices.reshape(NQ, NZ // NQ, NX, NC, mesh.shape["tp"]), SP_TP)
    return jax.shard_map(
        per_device,
        mesh=split,
        in_specs=(
            P(SP_TP, None),
            P(),
            P(SP, "tp"),
            P(SP, "tp"),
            P(None, "tp"),
            P("tp"),
            P("tp"),
            P(SP, "tp"),
            P(SP, "tp"),
            P(SP, "tp"),
            P(SP, "tp"),
            P("tp"),
            P("tp", SP),
            P("tp"),
            P("tp", SP),
            P("tp", SP),
        ),
        out_specs=P(SP_TP, None),
        check_vma=False,
    )
```

time: 211 us -> 235 us (1.11)
  blocking collectives: 80.8 us -> 112 us
  waiting for transfers between devices: 45.2 us -> 32.3 us
  Pallas kernels: 15.6 us -> 24.8 us
  starting transfers between devices: 43.6 us -> 49.5 us
  matrix products: 4.66 us -> 0 us
  local copies, waits for them, and re-layouts: 14.8 us -> 12 us
    all_gather x1 -> x3, blocking collectives: 40.1 us -> 76.5 us  [the longest x1 39.8 us: per_device(): along = lax.all_gather(shard[:, :768], (ZH, ZL), axis=0, tiled=True)]
    all_to_all x7 -> x4, waiting for transfers between devices: 44.5 us -> 22.4 us  [exchanged(): return lax.all_to_all(x, axes, split_axis=0, concat_axis=0, tiled=True)]
    ppermute x1 -> x7, starting transfers between devices: 5.34 us -> 22.7 us  [the longest x6 20.8 us: shifted(): lax.ppermute(x, axis, [((k + steps) % count, k) for k in range(count)])]
    all_to_all x7 -> x4, starting transfers between devices: 38.3 us -> 26.7 us  [exchanged(): return lax.all_to_all(x, axes, split_axis=0, concat_axis=0, tiled=True)]
    ppermute x1 -> x7, waiting for transfers between devices: 0.77 us -> 9.91 us  [the longest x6 6.04 us: shifted(): lax.ppermute(x, axis, [((k + steps) % count, k) for k in range(count)])]
    pallas_call x6 -> x8, Pallas kernels: 10.8 us -> 17.8 us  [the longest x1 3.58 us: per_device(): kernel_call(project_body, (shape((ROWS, 2 * CH), bf16), shape((ROWS, CH),...]
    all_to_all x5 -> x4, blocking collectives: 40.7 us -> 35.5 us  [exchanged(): return lax.all_to_all(x, axes, split_axis=0, concat_axis=0, tiled=True)]
    dot_general x3 -> x0, matrix products: 4.66 us -> none  [the longest x1 2.62 us: per_device(): jnp.dot(rows, rec_weight, preferred_element_type=f32).astype(bf16)]
  transfers between devices with their start and end apart: 8 -> 11, of which waited for: 7 -> 5; matrix products, arithmetic and copies ran while one was open for 3% -> 1% of each run, Pallas kernels for 6% -> 8%
where the time goes in v2:
time: 235 us; the launch traced here: 232 us
  blocking collectives  112 us (48%)
  starting transfers between devices  49.5 us (21%)
  waiting for transfers between devices  32.3 us (14%)
  Pallas kernels  24.8 us (11%)
  local copies, waits for them, and re-layouts  12 us (5%)
    all_gather x1, blocking collectives, per_device(): along = lax.all_gather(shard[:, :768], (ZH, ZL), axis=0, tiled=True)  39.8 us
    all_to_all x4, blocking collectives, exchanged(): return lax.all_to_all(x, axes, split_axis=0, concat_axis=0, tiled=True)  35.5 us
    all_to_all x4, starting transfers between devices, exchanged(): return lax.all_to_all(x, axes, split_axis=0, concat_axis=0, tiled=True)  26.7 us
    all_gather x1, blocking collectives, per_device(): all_sums = lax.all_gather(sums, (C, Y), axis=0)  23.6 us
    all_to_all x4, waiting for transfers between devices, exchanged(): return lax.all_to_all(x, axes, split_axis=0, concat_axis=0, tiled=True)  22.4 us
    ppermute x6, starting transfers between devices, shifted(): lax.ppermute(x, axis, [((k + steps) % count, k) for k in range(count)])  20.8 us
    all_gather x1, blocking collectives, per_device(): chips = lax.all_gather(packed, X, axis=0)  13.2 us
    ppermute x6, waiting for transfers between devices, shifted(): lax.ppermute(x, axis, [((k + steps) % count, k) for k in range(count)])  6.04 us
  transfers between devices with their start and end apart: 11, of which 5 were waited for; matrix products, arithmetic and copies ran while one was open for 1% of the time, Pallas kernels for 8%

profile of v2, /device:TPU:6, one launch (start us, length us, event | category | flops | bytes accessed | tf_op | source)
XLA Modules:
  0.0 231.6 jit_solution(8154554446214770885)
XLA Ops:
  5.0 5.1 %all_to_all.40 = bf16[2,48,2048]{2,1,0:T(8,128)(2,1)S(1)} all-to-all(bf16[2,48,2048]{2,1,0:T(8,128)(2,1)} %shard_map.154), channel_id=1, replica_groups=mesh['sp_0'=4,'sp_1'=4,'sp_2'=4,'sp_3'=2,'tp'=4] {'sp_3'}, dimensions={0} | all-to-all | bytes 786432 | tf_op jit(solution)/shard_map/all_to_all | solution.py:260
  10.1 39.8 %all_gather.15 = bf16[512,768]{1,0:T(8,128)(2,1)S(1)} all-gather(bf16[32,768]{1,0:T(8,128)(2,1)S(1)} %slice.46), channel_id=1, replica_groups=mesh['sp_0'=4,'sp_1'=4,'sp_2'=4,'sp_3'=2,'tp'=4] {'sp_0','sp_1'}, dimensions={0}, use_global_device_ids=true | all-gather | bytes 835584 | tf_op jit(solution)/shard_map/all_gather | solution.py:321
  51.3 4.8 %all-to-all-start.2 = ((bf16[4,512,384]{2,1,0:T(8,128)(2,1)}), bf16[4,512,384]{2,1,0:T(8,128)(2,1)S(1)}, u32[]{:S(2)}, u32[]{:S(2)}) async-start(bf16[4,512,384]{2,1,0:T(8,128)(2,1)} %broadcast_in_dim.16), calls=%async_computation.2 | async-start | bytes 3145728 | tf_op jit(solution)/shard_map/all_to_all | solution.py:260
  56.0 12.3 %all-to-all-done.2 = bf16[4,512,384]{2,1,0:T(8,128)(2,1)S(1)} async-done(((bf16[4,512,384]{2,1,0:T(8,128)(2,1)}), bf16[4,512,384]{2,1,0:T(8,128)(2,1)S(1)}, u32[]{:S(2)}, u32[]{:S(2)}) %all-to-all-start.2) | async-done | bytes 1572896 | tf_op jit(solution)/shard_map/all_to_all | solution.py:260
  69.2 6.5 %all-to-all-start.5 = ((bf16[16,32,256]{2,1,0:T(8,128)(2,1)}), bf16[16,32,256]{2,1,0:T(8,128)(2,1)S(1)}, u32[]{:S(2)}, u32[]{:S(2)}) async-start(bf16[16,32,256]{2,1,0:T(8,128)(2,1)} %broadcast_in_dim.19), calls=%async_computation.5 | async-start | bytes 524288 | tf_op jit(solution)/shard_map/all_to_all | solution.py:260
  75.7 4.9 %collective-permute-start = (bf16[64,2048]{1,0:T(8,128)(2,1)S(1)}, bf16[64,2048]{1,0:T(8,128)(2,1)S(1)}, u32[]{:S(2)}, u32[]{:S(2)}) collective-permute-start(bf16[64,2048]{1,0:T(8,128)(2,1)S(1)} %bitcast.24), channel_id=1, source_target_pairs={{1,0},{2,1},{3,2},{0,3},{5,4},{6,5},{7,6},{4,7},{9,8},{10,9},{11,1... | collective-permute-start | bytes 786440 | tf_op jit(solution)/shard_map/ppermute | solution.py:273
  80.7 2.5 %collective-permute-start.1 = (bf16[64,2048]{1,0:T(8,128)(2,1)S(1)}, bf16[64,2048]{1,0:T(8,128)(2,1)S(1)}, u32[]{:S(2)}, u32[]{:S(2)}) collective-permute-start(bf16[64,2048]{1,0:T(8,128)(2,1)S(1)} %bitcast.25), channel_id=1, source_target_pairs={{2,0},{3,1},{0,2},{1,3},{6,4},{7,5},{4,6},{5,7},{10,8},{11,9},{8,1... | collective-permute-start | bytes 786440 | tf_op jit(solution)/shard_map/ppermute | solution.py:273
  83.2 2.9 %collective-permute-start.2 = (bf16[64,2048]{1,0:T(8,128)(2,1)S(1)}, bf16[64,2048]{1,0:T(8,128)(2,1)}, u32[]{:S(2)}, u32[]{:S(2)}) collective-permute-start(bf16[64,2048]{1,0:T(8,128)(2,1)S(1)} %bitcast.26), channel_id=1, source_target_pairs={{3,0},{0,1},{1,2},{2,3},{7,4},{4,5},{5,6},{6,7},{11,8},{8,9},{9,10... | collective-permute-start | bytes 786440 | tf_op jit(solution)/shard_map/ppermute | solution.py:273
  87.3 3.2 %collective-permute-done.1.across = bf16[64,2048]{1,0:T(8,128)(2,1)S(1)} collective-permute-done((bf16[64,2048]{1,0:T(8,128)(2,1)S(1)}, bf16[64,2048]{1,0:T(8,128)(2,1)S(1)}, u32[]{:S(2)}, u32[]{:S(2)}) %collective-permute-start.1) | collective-permute-done | bytes 262176 | tf_op jit(solution)/shard_map/ppermute | solution.py:273
  90.5 2.9 %collective-permute-done.2.last_one = bf16[64,2048]{1,0:T(8,128)(2,1)} collective-permute-done((bf16[64,2048]{1,0:T(8,128)(2,1)S(1)}, bf16[64,2048]{1,0:T(8,128)(2,1)}, u32[]{:S(2)}, u32[]{:S(2)}) %collective-permute-start.2) | collective-permute-done | bytes 262176 | tf_op jit(solution)/shard_map/ppermute | solution.py:273
  93.4 5.0 %shard_map.158 = (f32[256,128]{1,0:T(8,128)}, bf16[256,128]{1,0:T(8,128)(2,1)}, bf16[136,128]{1,0:T(8,128)(2,1)}) custom-call(s32[5]{0:T(128)} %stack.23.place, bf16[64,2048]{1,0:T(8,128)(2,1)} %bitcast.27, bf16[64,2048]{1,0:T(8,128)(2,1)} %copy-done.4, bf16[64,2048]{1,0:T(8,128)(2,1)} %copy-done.5, bf16[64,2048]{1,0:T(8,128)(2,1)} %collective-permute-done.2.last_one, ...), custom_call_target="tpu_custom_call" | custom-call | tf_op jit(solution)/shard_map/pallas_call | solution.py:326
  98.4 13.2 %all-gather.1 = bf16[544,128]{1,0:T(8,128)(2,1)} all-gather(bf16[136,128]{1,0:T(8,128)(2,1)} %get-tuple-element.17), channel_id=3, replica_groups=mesh['sp_0'=4,'sp_1'=4,'sp_2'=4,'sp_3'=2,'tp'=4] {'sp_2'}, dimensions={0}, use_global_device_ids=true | all-gather | bytes 174080 | tf_op jit(solution)/shard_map/all_gather | solution.py:332
  113.9 11.5 %all_to_all.41.parts.slabs = bf16[4,136,128]{2,1,0:T(8,128)(2,1)} all-to-all(bf16[4,136,128]{2,1,0:T(8,128)(2,1)S(1)} %broadcast_in_dim.17), channel_id=1, replica_groups=mesh['sp_0'=4,'sp_1'=4,'sp_2'=4,'sp_3'=2,'tp'=4] {'sp_1'}, dimensions={0} | all-to-all | bytes 278528 | tf_op jit(solution)/shard_map/all_to_all | solution.py:260
  126.7 5.4 %all-to-all-start.1 = ((bf16[4,512,384]{2,1,0:T(8,128)(2,1)}), bf16[4,512,384]{2,1,0:T(8,128)(2,1)S(1)}, u32[]{:S(2)}, u32[]{:S(2)}) async-start(bf16[4,512,384]{2,1,0:T(8,128)(2,1)} %broadcast_in_dim.15), calls=%async_computation.1 | async-start | bytes 3145728 | tf_op jit(solution)/shard_map/all_to_all | solution.py:260
  133.7 10.1 %all-to-all-done.1 = bf16[4,512,384]{2,1,0:T(8,128)(2,1)S(1)} async-done(((bf16[4,512,384]{2,1,0:T(8,128)(2,1)}), bf16[4,512,384]{2,1,0:T(8,128)(2,1)S(1)}, u32[]{:S(2)}, u32[]{:S(2)}) %all-to-all-start.1) | async-done | bytes 1572896 | tf_op jit(solution)/shard_map/all_to_all | solution.py:260
  145.2 10.1 %all-to-all-start.4 = ((bf16[4,136,128]{2,1,0:T(8,128)(2,1)}), bf16[4,136,128]{2,1,0:T(8,128)(2,1)S(1)}, u32[]{:S(2)}, u32[]{:S(2)}) async-start(bf16[4,136,128]{2,1,0:T(8,128)(2,1)} %broadcast_in_dim.18), calls=%async_computation.4 | async-start | bytes 278528 | tf_op jit(solution)/shard_map/all_to_all | solution.py:260
  157.2 5.4 %collective-permute-start.5 = (bf16[512,256]{1,0:T(8,128)(2,1)S(1)}, bf16[512,256]{1,0:T(8,128)(2,1)S(1)}, u32[]{:S(2)}, u32[]{:S(2)}) collective-permute-start(bf16[512,256]{1,0:T(8,128)(2,1)S(1)} %bitcast.33), channel_id=1, source_target_pairs={{16,0},{24,8},{0,16},{8,24},{17,1},{25,9},{1,17},{9,25},{18,2},{26... | collective-permute-start | bytes 786440 | tf_op jit(solution)/shard_map/ppermute | solution.py:273
  162.6 3.1 %collective-permute-start.6 = (bf16[512,256]{1,0:T(8,128)(2,1)S(1)}, bf16[512,256]{1,0:T(8,128)(2,1)S(1)}, u32[]{:S(2)}, u32[]{:S(2)}) collective-permute-start(bf16[512,256]{1,0:T(8,128)(2,1)S(1)} %bitcast.34), channel_id=1, source_target_pairs={{24,0},{0,8},{8,16},{16,24},{25,1},{1,9},{9,17},{17,25},{26,2},{2,... | collective-permute-start | bytes 786440 | tf_op jit(solution)/shard_map/ppermute | solution.py:273
  165.7 3.6 %shard_map.155 = (bf16[256,256]{1,0:T(8,128)(2,1)}, bf16[256,128]{1,0:T(8,128)(2,1)}, bf16[32,256]{1,0:T(8,128)(2,1)}) custom-call(s32[5]{0:T(128)} %stack.23.place, bf16[64,2048]{1,0:T(8,128)(2,1)} %bitcast.28, bf16[64,2048]{1,0:T(8,128)(2,1)} %copy-done.4, bf16[64,2048]{1,0:T(8,128)(2,1)} %copy-done.5, bf16[64,2048]{1,0:T(8,128)(2,1)} %collective-permute-done.2.last_one, ...), custom_call_target="tpu_custom_call" | custom-call | tf_op jit(solution)/shard_map/pallas_call | solution.py:342
  171.3 3.9 %collective-permute-done.3.halo = bf16[32,256]{1,0:T(8,128)(2,1)S(1)} collective-permute-done((bf16[32,256]{1,0:T(8,128)(2,1)}, bf16[32,256]{1,0:T(8,128)(2,1)S(1)}, u32[]{:S(2)}, u32[]{:S(2)}) %collective-permute-start.3) | collective-permute-done | bytes 16416 | tf_op jit(solution)/shard_map/ppermute | solution.py:349
  177.9 23.6 %all-gather = f32[64,256]{1,0:T(8,128)} all-gather(f32[8,256]{1,0:T(8,128)} %get-tuple-element.16), channel_id=2, replica_groups=mesh['sp_0'=4,'sp_1'=4,'sp_2'=4,'sp_3'=2,'tp'=4] {'sp_3','tp'}, dimensions={0}, use_global_device_ids=true | all-gather | bytes 73728 | tf_op jit(solution)/shard_map/all_gather | solution.py:356
  207.8 2.7 %shard_map.162 = bf16[2,128,2048]{2,1,0:T(8,128)(2,1)} custom-call(s32[5]{0:T(128)} %stack.23.place, bf16[256,128]{1,0:T(8,128)(2,1)} %shard_map.157.conv_out, bf16[256,128]{1,0:T(8,128)(2,1)} %shard_map.161.rec_out, bf16[512,256]{1,0:T(8,128)(2,1)} %bitcast.35, bf16[512,256]{1,0:T(8,128)(2,1)} %copy-done.7, bf16[512,256]{1,0:T(8,128)(2,1)} %copy-done.8, ...), custom_call_target="tpu_custom_call" | custom-call | tf_op jit(solution)/shard_map/pallas_call | solution.py:368
  210.6 5.7 %all_to_all.42 = bf16[2,128,2048]{2,1,0:T(8,128)(2,1)S(1)} all-to-all(bf16[2,128,2048]{2,1,0:T(8,128)(2,1)} %shard_map.162), channel_id=1, replica_groups=mesh['sp_0'=4,'sp_1'=4,'sp_2'=4,'sp_3'=2,'tp'=4] {'sp_3'}, dimensions={0} | all-to-all | bytes 2097152 | tf_op jit(solution)/shard_map/all_to_all | solution.py:260
  216.6 13.2 %all_to_all.43.parts = bf16[4,32,2048]{2,1,0:T(8,128)(2,1)} all-to-all(bf16[4,32,2048]{2,1,0:T(8,128)(2,1)S(1)} %bitcast.29), channel_id=1, replica_groups=mesh['sp_0'=4,'sp_1'=4,'sp_2'=4,'sp_3'=2,'tp'=4] {'tp'}, dimensions={0} | all-to-all | bytes 1048576 | tf_op jit(solution)/shard_map/all_to_all | solution.py:260
  (55 shorter events, 30.2 us)
Async XLA Ops:
  51.3 17.1 %all-to-all-start.2 = ((bf16[4,512,384]{2,1,0:T(8,128)(2,1)}), bf16[4,512,384]{2,1,0:T(8,128)(2,1)S(1)}, u32[]{:S(2)}, u32[]{:S(2)}) async-start(bf16[4,512,384]{2,1,0:T(8,128)(2,1)} %broadcast_in_dim.16), calls=%async_computation.2 | async-start | bytes 3145728 | tf_op jit(solution)/shard_map/all_to_all | solution.py:260
  68.4 25.0 %copy-start = (bf16[4,512,384]{2,1,0:T(8,128)(2,1)}, bf16[4,512,384]{2,1,0:T(8,128)(2,1)S(1)}, u32[]{:S(2)}) copy-start(bf16[4,512,384]{2,1,0:T(8,128)(2,1)S(1)} %all-to-all-done.2) | copy-start | bytes 4718596
  69.2 43.9 %all-to-all-start.5 = ((bf16[16,32,256]{2,1,0:T(8,128)(2,1)}), bf16[16,32,256]{2,1,0:T(8,128)(2,1)S(1)}, u32[]{:S(2)}, u32[]{:S(2)}) async-start(bf16[16,32,256]{2,1,0:T(8,128)(2,1)} %broadcast_in_dim.19), calls=%async_computation.5 | async-start | bytes 524288 | tf_op jit(solution)/shard_map/all_to_all | solution.py:260
  75.7 17.6 %copy-start.2 = (bf16[2,32,2048]{2,1,0:T(8,128)(2,1)}, bf16[2,32,2048]{2,1,0:T(8,128)(2,1)S(1)}, u32[]{:S(2)}) copy-start(bf16[2,32,2048]{2,1,0:T(8,128)(2,1)S(1)} %slice.43) | copy-start | bytes 786436
  75.7 11.6 %collective-permute-start = (bf16[64,2048]{1,0:T(8,128)(2,1)S(1)}, bf16[64,2048]{1,0:T(8,128)(2,1)S(1)}, u32[]{:S(2)}, u32[]{:S(2)}) collective-permute-start(bf16[64,2048]{1,0:T(8,128)(2,1)S(1)} %bitcast.24), channel_id=1, source_target_pairs={{1,0},{2,1},{3,2},{0,3},{5,4},{6,5},{7,6},{4,7},{9,8},{10,9},{11,1... | collective-permute-start | bytes 786440 | tf_op jit(solution)/shard_map/ppermute | solution.py:273
  80.7 9.8 %collective-permute-start.1 = (bf16[64,2048]{1,0:T(8,128)(2,1)S(1)}, bf16[64,2048]{1,0:T(8,128)(2,1)S(1)}, u32[]{:S(2)}, u32[]{:S(2)}) collective-permute-start(bf16[64,2048]{1,0:T(8,128)(2,1)S(1)} %bitcast.25), channel_id=1, source_target_pairs={{2,0},{3,1},{0,2},{1,3},{6,4},{7,5},{4,6},{5,7},{10,8},{11,9},{8,1... | collective-permute-start | bytes 786440 | tf_op jit(solution)/shard_map/ppermute | solution.py:273
  83.2 10.1 %collective-permute-start.2 = (bf16[64,2048]{1,0:T(8,128)(2,1)S(1)}, bf16[64,2048]{1,0:T(8,128)(2,1)}, u32[]{:S(2)}, u32[]{:S(2)}) collective-permute-start(bf16[64,2048]{1,0:T(8,128)(2,1)S(1)} %bitcast.26), channel_id=1, source_target_pairs={{3,0},{0,1},{1,2},{2,3},{7,4},{4,5},{5,6},{6,7},{11,8},{8,9},{9,10... | collective-permute-start | bytes 786440 | tf_op jit(solution)/shard_map/ppermute | solution.py:273
  87.3 6.0 %copy-start.4 = (bf16[64,2048]{1,0:T(8,128)(2,1)}, bf16[64,2048]{1,0:T(8,128)(2,1)S(1)}, u32[]{:S(2)}) copy-start(bf16[64,2048]{1,0:T(8,128)(2,1)S(1)} %collective-permute-done.next_one) | copy-start | bytes 786436
  90.5 2.9 %copy-start.5 = (bf16[64,2048]{1,0:T(8,128)(2,1)}, bf16[64,2048]{1,0:T(8,128)(2,1)S(1)}, u32[]{:S(2)}) copy-start(bf16[64,2048]{1,0:T(8,128)(2,1)S(1)} %collective-permute-done.1.across) | copy-start | bytes 786436
  113.1 49.5 %copy-start.3 = (bf16[16,32,256]{2,1,0:T(8,128)(2,1)}, bf16[16,32,256]{2,1,0:T(8,128)(2,1)S(1)}, u32[]{:S(2)}) copy-start(bf16[16,32,256]{2,1,0:T(8,128)(2,1)S(1)} %all-to-all-done.5) | copy-start | bytes 786436
  126.7 17.0 %all-to-all-start.1 = ((bf16[4,512,384]{2,1,0:T(8,128)(2,1)}), bf16[4,512,384]{2,1,0:T(8,128)(2,1)S(1)}, u32[]{:S(2)}, u32[]{:S(2)}) async-start(bf16[4,512,384]{2,1,0:T(8,128)(2,1)} %broadcast_in_dim.15), calls=%async_computation.1 | async-start | bytes 3145728 | tf_op jit(solution)/shard_map/all_to_all | solution.py:260
  143.8 22.0 %copy-start.1 = (bf16[4,512,384]{2,1,0:T(8,128)(2,1)}, bf16[4,512,384]{2,1,0:T(8,128)(2,1)S(1)}, u32[]{:S(2)}) copy-start(bf16[4,512,384]{2,1,0:T(8,128)(2,1)S(1)} %all-to-all-done.1) | copy-start | bytes 4718596
  145.2 58.4 %all-to-all-start.4 = ((bf16[4,136,128]{2,1,0:T(8,128)(2,1)}), bf16[4,136,128]{2,1,0:T(8,128)(2,1)S(1)}, u32[]{:S(2)}, u32[]{:S(2)}) async-start(bf16[4,136,128]{2,1,0:T(8,128)(2,1)} %broadcast_in_dim.18), calls=%async_computation.4 | async-start | bytes 278528 | tf_op jit(solution)/shard_map/all_to_all | solution.py:260
  155.3 51.1 %collective-permute-start.4 = (bf16[512,256]{1,0:T(8,128)(2,1)S(1)}, bf16[512,256]{1,0:T(8,128)(2,1)S(1)}, u32[]{:S(2)}, u32[]{:S(2)}) collective-permute-start(bf16[512,256]{1,0:T(8,128)(2,1)S(1)} %bitcast.32), channel_id=1, source_target_pairs={{8,0},{16,8},{24,16},{0,24},{9,1},{17,9},{25,17},{1,25},{10,2},{18... | collective-permute-start | bytes 786440 | tf_op jit(solution)/shard_map/ppermute | solution.py:273
  157.2 49.2 %collective-permute-start.5 = (bf16[512,256]{1,0:T(8,128)(2,1)S(1)}, bf16[512,256]{1,0:T(8,128)(2,1)S(1)}, u32[]{:S(2)}, u32[]{:S(2)}) collective-permute-start(bf16[512,256]{1,0:T(8,128)(2,1)S(1)} %bitcast.33), channel_id=1, source_target_pairs={{16,0},{24,8},{0,16},{8,24},{17,1},{25,9},{1,17},{9,25},{18,2},{26... | collective-permute-start | bytes 786440 | tf_op jit(solution)/shard_map/ppermute | solution.py:273
  162.6 43.7 %collective-permute-start.6 = (bf16[512,256]{1,0:T(8,128)(2,1)S(1)}, bf16[512,256]{1,0:T(8,128)(2,1)S(1)}, u32[]{:S(2)}, u32[]{:S(2)}) collective-permute-start(bf16[512,256]{1,0:T(8,128)(2,1)S(1)} %bitcast.34), channel_id=1, source_target_pairs={{24,0},{0,8},{8,16},{16,24},{25,1},{1,9},{9,17},{17,25},{26,2},{2,... | collective-permute-start | bytes 786440 | tf_op jit(solution)/shard_map/ppermute | solution.py:273
  169.3 5.8 %collective-permute-start.3 = (bf16[32,256]{1,0:T(8,128)(2,1)}, bf16[32,256]{1,0:T(8,128)(2,1)S(1)}, u32[]{:S(2)}, u32[]{:S(2)}) collective-permute-start(bf16[32,256]{1,0:T(8,128)(2,1)} %get-tuple-element.14), channel_id=1, source_target_pairs={{0,8},{8,16},{16,24},{24,32},{32,40},{40,48},{48,56},{56,64},{64,7... | collective-permute-start | bytes 49160 | tf_op jit(solution)/shard_map/ppermute | solution.py:349
  175.1 0.6 copy-start.10
  203.5 0.7 copy-start.6
  206.3 0.7 copy-start.7
  206.3 0.8 copy-start.8
  207.1 0.7 copy-start.9

commit v3 on v2

v3 whole, which is shorter than its diff:
```python
import jax
import jax.numpy as jnp
from jax import lax
from jax.experimental import pallas as pl
from jax.experimental.pallas import tpu as pltpu
from jax.sharding import Mesh
from jax.sharding import PartitionSpec as P


ZH, ZL, X, C, Y = "sp_0", "sp_1", "sp_2", "sp_3", "tp"
SP = (ZH, ZL, X, C)
SP_TP = (ZH, ZL, X, C, Y)
NZ, NQ, NX, NC, NY = 16, 4, 4, 2, 4
CONV_CH = 1024
CH = 128
ROWS = 256
OWN = 32
BLOCK = 64
TAPS = 31
HALO = 32
STATE_ROWS = 136
HALF = 128
COLS = 384
CHUNK = 16
norm_eps = 1e-06
layer_eps = 1e-05
HIGH = lax.Precision.HIGHEST
bf16 = jnp.bfloat16
f32 = jnp.float32

VMEM = pl.BlockSpec(memory_space=pltpu.VMEM)
SMEM = pl.BlockSpec(memory_space=pltpu.SMEM)


def kernel_call(body, out, specs, scratch=()):
    return pl.pallas_call(
        body,
        out_shape=out,
        in_specs=specs,
        out_specs=jax.tree.map(lambda _: VMEM, out),
        scratch_shapes=scratch,
    )


def shape(dims, dtype):
    return jax.ShapeDtypeStruct(dims, dtype)


def matmul(a, b, dims, precision=None):
    return lax.dot_general(
        a, b, (dims, ((), ())), precision=precision, preferred_element_type=f32
    )


def sigmoid(v):
    return 1.0 / (1.0 + jnp.exp(-v))


def silu(v):
    return v * sigmoid(v)


def own_half(value, core):
    return jnp.where(core == 0, value[:, :CH], value[:, CH:])


def pack_body(query, forget, value, left, gate, outgate, conv_out, rec_out, out, rows):
    blocks = (query, forget, value, left, gate, outgate)
    for x in range(NX):
        mine = [3 * x + k for k in range(3)]
        for at, b in enumerate(sorted(mine, key=lambda b: ((b + x) % 2, b))):
            half = b % NC
            out[x, :, at * CH : (at + 1) * CH] = blocks[b // NC][:, half * CH : (half + 1) * CH]
    for c in range(NC):
        for k, block in enumerate((conv_out, rec_out)):
            at = (2 * c + k) * CH
            rows[:, at : at + CH] = block[:, c * CH : (c + 1) * CH]


def norm_body(tokens, gain, out):
    features = tokens[...].astype(f32)
    out[...] = (
        features
        * lax.rsqrt(jnp.mean(features * features, axis=1, keepdims=True) + norm_eps)
        * gain[...]
    ).astype(bf16)


def project_body(place, tokens, own, other, jump, out, weight):
    c = place[3]
    blocks = NZ * NX
    for core, piece in ((c, own), (1 - c, other)):

        def copy(k, carry, core=core, piece=piece):
            to = pl.multiple_of((NC * k + core) * CHUNK, CHUNK)
            weight[pl.ds(to, CHUNK)] = piece[pl.ds(pl.multiple_of(k * CHUNK, CHUNK), CHUNK)]
            return carry

        lax.fori_loop(0, blocks, copy, 0, unroll=8)
    even = lax.rem(place[2], 2)
    for x in range(NX):
        result = matmul(tokens[x * HALF : (x + 1) * HALF], weight[...], ((1,), (0,))).astype(bf16)
        first = NC * x + even
        second = NC * x + 1 - even
        out[first, :HALF] = result[:, : 2 * CH]
        out[second, :HALF, :CH] = result[:, 2 * CH :]
        out[second, :HALF, CH:] = jnp.zeros((HALF, CH), bf16)
        for k in range(NC):
            row = jnp.broadcast_to(jump[k : k + 1], (8, CH))
            high = row.astype(bf16)
            out[NC * x + k, HALF:, :CH] = high
            out[NC * x + k, HALF:, CH:] = (row - high.astype(f32)).astype(bf16)


PLACES = (
    ((0, 0), (0, 0)),
    ((0, 1), (1, 0)),
    ((1, 0), (1, 1)),
    ((2, 0), (2, 0)),
    ((2, 1), (3, 0)),
    ((3, 0), (3, 1)),
)


def block_of(spread, m, c):
    options = []
    for x, at in PLACES[m]:
        options.append(
            jnp.concatenate(
                [spread[NC * x + k, :HALF, at * CH : (at + 1) * CH] for k in range(NC)], axis=0
            )
        )
    if PLACES[m][0] == PLACES[m][1]:
        return options[0]
    return jnp.where(c == 0, options[0].astype(f32), options[1].astype(f32)).astype(bf16)


def local_body(place, spread, margin, inner, decayed, packed, tail):
    c = place[3]
    rows = []
    for k in range(NC):
        row = spread[NC * place[2] + k, HALF : HALF + 8].astype(f32)[:1]
        rows.append(row[:, :CH] + row[:, CH:])
    jump = jnp.concatenate(rows, axis=1)
    bound = own_half(margin[...], c)
    queries = silu(block_of(spread, 0, c).astype(f32))
    keys = bound * sigmoid(-block_of(spread, 1, c).astype(f32))
    inputs = block_of(spread, 2, c)
    for k in range(2):
        tail[:, k * CH : (k + 1) * CH] = block_of(spread, 3 + k, c)[ROWS - HALO :]
    log_forget = jnp.log1p(-keys)
    row = lax.broadcasted_iota(jnp.int32, (BLOCK, BLOCK), 0)
    col = lax.broadcasted_iota(jnp.int32, (BLOCK, BLOCK), 1)
    causal = row >= col
    lower = jnp.where(causal, 1.0, 0.0)
    state = jnp.zeros((CH, CH), f32)
    before = jnp.zeros((1, CH), f32)
    for n in range(ROWS // BLOCK):
        at = slice(n * BLOCK, (n + 1) * BLOCK)
        jumps = jump[:, n * BLOCK : (n + 1) * BLOCK]
        jumped = jnp.sum(jnp.where(causal, jumps, 0.0), axis=1, keepdims=True)
        running = matmul(lower, log_forget[at], ((1,), (0,)), HIGH) + jumped
        final = running[BLOCK - 1 : BLOCK]
        scaled = queries[at] * jnp.exp(running)
        scaled_keys = (keys[at] * jnp.exp(-running)).astype(bf16)
        final_keys = (keys[at] * jnp.exp(final - running)).astype(bf16)
        scores = matmul(scaled.astype(bf16), scaled_keys, ((1,), (1,)))
        scores = jnp.where(causal, scores, 0.0).astype(bf16)
        inner[at] = matmul(scores, inputs[at], ((1,), (0,))) + matmul(
            scaled.astype(bf16), state.astype(bf16), ((1,), (1,))
        )
        decayed[at] = (scaled * jnp.exp(before)).astype(bf16)
        state = state * jnp.exp(final) + matmul(inputs[at], final_keys, ((0,), (0,)))
        before = before + final
    pack(packed, state, before)


def pack(ref, state, decay):
    high = decay.astype(bf16).astype(f32)
    low = decay - high
    first = lax.broadcasted_iota(jnp.int32, (8, CH), 0)
    ref[:CH] = state.astype(bf16)
    ref[CH:] = jnp.where(first == 0, high, jnp.where(first == 1, low, 0.0)).astype(bf16)


def unpacked(block):
    wide = block.astype(f32)
    return wide[CH : CH + 1] + wide[CH + 1 : CH + 2], wide[:CH]


def total_body(parts, total):
    state = jnp.zeros((CH, CH), f32)
    decay = jnp.zeros((1, CH), f32)
    for k in range(NQ):
        step, add = unpacked(parts[k])
        state = state * jnp.exp(step) + add
        decay = decay + step
    for k in range(total.shape[0]):
        pack(total.at[k], state, decay)


def finish_body(place, quads, slabs, chips, inner, decayed, gain, spread, out):
    state = jnp.zeros((CH, CH), f32)
    for level, parts in enumerate((quads, slabs, chips)):
        for k in range(NQ):
            step, add = unpacked(parts[k])
            state = jnp.where(k < place[level], state * jnp.exp(step) + add, state)
    recurrent = inner[...] + matmul(decayed[...], state.astype(bf16), ((1,), (1,)))
    scale = lax.rsqrt(jnp.mean(recurrent * recurrent, axis=1, keepdims=True) + norm_eps)
    gate = silu(block_of(spread, 5, place[3]).astype(f32))
    out[...] = (recurrent * scale * own_half(gain[...], place[3]) * gate).astype(bf16)


def conv_body(place, spread, halo, taps, out, sums, gated):
    rim = halo[...].astype(f32)
    gated[:HALO] = rim[:, :CH] * sigmoid(rim[:, CH:])
    c = place[3]
    gated[HALO:] = block_of(spread, 3, c).astype(f32) * sigmoid(block_of(spread, 4, c).astype(f32))
    own_taps = own_half(taps[...], place[3])
    for n in range(ROWS // BLOCK):
        total = jnp.zeros((BLOCK, CH), f32)
        for j in range(TAPS):
            at = n * BLOCK + HALO - TAPS + 1 + j
            total = total + gated[at : at + BLOCK] * own_taps[j : j + 1]
        out[n * BLOCK : (n + 1) * BLOCK] = total.astype(bf16)
    values = out[...].astype(f32)
    ones = jnp.ones((8, CH), f32)
    first_sum = matmul(ones, values, ((1,), (1,)), HIGH)
    second_sum = matmul(ones, values * values, ((1,), (1,)), HIGH)
    row = lax.broadcasted_iota(jnp.int32, (8, ROWS), 0)
    both_sums = jnp.where(row == 0, first_sum, second_sum)
    for k in range(NC * NY):
        sums[k] = both_sums


def channel_body(place, values, sums, gain, bias, out):
    total = sums[0]
    for k in range(1, NC * NY):
        total = total + sums[k]
    row = lax.broadcasted_iota(jnp.int32, (8, CH), 0)
    pick_first = jnp.where(row == 0, 1.0 / CONV_CH, 0.0)
    pick_second = jnp.where(row == 1, 1.0 / CONV_CH, 0.0)
    mean = matmul(total, pick_first, ((0,), (0,)), HIGH)
    variance = matmul(total, pick_second, ((0,), (0,)), HIGH) - mean * mean
    shifted = (values[...].astype(f32) - mean) * lax.rsqrt(variance + layer_eps)
    out[...] = silu(
        shifted * own_half(gain[...], place[3]) + own_half(bias[...], place[3])
    ).astype(bf16)


def output_body(conv_out, rec_out, pieces, out, weight):
    for k in range(NX * NC):
        for z in range(NZ):
            to = (z * NX * NC + k) * CHUNK
            weight[to : to + CHUNK] = pieces[k, z * CHUNK : (z + 1) * CHUNK]
    both = jnp.concatenate([conv_out[...], rec_out[...]], axis=1)
    result = matmul(both, weight[...], ((1,), (1,))).astype(bf16)
    for c in range(NC):
        out[c] = result[c * HALF : (c + 1) * HALF]


def last_body(parts, out):
    total = parts[0].astype(f32)
    for y in range(1, NY):
        total = total + parts[y].astype(f32)
    out[...] = total.astype(bf16)


def exchanged(x, axes):
    return lax.all_to_all(x, axes, split_axis=0, concat_axis=0, tiled=True)


def to_everyone(x, axes):
    copies = jnp.broadcast_to(x, (lax.axis_size(axes), *x.shape))
    return exchanged(copies, axes)


def per_device(
    tokens,
    input_norm_gain,
    convolution_value_weight,
    convolution_gate_weight,
    depthwise_filter_taps,
    channel_norm_gain,
    channel_norm_bias,
    query_projection_weight,
    forget_gate_weight,
    recurrence_value_weight,
    output_gate_weight,
    forget_floor_margin,
    decay_jump_terms,
    head_norm_gain,
    convolution_output_weight,
    recurrence_output_weight,
):
    place = jnp.stack([lax.axis_index(a) for a in SP_TP]).astype(jnp.int32)
    width = tokens.shape[1]

    columns, out_rows = kernel_call(
        pack_body, (shape((NX, CHUNK, COLS), bf16), shape((CHUNK, 4 * CH), bf16)), [VMEM] * 8
    )(
        query_projection_weight,
        forget_gate_weight,
        recurrence_value_weight,
        convolution_value_weight,
        convolution_gate_weight,
        output_gate_weight,
        convolution_output_weight.T,
        recurrence_output_weight.T,
    )
    shard = exchanged(columns, X).reshape(NX * CHUNK, COLS)
    normed = kernel_call(norm_body, shape((OWN, width), bf16), [VMEM, VMEM])(
        tokens, input_norm_gain.reshape(1, width)
    )
    rows = to_everyone(normed, (X, Y)).reshape(NX * HALF, width)
    own = lax.all_gather(shard, (ZH, ZL), axis=0, tiled=True)
    other = lax.ppermute(own, C, [(0, 1), (1, 0)])
    spread = kernel_call(
        project_body,
        shape((NX * NC, HALF + 8, 2 * CH), bf16),
        [SMEM] + [VMEM] * 4,
        [pltpu.VMEM((width, COLS), bf16)],
    )(place, rows, own, other, decay_jump_terms)
    spread = exchanged(spread, (X, C))
    out_along = to_everyone(out_rows, (ZH, ZL))
    halves = out_along.reshape(NZ * CHUNK, NC, 2 * CH).transpose(1, 0, 2)
    halves = jnp.broadcast_to(halves, (NX, *halves.shape)).reshape(-1, *halves.shape[1:])
    out_pieces = exchanged(halves, (X, C))

    margin = forget_floor_margin.reshape(1, 2 * CH)
    inner, decayed, packed, tail = kernel_call(
        local_body,
        (
            shape((ROWS, CH), f32),
            shape((ROWS, CH), bf16),
            shape((STATE_ROWS, CH), bf16),
            shape((HALO, 2 * CH), bf16),
        ),
        [SMEM] + [VMEM] * 2,
    )(place, spread, margin)
    chips = lax.all_gather(packed, X, axis=0)

    def total_of(parts, copies):
        return kernel_call(total_body, shape((copies, STATE_ROWS, CH), bf16), [VMEM])(parts)

    slab_copies = total_of(chips, NQ)
    slabs = exchanged(slab_copies, ZL)
    quad = total_of(slabs, 1)[0]
    quads = lax.all_gather(quad, ZH, axis=0)

    blocks = NZ * NX
    halo = lax.ppermute(tail, (ZH, ZL, X), [(k, k + 1) for k in range(blocks - 1)])
    convolved, sums = kernel_call(
        conv_body,
        (shape((ROWS, CH), bf16), shape((NC * NY, 8, ROWS), f32)),
        [SMEM, VMEM, VMEM, VMEM],
        [pltpu.VMEM((HALO + ROWS, CH), f32)],
    )(place, spread, halo, depthwise_filter_taps)
    all_sums = exchanged(sums, (C, Y))
    conv_out = kernel_call(channel_body, shape((ROWS, CH), bf16), [SMEM, VMEM, VMEM, VMEM, VMEM])(
        place,
        convolved,
        all_sums,
        channel_norm_gain.reshape(1, 2 * CH),
        channel_norm_bias.reshape(1, 2 * CH),
    )
    rec_out = kernel_call(
        finish_body, shape((ROWS, CH), bf16), [SMEM] + [VMEM] * 7
    )(place, quads, slabs, chips, inner, decayed, head_norm_gain.reshape(1, 2 * CH), spread)

    partial = kernel_call(
        output_body, shape((NC, ROWS // NC, width), bf16), [VMEM] * 3,
        [pltpu.VMEM((width, 2 * CH), bf16)],
    )(conv_out, rec_out, out_pieces)
    pair_sum = exchanged(partial, C).astype(f32).sum(axis=0).astype(bf16)
    pieces = exchanged(pair_sum.reshape(NY, OWN, width), Y)
    return kernel_call(last_body, shape((OWN, width), bf16), [VMEM])(pieces)


def solution(mesh):
    split = Mesh(mesh.devices.reshape(NQ, NZ // NQ, NX, NC, mesh.shape["tp"]), SP_TP)
    return jax.shard_map(
        per_device,
        mesh=split,
        in_specs=(
            P(SP_TP, None),
            P(),
            P(SP, "tp"),
            P(SP, "tp"),
            P(None, "tp"),
            P("tp"),
            P("tp"),
            P(SP, "tp"),
            P(SP, "tp"),
            P(SP, "tp"),
            P(SP, "tp"),
            P("tp"),
            P("tp", SP),
            P("tp"),
            P("tp", SP),
            P("tp", SP),
        ),
        out_specs=P(SP_TP, None),
        check_vma=False,
    )
```

time: 235 us -> 199 us (0.85); the launches traced: 232 us -> 198 us
  waiting for transfers between devices: 32.3 us -> 17 us
  blocking collectives: 112 us -> 105 us
  starting transfers between devices: 49.5 us -> 42.8 us
  local copies, waits for them, and re-layouts: 12 us -> 7.95 us
    ppermute x6 -> x1, starting transfers between devices: 20.8 us -> 1.91 us  [per_device(): other = lax.ppermute(own, C, [(0, 1), (1, 0)])]
    all_to_all x4 -> x6, starting transfers between devices: 26.7 us -> 35.6 us  [exchanged(): return lax.all_to_all(x, axes, split_axis=0, concat_axis=0, tiled=True)]
    all_to_all x4 -> x6, waiting for transfers between devices: 22.4 us -> 13.6 us  [exchanged(): return lax.all_to_all(x, axes, split_axis=0, concat_axis=0, tiled=True)]
    all_gather x2, blocking collectives: 63.4 us -> 58.1 us  [the longest x1 37.2 us: per_device(): own = lax.all_gather(shard, (ZH, ZL), axis=0, tiled=True)]
    ppermute x6 -> x1, waiting for transfers between devices: 6.04 us -> 1.71 us  [per_device(): other = lax.ppermute(own, C, [(0, 1), (1, 0)])]
    ppermute x1, starting transfers between devices: 1.95 us -> 5.33 us  [per_device(): lax.ppermute(tail, (ZH, ZL, X), [(k, k + 1) for k in range(blocks - 1)])]
    unnamed x25 -> x14, local copies, waits for them, and re-layouts: 5.58 us -> 2.93 us
    broadcast_in_dim x5 -> x2, local copies, waits for them, and re-layouts: 5.65 us -> 3.21 us  [to_everyone(): copies = jnp.broadcast_to(x, (lax.axis_size(axes), *x.shape))]
  transfers between devices with their start and end apart: 11 -> 8, of which waited for: 5 -> 5; matrix products, arithmetic and copies ran while one was open for 1% -> 0% of each run, Pallas kernels for 8% -> 7%
where the time goes in v3:
time: 199 us; the launch traced here: 198 us
  blocking collectives  105 us (53%)
  starting transfers between devices  42.8 us (22%)
  Pallas kernels  25.1 us (13%)
  waiting for transfers between devices  17 us (9%)
  local copies, waits for them, and re-layouts  7.95 us (4%)
    all_gather x1, blocking collectives, per_device(): own = lax.all_gather(shard, (ZH, ZL), axis=0, tiled=True)  37.2 us
    all_to_all x6, starting transfers between devices, exchanged(): return lax.all_to_all(x, axes, split_axis=0, concat_axis=0, tiled=True)  35.6 us
    all_to_all x3, blocking collectives, exchanged(): return lax.all_to_all(x, axes, split_axis=0, concat_axis=0, tiled=True)  33.7 us
    all_gather x1, blocking collectives, per_device(): quads = lax.all_gather(quad, ZH, axis=0)  20.9 us
    all_to_all x6, waiting for transfers between devices, exchanged(): return lax.all_to_all(x, axes, split_axis=0, concat_axis=0, tiled=True)  13.6 us
    all_gather x1, blocking collectives, per_device(): chips = lax.all_gather(packed, X, axis=0)  12.9 us
    ppermute x1, starting transfers between devices, per_device(): lax.ppermute(tail, (ZH, ZL, X), [(k, k + 1) for k in range(blocks - 1)])  5.33 us
    pallas_call x1, Pallas kernels, per_device(): kernel_call(project_body, shape((NX * NC, HALF + 8, 2 * CH), bf16), [SMEM...  4.53 us
  transfers between devices with their start and end apart: 8, of which 5 were waited for; matrix products, arithmetic and copies ran while one was open for 0% of the time, Pallas kernels for 7%

profile of v3, /device:TPU:6, one launch (start us, length us, event | category | flops | bytes accessed | tf_op | source)
XLA Modules:
  0.0 198.0 jit_solution(16446129683284718023)
XLA Ops:
  1.4 9.1 %all-to-all-start.1 = ((bf16[4,16,384]{2,1,0:T(8,128)(2,1)}), bf16[4,16,384]{2,1,0:T(8,128)(2,1)S(1)}, u32[]{:S(2)}, u32[]{:S(2)}) async-start(bf16[4,16,384]{2,1,0:T(8,128)(2,1)} %get-tuple-element.13), calls=%async_computation.1 | async-start | bytes 98304 | tf_op jit(solution)/shard_map/all_to_all | solution.py:270
  12.2 1.8 all-to-all-done.1
  14.0 2.5 %broadcast_in_dim.9 = bf16[16,32,2048]{2,1,0:T(8,128)(2,1)} broadcast(bf16[32,2048]{1,0:T(8,128)(2,1)} %shard_map.154), dimensions={1,2} | broadcast | bytes 2228224 | tf_op jit(solution)/shard_map/broadcast_in_dim | solution.py:274
  16.5 5.7 %all-to-all-start = ((bf16[16,32,2048]{2,1,0:T(8,128)(2,1)}), bf16[16,32,2048]{2,1,0:T(8,128)(2,1)S(1)}, u32[]{:S(2)}, u32[]{:S(2)}) async-start(bf16[16,32,2048]{2,1,0:T(8,128)(2,1)} %broadcast_in_dim.9), calls=%async_computation | async-start | bytes 4194304 | tf_op jit(solution)/shard_map/all_to_all | solution.py:270
  22.1 37.2 %all_gather.12.own = bf16[1024,384]{1,0:T(8,128)(2,1)S(1)} all-gather(bf16[64,384]{1,0:T(8,128)(2,1)S(1)} %bitcast.23), channel_id=1, replica_groups=mesh['sp_0'=4,'sp_1'=4,'sp_2'=4,'sp_3'=2,'tp'=4] {'sp_0','sp_1'}, dimensions={0}, use_global_device_ids=true | all-gather | bytes 835584 | tf_op jit(solution)/shard_map/all_gather | solution.py:316
  59.3 1.9 collective-permute-start
  64.9 4.5 %shard_map.156 = bf16[8,136,256]{2,1,0:T(8,128)(2,1)} custom-call(s32[5]{0:T(128)} %stack.23.place, bf16[512,2048]{1,0:T(8,128)(2,1)} %bitcast.18, bf16[1024,384]{1,0:T(8,128)(2,1)} %copy-done.2, bf16[1024,384]{1,0:T(8,128)(2,1)} %collective-permute-done.other, f32[2,128]{1,0:T(2,128)} %jump.1), custom_call_target="tpu_custom_call" | custom-call | tf_op jit(solution)/shard_map/pallas_call | solution.py:318
  69.5 13.5 %all_to_all.45.spread = bf16[8,136,256]{2,1,0:T(8,128)(2,1)} all-to-all(bf16[8,136,256]{2,1,0:T(8,128)(2,1)} %shard_map.156), channel_id=1, replica_groups=mesh['sp_0'=4,'sp_1'=4,'sp_2'=4,'sp_3'=2,'tp'=4] {'sp_2','sp_3'}, dimensions={0} | all-to-all | bytes 1114112 | tf_op jit(solution)/shard_map/all_to_all | solution.py:270
  83.7 7.3 %all-to-all-start.5 = ((bf16[16,16,512]{2,1,0:T(8,128)(2,1)}), bf16[16,16,512]{2,1,0:T(8,128)(2,1)S(1)}, u32[]{:S(2)}, u32[]{:S(2)}) async-start(bf16[16,16,512]{2,1,0:T(8,128)(2,1)} %broadcast_in_dim.10), calls=%async_computation.5 | async-start | bytes 524288 | tf_op jit(solution)/shard_map/all_to_all | solution.py:270
  91.0 3.0 %shard_map.157 = (f32[256,128]{1,0:T(8,128)}, bf16[256,128]{1,0:T(8,128)(2,1)}, bf16[136,128]{1,0:T(8,128)(2,1)}, bf16[32,256]{1,0:T(8,128)(2,1)}) custom-call(s32[5]{0:T(128)} %stack.23.place, bf16[8,136,256]{2,1,0:T(8,128)(2,1)} %all_to_all.45.spread, f32[1,256]{1,0:T(1,128)} %bitcast.27), custom_call_target="tpu_custom_call" | custom-call | tf_op jit(solution)/shard_map/pallas_call | solution.py:331
  94.0 5.3 %collective-permute-start.1 = (bf16[32,256]{1,0:T(8,128)(2,1)}, bf16[32,256]{1,0:T(8,128)(2,1)S(1)}, u32[]{:S(2)}, u32[]{:S(2)}) collective-permute-start(bf16[32,256]{1,0:T(8,128)(2,1)} %get-tuple-element.14), channel_id=1, source_target_pairs={{0,8},{8,16},{16,24},{24,32},{32,40},{40,48},{48,56},{56,64},{64,7... | collective-permute-start | bytes 49160 | tf_op jit(solution)/shard_map/ppermute | solution.py:352
  101.6 2.4 %shard_map.158 = (bf16[256,128]{1,0:T(8,128)(2,1)}, f32[8,8,256]{2,1,0:T(8,128)}) custom-call(s32[5]{0:T(128)} %stack.23.place, bf16[8,136,256]{2,1,0:T(8,128)(2,1)} %all_to_all.45.spread, bf16[32,256]{1,0:T(8,128)(2,1)} %copy-done.6, f32[31,256]{1,0:T(8,128)} %taps.1), custom_call_target="tpu_custom_call" | custom-call | tf_op jit(solution)/shard_map/pallas_call | solution.py:353
  104.0 6.0 %all-to-all-done.5 = bf16[16,16,512]{2,1,0:T(8,128)(2,1)S(1)} async-done(((bf16[16,16,512]{2,1,0:T(8,128)(2,1)}), bf16[16,16,512]{2,1,0:T(8,128)(2,1)S(1)}, u32[]{:S(2)}, u32[]{:S(2)}) %all-to-all-start.5) | async-done | bytes 262176 | tf_op jit(solution)/shard_map/all_to_all | solution.py:270
  110.0 4.1 %all-to-all-start.3 = ((f32[8,8,256]{2,1,0:T(8,128)}), f32[8,8,256]{2,1,0:T(8,128)S(1)}, u32[]{:S(2)}, u32[]{:S(2)}) async-start(f32[8,8,256]{2,1,0:T(8,128)} %get-tuple-element.16), calls=%async_computation.3 | async-start | bytes 131072 | tf_op jit(solution)/shard_map/all_to_all | solution.py:270
  114.1 12.9 %all-gather = bf16[544,128]{1,0:T(8,128)(2,1)} all-gather(bf16[136,128]{1,0:T(8,128)(2,1)} %get-tuple-element.17), channel_id=2, replica_groups=mesh['sp_0'=4,'sp_1'=4,'sp_2'=4,'sp_3'=2,'tp'=4] {'sp_2'}, dimensions={0}, use_global_device_ids=true | all-gather | bytes 174080 | tf_op jit(solution)/shard_map/all_gather | solution.py:341
  128.7 4.1 %all-to-all-start.4 = ((bf16[4,136,128]{2,1,0:T(8,128)(2,1)}), bf16[4,136,128]{2,1,0:T(8,128)(2,1)S(1)}, u32[]{:S(2)}, u32[]{:S(2)}) async-start(bf16[4,136,128]{2,1,0:T(8,128)(2,1)} %shard_map.160), calls=%async_computation.4 | async-start | bytes 278528 | tf_op jit(solution)/shard_map/all_to_all | solution.py:270
  132.9 5.8 %all-to-all-done.4.parts.slabs = bf16[4,136,128]{2,1,0:T(8,128)(2,1)S(1)} async-done(((bf16[4,136,128]{2,1,0:T(8,128)(2,1)}), bf16[4,136,128]{2,1,0:T(8,128)(2,1)S(1)}, u32[]{:S(2)}, u32[]{:S(2)}) %all-to-all-start.4) | async-done | bytes 139296 | tf_op jit(solution)/shard_map/all_to_all | solution.py:270
  139.8 5.4 %all-to-all-start.6 = ((bf16[8,256,256]{2,1,0:T(8,128)(2,1)}), bf16[8,256,256]{2,1,0:T(8,128)(2,1)S(1)}, u32[]{:S(2)}, u32[]{:S(2)}) async-start(bf16[8,256,256]{2,1,0:T(8,128)(2,1)} %bitcast.16), calls=%async_computation.6 | async-start | bytes 2097152 | tf_op jit(solution)/shard_map/all_to_all | solution.py:270
  145.1 2.0 %shard_map.159.conv_out = bf16[256,128]{1,0:T(8,128)(2,1)} custom-call(s32[5]{0:T(128)} %stack.23.place, bf16[256,128]{1,0:T(8,128)(2,1)} %get-tuple-element.15.values, f32[8,8,256]{2,1,0:T(8,128)} %copy-done.4, f32[1,256]{1,0:T(1,128)} %bitcast.28, f32[1,256]{1,0:T(1,128)} %bitcast.29), custom_call_target="tpu_custom_call" | custom-call | tf_op jit(solution)/shard_map/pallas_call | solution.py:360
  148.7 20.9 %all_gather.15.quads = bf16[4,136,128]{2,1,0:T(8,128)(2,1)} all-gather(bf16[1,136,128]{2,1,0:T(8,128)(2,1)} %shard_map.161), channel_id=1, replica_groups=mesh['sp_0'=4,'sp_1'=4,'sp_2'=4,'sp_3'=2,'tp'=4] {'sp_0'}, dimensions={0}, use_global_device_ids=true | all-gather | bytes 174080 | tf_op jit(solution)/shard_map/all_gather | solution.py:349
  169.6 2.4 %shard_map.162.rec_out = bf16[256,128]{1,0:T(8,128)(2,1)} custom-call(s32[5]{0:T(128)} %stack.23.place, bf16[4,136,128]{2,1,0:T(8,128)(2,1)} %all_gather.15.quads, bf16[4,136,128]{2,1,0:T(8,128)(2,1)} %copy-done.3, bf16[4,136,128]{2,1,0:T(8,128)(2,1)} %bitcast.21, f32[256,128]{1,0:T(8,128)} %get-tuple-element.18.inner, ...), custom_call_target="tpu_custom_call" | custom-call | tf_op jit(solution)/shard_map/pallas_call | solution.py:367
  173.0 2.7 %shard_map.163 = bf16[2,128,2048]{2,1,0:T(8,128)(2,1)} custom-call(bf16[256,128]{1,0:T(8,128)(2,1)} %shard_map.159.conv_out, bf16[256,128]{1,0:T(8,128)(2,1)} %shard_map.162.rec_out, bf16[8,256,256]{2,1,0:T(8,128)(2,1)} %copy-done.1), custom_call_target="tpu_custom_call" | custom-call | tf_op jit(solution)/shard_map/pallas_call | solution.py:371
  175.7 5.7 %all_to_all.46 = bf16[2,128,2048]{2,1,0:T(8,128)(2,1)S(1)} all-to-all(bf16[2,128,2048]{2,1,0:T(8,128)(2,1)} %shard_map.163), channel_id=1, replica_groups=mesh['sp_0'=4,'sp_1'=4,'sp_2'=4,'sp_3'=2,'tp'=4] {'sp_3'}, dimensions={0} | all-to-all | bytes 2097152 | tf_op jit(solution)/shard_map/all_to_all | solution.py:270
  181.7 14.5 %all_to_all.47.parts = bf16[4,32,2048]{2,1,0:T(8,128)(2,1)} all-to-all(bf16[4,32,2048]{2,1,0:T(8,128)(2,1)S(1)} %bitcast.19), channel_id=1, replica_groups=mesh['sp_0'=4,'sp_1'=4,'sp_2'=4,'sp_3'=2,'tp'=4] {'tp'}, dimensions={0} | all-to-all | bytes 1048576 | tf_op jit(solution)/shard_map/all_to_all | solution.py:270
  (30 shorter events, 17.2 us)
Async XLA Ops:
  1.4 12.5 %all-to-all-start.1 = ((bf16[4,16,384]{2,1,0:T(8,128)(2,1)}), bf16[4,16,384]{2,1,0:T(8,128)(2,1)S(1)}, u32[]{:S(2)}, u32[]{:S(2)}) async-start(bf16[4,16,384]{2,1,0:T(8,128)(2,1)} %get-tuple-element.13), calls=%async_computation.1 | async-start | bytes 98304 | tf_op jit(solution)/shard_map/all_to_all | solution.py:270
  16.5 47.1 %all-to-all-start = ((bf16[16,32,2048]{2,1,0:T(8,128)(2,1)}), bf16[16,32,2048]{2,1,0:T(8,128)(2,1)S(1)}, u32[]{:S(2)}, u32[]{:S(2)}) async-start(bf16[16,32,2048]{2,1,0:T(8,128)(2,1)} %broadcast_in_dim.9), calls=%async_computation | async-start | bytes 4194304 | tf_op jit(solution)/shard_map/all_to_all | solution.py:270
  59.3 4.3 %copy-start.2 = (bf16[1024,384]{1,0:T(8,128)(2,1)}, bf16[1024,384]{1,0:T(8,128)(2,1)S(1)}, u32[]{:S(2)}) copy-start(bf16[1024,384]{1,0:T(8,128)(2,1)S(1)} %all_gather.12.own) | copy-start | bytes 2359300
  59.3 4.3 %collective-permute-start = (bf16[1024,384]{1,0:T(8,128)(2,1)S(1)}, bf16[1024,384]{1,0:T(8,128)(2,1)}, u32[]{:S(2)}, u32[]{:S(2)}) collective-permute-start(bf16[1024,384]{1,0:T(8,128)(2,1)S(1)} %all_gather.12.own), channel_id=1, source_target_pairs={{0,4},{4,0},{1,5},{5,1},{2,6},{6,2},{3,7},{7,3},{8,12},{12,8},{9,1... | collective-permute-start | bytes 2359304 | tf_op jit(solution)/shard_map/ppermute | solution.py:317
  63.6 1.3 copy-start
  64.9 18.1 %copy-start.5 = (bf16[16,512]{1,0:T(8,128)(2,1)S(1)}, bf16[16,512]{1,0:T(8,128)(2,1)}, u32[]{:S(2)}) copy-start(bf16[16,512]{1,0:T(8,128)(2,1)} %get-tuple-element.20) | copy-start | bytes 49156
  83.7 26.3 %all-to-all-start.5 = ((bf16[16,16,512]{2,1,0:T(8,128)(2,1)}), bf16[16,16,512]{2,1,0:T(8,128)(2,1)S(1)}, u32[]{:S(2)}, u32[]{:S(2)}) async-start(bf16[16,16,512]{2,1,0:T(8,128)(2,1)} %broadcast_in_dim.10), calls=%async_computation.5 | async-start | bytes 524288 | tf_op jit(solution)/shard_map/all_to_all | solution.py:270
  94.0 7.0 %collective-permute-start.1 = (bf16[32,256]{1,0:T(8,128)(2,1)}, bf16[32,256]{1,0:T(8,128)(2,1)S(1)}, u32[]{:S(2)}, u32[]{:S(2)}) collective-permute-start(bf16[32,256]{1,0:T(8,128)(2,1)} %get-tuple-element.14), channel_id=1, source_target_pairs={{0,8},{8,16},{16,24},{24,32},{32,40},{40,48},{48,56},{56,64},{64,7... | collective-permute-start | bytes 49160 | tf_op jit(solution)/shard_map/ppermute | solution.py:352
  101.0 0.6 copy-start.6
  110.0 18.6 %all-to-all-start.3 = ((f32[8,8,256]{2,1,0:T(8,128)}), f32[8,8,256]{2,1,0:T(8,128)S(1)}, u32[]{:S(2)}, u32[]{:S(2)}) async-start(f32[8,8,256]{2,1,0:T(8,128)} %get-tuple-element.16), calls=%async_computation.3 | async-start | bytes 131072 | tf_op jit(solution)/shard_map/all_to_all | solution.py:270
  128.6 11.1 %copy-start.4 = (f32[8,8,256]{2,1,0:T(8,128)}, f32[8,8,256]{2,1,0:T(8,128)S(1)}, u32[]{:S(2)}) copy-start(f32[8,8,256]{2,1,0:T(8,128)S(1)} %all-to-all-done.3.sums) | copy-start | bytes 196612
  128.7 10.1 %all-to-all-start.4 = ((bf16[4,136,128]{2,1,0:T(8,128)(2,1)}), bf16[4,136,128]{2,1,0:T(8,128)(2,1)S(1)}, u32[]{:S(2)}, u32[]{:S(2)}) async-start(bf16[4,136,128]{2,1,0:T(8,128)(2,1)} %shard_map.160), calls=%async_computation.4 | async-start | bytes 278528 | tf_op jit(solution)/shard_map/all_to_all | solution.py:270
  138.7 8.4 %copy-start.3 = (bf16[4,136,128]{2,1,0:T(8,128)(2,1)}, bf16[4,136,128]{2,1,0:T(8,128)(2,1)S(1)}, u32[]{:S(2)}) copy-start(bf16[4,136,128]{2,1,0:T(8,128)(2,1)S(1)} %all-to-all-done.4.parts.slabs) | copy-start | bytes 417796
  139.8 32.2 %all-to-all-start.6 = ((bf16[8,256,256]{2,1,0:T(8,128)(2,1)}), bf16[8,256,256]{2,1,0:T(8,128)(2,1)S(1)}, u32[]{:S(2)}, u32[]{:S(2)}) async-start(bf16[8,256,256]{2,1,0:T(8,128)(2,1)} %bitcast.16), calls=%async_computation.6 | async-start | bytes 2097152 | tf_op jit(solution)/shard_map/all_to_all | solution.py:270
  172.0 1.0 copy-start.1

commit v4 on v3

--- a/solution.py
+++ b/solution.py
@@ -20,8 +20,10 @@
 HALO = 32
 STATE_ROWS = 136
 HALF = 128
-COLS = 384
 CHUNK = 16
+COLUMN_ROWS = 24
+OUT_ROWS = 32
+SENT_ROWS = 64
 norm_eps = 1e-06
 layer_eps = 1e-05
 HIGH = lax.Precision.HIGHEST
@@ -64,90 +66,98 @@
     return jnp.where(core == 0, value[:, :CH], value[:, CH:])
 
 
-def pack_body(query, forget, value, left, gate, outgate, conv_out, rec_out, out, rows):
-    blocks = (query, forget, value, left, gate, outgate)
-    for x in range(NX):
-        mine = [3 * x + k for k in range(3)]
-        for at, b in enumerate(sorted(mine, key=lambda b: ((b + x) % 2, b))):
-            half = b % NC
-            out[x, :, at * CH : (at + 1) * CH] = blocks[b // NC][:, half * CH : (half + 1) * CH]
+def pack_body(query, forget, value, left, gate, outgate, conv_out, rec_out, jump, out):
+    whole = (query, value, left, outgate)
+    split = (forget, forget, gate, gate)
+    lane = lax.broadcasted_iota(jnp.int32, (8, CH), 1)
     for c in range(NC):
-        for k, block in enumerate((conv_out, rec_out)):
-            at = (2 * c + k) * CH
-            rows[:, at : at + CH] = block[:, c * CH : (c + 1) * CH]
+        half = slice(c * CH, (c + 1) * CH)
+        row = jnp.broadcast_to(jump[c : c + 1], (8, CH))
+        high = row.astype(bf16).astype(f32)
+        first = lax.broadcasted_iota(jnp.int32, (8, CH), 0)
+        jumps = jnp.where(first == 0, high, row - high).astype(bf16)
+        for x in range(NX):
+            to = NC * x + c
+            out[to, :CHUNK] = whole[x][:, half]
+            rows = split[x][:, half].astype(f32)
+            turned = pltpu.roll(rows[8:], CH // 2, 1)
+            keep = lane < CH // 2 if x % 2 == 0 else lane >= CH // 2
+            out[to, CHUNK:COLUMN_ROWS] = jnp.where(keep, rows[:8], turned).astype(bf16)
+            out[to, COLUMN_ROWS : COLUMN_ROWS + CHUNK] = conv_out[:, half]
+            out[to, COLUMN_ROWS + CHUNK : COLUMN_ROWS + OUT_ROWS] = rec_out[:, half]
+            out[to, COLUMN_ROWS + OUT_ROWS :] = jumps
 
 
 def norm_body(tokens, gain, out):
     features = tokens[...].astype(f32)
-    out[...] = (
+    normed = (
         features
         * lax.rsqrt(jnp.mean(features * features, axis=1, keepdims=True) + norm_eps)
         * gain[...]
     ).astype(bf16)
-
-
-def project_body(place, tokens, own, other, jump, out, weight):
+    for k in range(NX * NY):
+        out[k] = normed
+
+
+def project_body(place, own, other, columns, out, weight):
     c = place[3]
-    blocks = NZ * NX
-    for core, piece in ((c, own), (1 - c, other)):
-
-        def copy(k, carry, core=core, piece=piece):
-            to = pl.multiple_of((NC * k + core) * CHUNK, CHUNK)
-            weight[pl.ds(to, CHUNK)] = piece[pl.ds(pl.multiple_of(k * CHUNK, CHUNK), CHUNK)]
-            return carry
-
-        lax.fori_loop(0, blocks, copy, 0, unroll=8)
-    even = lax.rem(place[2], 2)
-    for x in range(NX):
-        result = matmul(tokens[x * HALF : (x + 1) * HALF], weight[...], ((1,), (0,))).astype(bf16)
-        first = NC * x + even
-        second = NC * x + 1 - even
-        out[first, :HALF] = result[:, : 2 * CH]
-        out[second, :HALF, :CH] = result[:, 2 * CH :]
-        out[second, :HALF, CH:] = jnp.zeros((HALF, CH), bf16)
-        for k in range(NC):
-            row = jnp.broadcast_to(jump[k : k + 1], (8, CH))
-            high = row.astype(bf16)
-            out[NC * x + k, HALF:, :CH] = high
-            out[NC * x + k, HALF:, CH:] = (row - high.astype(f32)).astype(bf16)
-
-
-PLACES = (
-    ((0, 0), (0, 0)),
-    ((0, 1), (1, 0)),
-    ((1, 0), (1, 1)),
-    ((2, 0), (2, 0)),
-    ((2, 1), (3, 0)),
-    ((3, 0), (3, 1)),
-)
-
-
-def block_of(spread, m, c):
-    options = []
-    for x, at in PLACES[m]:
-        options.append(
-            jnp.concatenate(
-                [spread[NC * x + k, :HALF, at * CH : (at + 1) * CH] for k in range(NC)], axis=0
-            )
-        )
-    if PLACES[m][0] == PLACES[m][1]:
-        return options[0]
-    return jnp.where(c == 0, options[0].astype(f32), options[1].astype(f32)).astype(bf16)
-
-
-def local_body(place, spread, margin, inner, decayed, packed, tail):
+    blocks = NX * NC
+    step = blocks * CHUNK
+    for z in range(NZ):
+        at = z * step
+        piece = columns[z * blocks : (z + 1) * blocks]
+        weight[at : at + step, :CH] = piece[:, :CHUNK].reshape(step, CH)
+        packed = piece[:, CHUNK:].reshape(blocks * 8, CH).astype(f32)
+        turned = pltpu.roll(packed, CH // 2, 1).reshape(blocks, 8, CH)
+        both = jnp.concatenate([packed.reshape(blocks, 8, CH), turned], axis=1)
+        weight[at : at + step, CH:] = both.reshape(step, CH).astype(bf16)
+    for k in range(NX):
+        x = lax.rem(place[2] + k, NX)
+        rows = pl.ds(pl.multiple_of(x * HALF, HALF), HALF)
+        for core, tokens in ((c, own), (1 - c, other)):
+            to = pl.ds(pl.multiple_of(core * HALF, HALF), HALF)
+            out[k, to] = matmul(tokens[rows], weight[...], ((1,), (0,))).astype(bf16)
+
+
+def source(pieces, place, x, second):
+    slot = lax.rem(place[2] - x + NX, NX)
+    at = slice(CH, 2 * CH) if second else slice(0, CH)
+    value = pieces[0][:, at].astype(f32)
+    for k in range(1, NX):
+        value = jnp.where(slot == k, pieces[k][:, at].astype(f32), value)
+    return value
+
+
+def joined(pieces, place, x):
+    lane = lax.broadcasted_iota(jnp.int32, (ROWS, CH), 1)
+    return jnp.where(
+        lane < CH // 2, source(pieces, place, x, True), source(pieces, place, x + 1, True)
+    )
+
+
+def local_body(place, p0, p1, p2, p3, margin, jumps, inner, decayed, packed, rest, tail):
     c = place[3]
-    rows = []
-    for k in range(NC):
-        row = spread[NC * place[2] + k, HALF : HALF + 8].astype(f32)[:1]
-        rows.append(row[:, :CH] + row[:, CH:])
-    jump = jnp.concatenate(rows, axis=1)
+    pieces = (p0, p1, p2, p3)
+    jump = jnp.concatenate(
+        [
+            jumps[k, :1].astype(f32) + jumps[k, 1:2].astype(f32)
+            for k in range(NC)
+        ],
+        axis=1,
+    )
     bound = own_half(margin[...], c)
-    queries = silu(block_of(spread, 0, c).astype(f32))
-    keys = bound * sigmoid(-block_of(spread, 1, c).astype(f32))
-    inputs = block_of(spread, 2, c)
-    for k in range(2):
-        tail[:, k * CH : (k + 1) * CH] = block_of(spread, 3 + k, c)[ROWS - HALO :]
+    queries = silu(source(pieces, place, 0, False))
+    keys = bound * sigmoid(-joined(pieces, place, 0))
+    inputs = source(pieces, place, 1, False).astype(bf16)
+    others = (
+        source(pieces, place, 2, False),
+        joined(pieces, place, 2),
+        source(pieces, place, 3, False),
+    )
+    for k, value in enumerate(others):
+        rest[:, k * CH : (k + 1) * CH] = value.astype(bf16)
+        if k < 2:
+            tail[:, k * CH : (k + 1) * CH] = value[ROWS - HALO :].astype(bf16)
     log_forget = jnp.log1p(-keys)
     row = lax.broadcasted_iota(jnp.int32, (BLOCK, BLOCK), 0)
     col = lax.broadcasted_iota(jnp.int32, (BLOCK, BLOCK), 1)
@@ -199,7 +209,7 @@
         pack(total.at[k], state, decay)
 
 
-def finish_body(place, quads, slabs, chips, inner, decayed, gain, spread, out):
+def finish_body(place, quads, slabs, chips, inner, decayed, gain, rest, out):
     state = jnp.zeros((CH, CH), f32)
     for level, parts in enumerate((quads, slabs, chips)):
         for k in range(NQ):
@@ -207,15 +217,14 @@
             state = jnp.where(k < place[level], state * jnp.exp(step) + add, state)
     recurrent = inner[...] + matmul(decayed[...], state.astype(bf16), ((1,), (1,)))
     scale = lax.rsqrt(jnp.mean(recurrent * recurrent, axis=1, keepdims=True) + norm_eps)
-    gate = silu(block_of(spread, 5, place[3]).astype(f32))
+    gate = silu(rest[:, 2 * CH :].astype(f32))
     out[...] = (recurrent * scale * own_half(gain[...], place[3]) * gate).astype(bf16)
 
 
-def conv_body(place, spread, halo, taps, out, sums, gated):
+def conv_body(place, rest, halo, taps, out, sums, gated):
     rim = halo[...].astype(f32)
     gated[:HALO] = rim[:, :CH] * sigmoid(rim[:, CH:])
-    c = place[3]
-    gated[HALO:] = block_of(spread, 3, c).astype(f32) * sigmoid(block_of(spread, 4, c).astype(f32))
+    gated[HALO:] = rest[:, :CH].astype(f32) * sigmoid(rest[:, CH : 2 * CH].astype(f32))
     own_taps = own_half(taps[...], place[3])
     for n in range(ROWS // BLOCK):
         total = jnp.zeros((BLOCK, CH), f32)
@@ -248,15 +257,19 @@
     ).astype(bf16)
 
 
-def output_body(conv_out, rec_out, pieces, out, weight):
-    for k in range(NX * NC):
-        for z in range(NZ):
-            to = (z * NX * NC + k) * CHUNK
-            weight[to : to + CHUNK] = pieces[k, z * CHUNK : (z + 1) * CHUNK]
-    both = jnp.concatenate([conv_out[...], rec_out[...]], axis=1)
-    result = matmul(both, weight[...], ((1,), (1,))).astype(bf16)
-    for c in range(NC):
-        out[c] = result[c * HALF : (c + 1) * HALF]
+def output_body(place, conv_out, rec_out, pieces, mine, theirs, weight, both):
+    blocks = NX * NC
+    step = blocks * CHUNK
+    for z in range(NZ):
+        at = z * step
+        piece = pieces[z]
+        weight[at : at + step, :CH] = piece[:, :CHUNK].reshape(step, CH)
+        weight[at : at + step, CH:] = piece[:, CHUNK:].reshape(step, CH)
+    both[:, :CH] = conv_out[...]
+    both[:, CH:] = rec_out[...]
+    for core, out in ((place[3], mine), (1 - place[3], theirs)):
+        rows = pl.ds(pl.multiple_of(core * HALF, HALF), HALF)
+        out[...] = matmul(both[rows], weight[...], ((1,), (1,))).astype(bf16)
 
 
 def last_body(parts, out):
@@ -296,9 +309,7 @@
     place = jnp.stack([lax.axis_index(a) for a in SP_TP]).astype(jnp.int32)
     width = tokens.shape[1]
 
-    columns, out_rows = kernel_call(
-        pack_body, (shape((NX, CHUNK, COLS), bf16), shape((CHUNK, 4 * CH), bf16)), [VMEM] * 8
-    )(
+    payload = kernel_call(pack_body, shape((NX * NC, SENT_ROWS, CH), bf16), [VMEM] * 9)(
         query_projection_weight,
         forget_gate_weight,
         recurrence_value_weight,
@@ -307,46 +318,54 @@
         output_gate_weight,
         convolution_output_weight.T,
         recurrence_output_weight.T,
-    )
-    shard = exchanged(columns, X).reshape(NX * CHUNK, COLS)
-    normed = kernel_call(norm_body, shape((OWN, width), bf16), [VMEM, VMEM])(
-        tokens, input_norm_gain.reshape(1, width)
-    )
-    rows = to_everyone(normed, (X, Y)).reshape(NX * HALF, width)
-    own = lax.all_gather(shard, (ZH, ZL), axis=0, tiled=True)
+        decay_jump_terms,
+    )
+    arrived = exchanged(payload, (X, C))
+    copies = kernel_call(
+        norm_body, shape((NX * NY, OWN, width), bf16), [VMEM, VMEM]
+    )(tokens, input_norm_gain.reshape(1, width))
+    own = exchanged(copies, (X, Y)).reshape(NX * HALF, width)
     other = lax.ppermute(own, C, [(0, 1), (1, 0)])
-    spread = kernel_call(
+    columns = lax.all_gather(arrived[:, :COLUMN_ROWS], (ZH, ZL), axis=0, tiled=True)
+    out_pieces = to_everyone(arrived[:, COLUMN_ROWS : COLUMN_ROWS + OUT_ROWS], (ZH, ZL))
+    jumps = lax.dynamic_slice_in_dim(
+        arrived[:, COLUMN_ROWS + OUT_ROWS :], NC * lax.axis_index(X), NC, axis=0
+    )
+    projected = kernel_call(
         project_body,
-        shape((NX * NC, HALF + 8, 2 * CH), bf16),
-        [SMEM] + [VMEM] * 4,
-        [pltpu.VMEM((width, COLS), bf16)],
-    )(place, rows, own, other, decay_jump_terms)
-    spread = exchanged(spread, (X, C))
-    out_along = to_everyone(out_rows, (ZH, ZL))
-    halves = out_along.reshape(NZ * CHUNK, NC, 2 * CH).transpose(1, 0, 2)
-    halves = jnp.broadcast_to(halves, (NX, *halves.shape)).reshape(-1, *halves.shape[1:])
-    out_pieces = exchanged(halves, (X, C))
+        shape((NX, ROWS, 2 * CH), bf16),
+        [SMEM] + [VMEM] * 3,
+        [pltpu.VMEM((width, 2 * CH), bf16)],
+    )(place, own, other, columns)
+    pieces = [projected[0]]
+    for k in range(1, NX):
+        pieces.append(
+            lax.ppermute(projected[k], X, [(x, (x + k) % NX) for x in range(NX)])
+        )
 
     margin = forget_floor_margin.reshape(1, 2 * CH)
-    inner, decayed, packed, tail = kernel_call(
+    inner, decayed, packed, rest, tail = kernel_call(
         local_body,
         (
             shape((ROWS, CH), f32),
             shape((ROWS, CH), bf16),
             shape((STATE_ROWS, CH), bf16),
+            shape((ROWS, 3 * CH), bf16),
             shape((HALO, 2 * CH), bf16),
         ),
-        [SMEM] + [VMEM] * 2,
-    )(place, spread, margin)
+        [SMEM] + [VMEM] * 6,
+    )(place, *pieces, margin, jumps)
     chips = lax.all_gather(packed, X, axis=0)
 
     def total_of(parts, copies):
-        return kernel_call(total_body, shape((copies, STATE_ROWS, CH), bf16), [VMEM])(parts)
+        return kernel_call(
+            total_body, shape((copies, STATE_ROWS, CH), bf16), [VMEM]
+        )(parts)
 
     slab_copies = total_of(chips, NQ)
     slabs = exchanged(slab_copies, ZL)
-    quad = total_of(slabs, 1)[0]
-    quads = lax.all_gather(quad, ZH, axis=0)
+    quad_copies = total_of(slabs, NQ)
+    quads = exchanged(quad_copies, ZH)
 
     blocks = NZ * NX
     halo = lax.ppermute(tail, (ZH, ZL, X), [(k, k + 1) for k in range(blocks - 1)])
@@ -355,9 +374,11 @@
         (shape((ROWS, CH), bf16), shape((NC * NY, 8, ROWS), f32)),
         [SMEM, VMEM, VMEM, VMEM],
         [pltpu.VMEM((HALO + ROWS, CH), f32)],
-    )(place, spread, halo, depthwise_filter_taps)
+    )(place, rest, halo, depthwise_filter_taps)
     all_sums = exchanged(sums, (C, Y))
-    conv_out = kernel_call(channel_body, shape((ROWS, CH), bf16), [SMEM, VMEM, VMEM, VMEM, VMEM])(
+    conv_out = kernel_call(
+        channel_body, shape((ROWS, CH), bf16), [SMEM, VMEM, VMEM, VMEM, VMEM]
+    )(
         place,
         convolved,
         all_sums,
@@ -366,13 +387,16 @@
     )
     rec_out = kernel_call(
         finish_body, shape((ROWS, CH), bf16), [SMEM] + [VMEM] * 7
-    )(place, quads, slabs, chips, inner, decayed, head_norm_gain.reshape(1, 2 * CH), spread)
-
-    partial = kernel_call(
-        output_body, shape((NC, ROWS // NC, width), bf16), [VMEM] * 3,
-        [pltpu.VMEM((width, 2 * CH), bf16)],
-    )(conv_out, rec_out, out_pieces)
-    pair_sum = exchanged(partial, C).astype(f32).sum(axis=0).astype(bf16)
+    )(place, quads, slabs, chips, inner, decayed, head_norm_gain.reshape(1, 2 * CH), rest)
+
+    mine, theirs = kernel_call(
+        output_body,
+        (shape((HALF, width), bf16), shape((HALF, width), bf16)),
+        [SMEM] + [VMEM] * 3,
+        [pltpu.VMEM((width, 2 * CH), bf16), pltpu.VMEM((ROWS, 2 * CH), bf16)],
+    )(place, conv_out, rec_out, out_pieces)
+    given = lax.ppermute(theirs, C, [(0, 1), (1, 0)])
+    pair_sum = (mine.astype(f32) + given.astype(f32)).astype(bf16)
     pieces = exchanged(pair_sum.reshape(NY, OWN, width), Y)
     return kernel_call(last_body, shape((OWN, width), bf16), [VMEM])(pieces)
 

time: 199 us -> 257 us (1.29); the launches traced: 198 us -> 253 us
  waiting for transfers between devices: 17 us -> 76.6 us
  blocking collectives: 105 us -> 102 us
    all_to_all x6 -> x5, waiting for transfers between devices: 13.6 us -> 68.4 us  [exchanged(): return lax.all_to_all(x, axes, split_axis=0, concat_axis=0, tiled=True)]
    all_gather x2 -> x1, blocking collectives: 58.1 us -> 42 us  [per_device(): lax.all_gather(arrived[:, :COLUMN_ROWS], (ZH, ZL), axis=0, tiled=True)]
    all_to_all x3 -> x2, blocking collectives: 33.7 us -> 46.9 us  [exchanged(): return lax.all_to_all(x, axes, split_axis=0, concat_axis=0, tiled=True)]
    all_to_all x6 -> x5, starting transfers between devices: 35.6 us -> 22.7 us  [exchanged(): return lax.all_to_all(x, axes, split_axis=0, concat_axis=0, tiled=True)]
    ppermute x0 -> x4, starting transfers between devices: none -> 11.1 us  [the longest x3 9.23 us: per_device(): lax.ppermute(projected[k], X, [(x, (x + k) % NX) for x in range(NX)])]
    ppermute x0 -> x4, waiting for transfers between devices: none -> 6.59 us  [the longest x3 4.51 us: per_device(): lax.ppermute(projected[k], X, [(x, (x + k) % NX) for x in range(NX)])]
  transfers between devices with their start and end apart: 8 -> 11, of which waited for: 5 -> 8; matrix products, arithmetic and copies ran while one was open for 0% -> 0% of each run, Pallas kernels for 7% -> 4%
where the time goes in v4:
time: 257 us; the launch traced here: 253 us
  blocking collectives  102 us (40%)
  waiting for transfers between devices  76.6 us (30%)
  starting transfers between devices  40.4 us (16%)
  Pallas kernels  26.2 us (10%)
  local copies, waits for them, and re-layouts  6.5 us (3%)
    all_to_all x5, waiting for transfers between devices, exchanged(): return lax.all_to_all(x, axes, split_axis=0, concat_axis=0, tiled=True)  68.4 us
    all_to_all x2, blocking collectives, exchanged(): return lax.all_to_all(x, axes, split_axis=0, concat_axis=0, tiled=True)  46.9 us
    all_gather x1, blocking collectives, per_device(): lax.all_gather(arrived[:, :COLUMN_ROWS], (ZH, ZL), axis=0, tiled=True)  42 us
    all_to_all x5, starting transfers between devices, exchanged(): return lax.all_to_all(x, axes, split_axis=0, concat_axis=0, tiled=True)  22.7 us
    all_gather x1, blocking collectives, per_device(): chips = lax.all_gather(packed, X, axis=0)  13 us
    ppermute x3, starting transfers between devices, per_device(): lax.ppermute(projected[k], X, [(x, (x + k) % NX) for x in range(NX)])  9.23 us
  transfers between devices with their start and end apart: 11, of which 8 were waited for; matrix products, arithmetic and copies ran while one was open for 0% of the time, Pallas kernels for 4%

profile of v4, /device:TPU:6, one launch (start us, length us, event | category | flops | bytes accessed | tf_op | source)
XLA Modules:
  0.0 252.8 jit_solution(11896177295691564473)
XLA Ops:
  0.0 2.5 shard_map.154
  2.5 33.7 %all_to_all.35 = bf16[16,32,2048]{2,1,0:T(8,128)(2,1)S(1)} all-to-all(bf16[16,32,2048]{2,1,0:T(8,128)(2,1)} %shard_map.154), channel_id=1, replica_groups=mesh['sp_0'=4,'sp_1'=4,'sp_2'=4,'sp_3'=2,'tp'=4] {'sp_2','tp'}, dimensions={0} | all-to-all | bytes 4194304 | tf_op jit(solution)/shard_map/all_to_all | solution.py:283
  39.7 5.4 %all-to-all-start.1 = ((bf16[8,64,128]{2,1,0:T(8,128)(2,1)}), bf16[8,64,128]{2,1,0:T(8,128)(2,1)S(1)}, u32[]{:S(2)}, u32[]{:S(2)}) async-start(bf16[8,64,128]{2,1,0:T(8,128)(2,1)} %shard_map.155), calls=%async_computation.1 | async-start | bytes 262144 | tf_op jit(solution)/shard_map/all_to_all | solution.py:283
  45.7 3.4 %all-to-all-done.1 = bf16[8,64,128]{2,1,0:T(8,128)(2,1)S(1)} async-done(((bf16[8,64,128]{2,1,0:T(8,128)(2,1)}), bf16[8,64,128]{2,1,0:T(8,128)(2,1)S(1)}, u32[]{:S(2)}, u32[]{:S(2)}) %all-to-all-start.1) | async-done | bytes 131104 | tf_op jit(solution)/shard_map/all_to_all | solution.py:283
  49.2 42.0 %all_gather.9.columns = bf16[128,24,128]{2,1,0:T(8,128)(2,1)} all-gather(bf16[8,24,128]{2,1,0:T(8,128)(2,1)S(1)} %slice.28), channel_id=1, replica_groups=mesh['sp_0'=4,'sp_1'=4,'sp_2'=4,'sp_3'=2,'tp'=4] {'sp_0','sp_1'}, dimensions={0}, use_global_device_ids=true | all-gather | bytes 835584 | tf_op jit(solution)/shard_map/all_gather | solution.py:329
  91.2 4.6 %shard_map.156 = bf16[4,256,256]{2,1,0:T(8,128)(2,1)} custom-call(s32[5]{0:T(128)} %stack.23.place, bf16[512,2048]{1,0:T(8,128)(2,1)} %bitcast.24, bf16[512,2048]{1,0:T(8,128)(2,1)} %collective-permute-done.other, bf16[128,24,128]{2,1,0:T(8,128)(2,1)} %all_gather.9.columns), custom_call_target="tpu_custom_call" | custom-call | tf_op jit(solution)/shard_map/pallas_call | solution.py:334
  97.6 4.0 %collective-permute-start.1 = (bf16[256,256]{1,0:T(8,128)(2,1)S(1)}, bf16[256,256]{1,0:T(8,128)(2,1)S(1)}, u32[]{:S(2)}, u32[]{:S(2)}) collective-permute-start(bf16[256,256]{1,0:T(8,128)(2,1)S(1)} %get-tuple-element.25), channel_id=1, source_target_pairs={{0,8},{8,16},{16,24},{24,0},{1,9},{9,17},{17,25},{25,1},{2,10},{10... | collective-permute-start | bytes 393224 | tf_op jit(solution)/shard_map/ppermute | solution.py:343
  101.5 2.2 collective-permute-start.2
  103.7 3.1 %collective-permute-start.3 = (bf16[256,256]{1,0:T(8,128)(2,1)S(1)}, bf16[256,256]{1,0:T(8,128)(2,1)S(1)}, u32[]{:S(2)}, u32[]{:S(2)}) collective-permute-start(bf16[256,256]{1,0:T(8,128)(2,1)S(1)} %get-tuple-element.23), channel_id=1, source_target_pairs={{0,24},{8,0},{16,8},{24,16},{1,25},{9,1},{17,9},{25,17},{2,26},{10... | collective-permute-start | bytes 393224 | tf_op jit(solution)/shard_map/ppermute | solution.py:343
  107.4 2.5 collective-permute-done.2.p2
  112.6 3.1 %shard_map.157 = (f32[256,128]{1,0:T(8,128)}, bf16[256,128]{1,0:T(8,128)(2,1)}, bf16[136,128]{1,0:T(8,128)(2,1)}, bf16[256,384]{1,0:T(8,128)(2,1)}, bf16[32,256]{1,0:T(8,128)(2,1)}) custom-call(s32[5]{0:T(128)} %stack.23.place, bf16[256,256]{1,0:T(8,128)(2,1)} %get-tuple-element.26.p0, bf16[256,256]{1,0:T(8,128)(2,1)} %copy-done.5, ...), custom_call_target="tpu_custom_call" | custom-call | tf_op jit(solution)/shard_map/pallas_call | solution.py:347
  115.6 13.0 %all-gather = bf16[544,128]{1,0:T(8,128)(2,1)} all-gather(bf16[136,128]{1,0:T(8,128)(2,1)} %get-tuple-element.18), channel_id=2, replica_groups=mesh['sp_0'=4,'sp_1'=4,'sp_2'=4,'sp_3'=2,'tp'=4] {'sp_2'}, dimensions={0}, use_global_device_ids=true | all-gather | bytes 174080 | tf_op jit(solution)/shard_map/all_gather | solution.py:358
  130.2 3.3 %all-to-all-start.3 = ((bf16[4,136,128]{2,1,0:T(8,128)(2,1)}), bf16[4,136,128]{2,1,0:T(8,128)(2,1)S(1)}, u32[]{:S(2)}, u32[]{:S(2)}) async-start(bf16[4,136,128]{2,1,0:T(8,128)(2,1)} %shard_map.160), calls=%async_computation.3 | async-start | bytes 278528 | tf_op jit(solution)/shard_map/all_to_all | solution.py:283
  133.6 4.7 %collective-permute-start.4 = (bf16[32,256]{1,0:T(8,128)(2,1)}, bf16[32,256]{1,0:T(8,128)(2,1)S(1)}, u32[]{:S(2)}, u32[]{:S(2)}) collective-permute-start(bf16[32,256]{1,0:T(8,128)(2,1)} %get-tuple-element.15), channel_id=1, source_target_pairs={{0,8},{8,16},{16,24},{24,32},{32,40},{40,48},{48,56},{56,64},{64,7... | collective-permute-start | bytes 49160 | tf_op jit(solution)/shard_map/ppermute | solution.py:371
  140.5 2.3 shard_map.158
  142.8 3.4 %all-to-all-start.2 = ((f32[8,8,256]{2,1,0:T(8,128)}), f32[8,8,256]{2,1,0:T(8,128)S(1)}, u32[]{:S(2)}, u32[]{:S(2)}) async-start(f32[8,8,256]{2,1,0:T(8,128)} %get-tuple-element.17), calls=%async_computation.2 | async-start | bytes 131072 | tf_op jit(solution)/shard_map/all_to_all | solution.py:283
  147.8 3.6 %all-to-all-done.2.sums = f32[8,8,256]{2,1,0:T(8,128)S(1)} async-done(((f32[8,8,256]{2,1,0:T(8,128)}), f32[8,8,256]{2,1,0:T(8,128)S(1)}, u32[]{:S(2)}, u32[]{:S(2)}) %all-to-all-start.2) | async-done | bytes 65568 | tf_op jit(solution)/shard_map/all_to_all | solution.py:283
  151.4 6.9 %all-to-all-start.4 = ((bf16[4,136,128]{2,1,0:T(8,128)(2,1)}), bf16[4,136,128]{2,1,0:T(8,128)(2,1)S(1)}, u32[]{:S(2)}, u32[]{:S(2)}) async-start(bf16[4,136,128]{2,1,0:T(8,128)(2,1)} %shard_map.161), calls=%async_computation.4 | async-start | bytes 278528 | tf_op jit(solution)/shard_map/all_to_all | solution.py:283
  158.3 16.3 %all-to-all-done.4.quads = bf16[4,136,128]{2,1,0:T(8,128)(2,1)S(1)} async-done(((bf16[4,136,128]{2,1,0:T(8,128)(2,1)}), bf16[4,136,128]{2,1,0:T(8,128)(2,1)S(1)}, u32[]{:S(2)}, u32[]{:S(2)}) %all-to-all-start.4) | async-done | bytes 139296 | tf_op jit(solution)/shard_map/all_to_all | solution.py:283
  175.8 3.7 %all-to-all-start.5 = ((bf16[16,8,32,128]{3,2,1,0:T(8,128)(2,1)}), bf16[16,8,32,128]{3,2,1,0:T(8,128)(2,1)S(1)}, u32[]{:S(2)}, u32[]{:S(2)}) async-start(bf16[16,8,32,128]{3,2,1,0:T(8,128)(2,1)} %broadcast_in_dim.3), calls=%async_computation.5 | async-start | bytes 2097152 | tf_op jit(solution)/shard_map/all_to_all | solution.py:283
  181.5 2.2 shard_map.162.rec_out
  183.8 45.0 %all-to-all-done.5.pieces = bf16[16,8,32,128]{3,2,1,0:T(8,128)(2,1)S(1)} async-done(((bf16[16,8,32,128]{3,2,1,0:T(8,128)(2,1)}), bf16[16,8,32,128]{3,2,1,0:T(8,128)(2,1)S(1)}, u32[]{:S(2)}, u32[]{:S(2)}) %all-to-all-start.5) | async-done | bytes 1048608 | tf_op jit(solution)/shard_map/all_to_all | solution.py:283
  229.8 2.9 %shard_map.163 = (bf16[128,2048]{1,0:T(8,128)(2,1)}, bf16[128,2048]{1,0:T(8,128)(2,1)}) custom-call(s32[5]{0:T(128)} %stack.23.place, bf16[256,128]{1,0:T(8,128)(2,1)} %shard_map.159.conv_out, bf16[256,128]{1,0:T(8,128)(2,1)} %shard_map.162.rec_out, bf16[16,8,32,128]{3,2,1,0:T(8,128)(2,1)} %copy-done.1), custom_call_target="tpu_custom_call" | custom-call | tf_op jit(solution)/shard_map/pallas_call | solution.py:392
  237.9 13.2 %all_to_all.36.parts = bf16[4,32,2048]{2,1,0:T(8,128)(2,1)} all-to-all(bf16[4,32,2048]{2,1,0:T(8,128)(2,1)S(1)} %bitcast.25), channel_id=1, replica_groups=mesh['sp_0'=4,'sp_1'=4,'sp_2'=4,'sp_3'=2,'tp'=4] {'tp'}, dimensions={0} | all-to-all | bytes 1048576 | tf_op jit(solution)/shard_map/all_to_all | solution.py:283
  (39 shorter events, 25.8 us)
Async XLA Ops:
  36.2 54.9 %copy-start = (bf16[16,32,2048]{2,1,0:T(8,128)(2,1)}, bf16[16,32,2048]{2,1,0:T(8,128)(2,1)S(1)}, u32[]{:S(2)}) copy-start(bf16[16,32,2048]{2,1,0:T(8,128)(2,1)S(1)} %all_to_all.35) | copy-start | bytes 6291460
  36.2 54.9 %collective-permute-start = (bf16[512,2048]{1,0:T(8,128)(2,1)S(1)}, bf16[512,2048]{1,0:T(8,128)(2,1)}, u32[]{:S(2)}, u32[]{:S(2)}) collective-permute-start(bf16[512,2048]{1,0:T(8,128)(2,1)S(1)} %bitcast.23), channel_id=1, source_target_pairs={{0,4},{4,0},{1,5},{5,1},{2,6},{6,2},{3,7},{7,3},{8,12},{12,8},{9,1... | collective-permute-start | bytes 6291464 | tf_op jit(solution)/shard_map/ppermute | solution.py:328
  39.7 9.5 %all-to-all-start.1 = ((bf16[8,64,128]{2,1,0:T(8,128)(2,1)}), bf16[8,64,128]{2,1,0:T(8,128)(2,1)S(1)}, u32[]{:S(2)}, u32[]{:S(2)}) async-start(bf16[8,64,128]{2,1,0:T(8,128)(2,1)} %shard_map.155), calls=%async_computation.1 | async-start | bytes 262144 | tf_op jit(solution)/shard_map/all_to_all | solution.py:283
  97.6 9.9 %collective-permute-start.1 = (bf16[256,256]{1,0:T(8,128)(2,1)S(1)}, bf16[256,256]{1,0:T(8,128)(2,1)S(1)}, u32[]{:S(2)}, u32[]{:S(2)}) collective-permute-start(bf16[256,256]{1,0:T(8,128)(2,1)S(1)} %get-tuple-element.25), channel_id=1, source_target_pairs={{0,8},{8,16},{16,24},{24,0},{1,9},{9,17},{17,25},{25,1},{2,10},{10... | collective-permute-start | bytes 393224 | tf_op jit(solution)/shard_map/ppermute | solution.py:343
  101.5 8.4 %collective-permute-start.2 = (bf16[256,256]{1,0:T(8,128)(2,1)S(1)}, bf16[256,256]{1,0:T(8,128)(2,1)S(1)}, u32[]{:S(2)}, u32[]{:S(2)}) collective-permute-start(bf16[256,256]{1,0:T(8,128)(2,1)S(1)} %get-tuple-element.24), channel_id=1, source_target_pairs={{0,16},{8,24},{16,0},{24,8},{1,17},{9,25},{17,1},{25,9},{2,18},{10... | collective-permute-start | bytes 393224 | tf_op jit(solution)/shard_map/ppermute | solution.py:343
  103.7 8.2 %collective-permute-start.3 = (bf16[256,256]{1,0:T(8,128)(2,1)S(1)}, bf16[256,256]{1,0:T(8,128)(2,1)S(1)}, u32[]{:S(2)}, u32[]{:S(2)}) collective-permute-start(bf16[256,256]{1,0:T(8,128)(2,1)S(1)} %get-tuple-element.23), channel_id=1, source_target_pairs={{0,24},{8,0},{16,8},{24,16},{1,25},{9,1},{17,9},{25,17},{2,26},{10... | collective-permute-start | bytes 393224 | tf_op jit(solution)/shard_map/ppermute | solution.py:343
  107.4 4.5 %copy-start.5 = (bf16[256,256]{1,0:T(8,128)(2,1)}, bf16[256,256]{1,0:T(8,128)(2,1)S(1)}, u32[]{:S(2)}) copy-start(bf16[256,256]{1,0:T(8,128)(2,1)S(1)} %collective-permute-done.1.p1) | copy-start | bytes 393220
  109.9 2.0 copy-start.6
  111.9 0.7 copy-start.7
  130.2 12.6 %all-to-all-start.3 = ((bf16[4,136,128]{2,1,0:T(8,128)(2,1)}), bf16[4,136,128]{2,1,0:T(8,128)(2,1)S(1)}, u32[]{:S(2)}, u32[]{:S(2)}) async-start(bf16[4,136,128]{2,1,0:T(8,128)(2,1)} %shard_map.160), calls=%async_computation.3 | async-start | bytes 278528 | tf_op jit(solution)/shard_map/all_to_all | solution.py:283
  133.6 6.3 %collective-permute-start.4 = (bf16[32,256]{1,0:T(8,128)(2,1)}, bf16[32,256]{1,0:T(8,128)(2,1)S(1)}, u32[]{:S(2)}, u32[]{:S(2)}) collective-permute-start(bf16[32,256]{1,0:T(8,128)(2,1)} %get-tuple-element.15), channel_id=1, source_target_pairs={{0,8},{8,16},{16,24},{24,32},{32,40},{40,48},{48,56},{56,64},{64,7... | collective-permute-start | bytes 49160 | tf_op jit(solution)/shard_map/ppermute | solution.py:371
  139.9 0.6 copy-start.8
  142.8 3.4 %copy-start.2 = (bf16[4,136,128]{2,1,0:T(8,128)(2,1)}, bf16[4,136,128]{2,1,0:T(8,128)(2,1)S(1)}, u32[]{:S(2)}) copy-start(bf16[4,136,128]{2,1,0:T(8,128)(2,1)S(1)} %all-to-all-done.3.parts.slabs) | copy-start | bytes 417796
  142.8 8.6 %all-to-all-start.2 = ((f32[8,8,256]{2,1,0:T(8,128)}), f32[8,8,256]{2,1,0:T(8,128)S(1)}, u32[]{:S(2)}, u32[]{:S(2)}) async-start(f32[8,8,256]{2,1,0:T(8,128)} %get-tuple-element.17), calls=%async_computation.2 | async-start | bytes 131072 | tf_op jit(solution)/shard_map/all_to_all | solution.py:283
  151.4 28.1 %copy-start.4 = (f32[8,8,256]{2,1,0:T(8,128)}, f32[8,8,256]{2,1,0:T(8,128)S(1)}, u32[]{:S(2)}) copy-start(f32[8,8,256]{2,1,0:T(8,128)S(1)} %all-to-all-done.2.sums) | copy-start | bytes 196612
  151.4 23.2 %all-to-all-start.4 = ((bf16[4,136,128]{2,1,0:T(8,128)(2,1)}), bf16[4,136,128]{2,1,0:T(8,128)(2,1)S(1)}, u32[]{:S(2)}, u32[]{:S(2)}) async-start(bf16[4,136,128]{2,1,0:T(8,128)(2,1)} %shard_map.161), calls=%async_computation.4 | async-start | bytes 278528 | tf_op jit(solution)/shard_map/all_to_all | solution.py:283
  174.6 6.9 %copy-start.3 = (bf16[4,136,128]{2,1,0:T(8,128)(2,1)}, bf16[4,136,128]{2,1,0:T(8,128)(2,1)S(1)}, u32[]{:S(2)}) copy-start(bf16[4,136,128]{2,1,0:T(8,128)(2,1)S(1)} %all-to-all-done.4.quads) | copy-start | bytes 417796
  175.8 53.0 %all-to-all-start.5 = ((bf16[16,8,32,128]{3,2,1,0:T(8,128)(2,1)}), bf16[16,8,32,128]{3,2,1,0:T(8,128)(2,1)S(1)}, u32[]{:S(2)}, u32[]{:S(2)}) async-start(bf16[16,8,32,128]{3,2,1,0:T(8,128)(2,1)} %broadcast_in_dim.3), calls=%async_computation.5 | async-start | bytes 2097152 | tf_op jit(solution)/shard_map/all_to_all | solution.py:283
  228.8 1.0 copy-start.1
  232.7 4.0 %collective-permute-start.5 = (bf16[128,2048]{1,0:T(8,128)(2,1)}, bf16[128,2048]{1,0:T(8,128)(2,1)S(1)}, u32[]{:S(2)}, u32[]{:S(2)}) collective-permute-start(bf16[128,2048]{1,0:T(8,128)(2,1)} %get-tuple-element.22), channel_id=1, source_target_pairs={{0,4},{4,0},{1,5},{5,1},{2,6},{6,2},{3,7},{7,3},{8,12},{12,8},{9,1... | collective-permute-start | bytes 1572872 | tf_op jit(solution)/shard_map/ppermute | solution.py:398

commit v5 on v4

--- a/solution.py
+++ b/solution.py
@@ -24,6 +24,7 @@
 COLUMN_ROWS = 24
 OUT_ROWS = 32
 SENT_ROWS = 64
+CARRIED = 7
 norm_eps = 1e-06
 layer_eps = 1e-05
 HIGH = lax.Precision.HIGHEST
@@ -99,24 +100,39 @@
         out[k] = normed
 
 
-def project_body(place, own, other, columns, out, weight):
+def sort_body(arrived, along, rest):
+    blocks = NX * NC
+    split = COLUMN_ROWS + OUT_ROWS - 8
+    for k in range(blocks):
+        along[k * COLUMN_ROWS : (k + 1) * COLUMN_ROWS] = arrived[k, :COLUMN_ROWS]
+        rest[k * 24 : (k + 1) * 24] = arrived[k, COLUMN_ROWS:split]
+        last = arrived[k, split : split + 8]
+        if k < CARRIED:
+            at = blocks * COLUMN_ROWS + k * 8
+            along[at : at + 8] = last
+        else:
+            rest[blocks * 24 :] = last
+
+
+def project_body(place, own, other, columns, out0, out1, out2, out3, weight):
     c = place[3]
     blocks = NX * NC
     step = blocks * CHUNK
     for z in range(NZ):
         at = z * step
-        piece = columns[z * blocks : (z + 1) * blocks]
+        piece = columns[z, : blocks * COLUMN_ROWS].reshape(blocks, COLUMN_ROWS, CH)
         weight[at : at + step, :CH] = piece[:, :CHUNK].reshape(step, CH)
         packed = piece[:, CHUNK:].reshape(blocks * 8, CH).astype(f32)
         turned = pltpu.roll(packed, CH // 2, 1).reshape(blocks, 8, CH)
         both = jnp.concatenate([packed.reshape(blocks, 8, CH), turned], axis=1)
         weight[at : at + step, CH:] = both.reshape(step, CH).astype(bf16)
+    outs = (out0, out1, out2, out3)
     for k in range(NX):
         x = lax.rem(place[2] + k, NX)
         rows = pl.ds(pl.multiple_of(x * HALF, HALF), HALF)
         for core, tokens in ((c, own), (1 - c, other)):
             to = pl.ds(pl.multiple_of(core * HALF, HALF), HALF)
-            out[k, to] = matmul(tokens[rows], weight[...], ((1,), (0,))).astype(bf16)
+            outs[k][to] = matmul(tokens[rows], weight[...], ((1,), (0,))).astype(bf16)
 
 
 def source(pieces, place, x, second):
@@ -135,16 +151,12 @@
     )
 
 
-def local_body(place, p0, p1, p2, p3, margin, jumps, inner, decayed, packed, rest, tail):
+def local_body(place, p0, p1, p2, p3, margin, arrived, inner, decayed, packed, rest, tail):
     c = place[3]
     pieces = (p0, p1, p2, p3)
-    jump = jnp.concatenate(
-        [
-            jumps[k, :1].astype(f32) + jumps[k, 1:2].astype(f32)
-            for k in range(NC)
-        ],
-        axis=1,
-    )
+    at = COLUMN_ROWS + OUT_ROWS
+    rows = [arrived[NC * place[2] + k, at : at + 8].astype(f32) for k in range(NC)]
+    jump = jnp.concatenate([r[:1] + r[1:2] for r in rows], axis=1)
     bound = own_half(margin[...], c)
     queries = silu(source(pieces, place, 0, False))
     keys = bound * sigmoid(-joined(pieces, place, 0))
@@ -209,12 +221,12 @@
         pack(total.at[k], state, decay)
 
 
-def finish_body(place, quads, slabs, chips, inner, decayed, gain, rest, out):
+def finish_body(place, slabs, chips, inner, decayed, gain, rest, out):
     state = jnp.zeros((CH, CH), f32)
-    for level, parts in enumerate((quads, slabs, chips)):
-        for k in range(NQ):
+    for parts, mine in ((slabs, NQ * place[0] + place[1]), (chips, place[2])):
+        for k in range(parts.shape[0]):
             step, add = unpacked(parts[k])
-            state = jnp.where(k < place[level], state * jnp.exp(step) + add, state)
+            state = jnp.where(k < mine, state * jnp.exp(step) + add, state)
     recurrent = inner[...] + matmul(decayed[...], state.astype(bf16), ((1,), (1,)))
     scale = lax.rsqrt(jnp.mean(recurrent * recurrent, axis=1, keepdims=True) + norm_eps)
     gate = silu(rest[:, 2 * CH :].astype(f32))
@@ -237,15 +249,11 @@
     first_sum = matmul(ones, values, ((1,), (1,)), HIGH)
     second_sum = matmul(ones, values * values, ((1,), (1,)), HIGH)
     row = lax.broadcasted_iota(jnp.int32, (8, ROWS), 0)
-    both_sums = jnp.where(row == 0, first_sum, second_sum)
-    for k in range(NC * NY):
-        sums[k] = both_sums
-
-
-def channel_body(place, values, sums, gain, bias, out):
-    total = sums[0]
-    for k in range(1, NC * NY):
-        total = total + sums[k]
+    sums[...] = jnp.where(row == 0, first_sum, second_sum)
+
+
+def channel_body(place, values, s0, s1, s2, s3, gain, bias, out):
+    total = s0[...] + s1[...] + s2[...] + s3[...]
     row = lax.broadcasted_iota(jnp.int32, (8, CH), 0)
     pick_first = jnp.where(row == 0, 1.0 / CONV_CH, 0.0)
     pick_second = jnp.where(row == 1, 1.0 / CONV_CH, 0.0)
@@ -257,26 +265,24 @@
     ).astype(bf16)
 
 
-def output_body(place, conv_out, rec_out, pieces, mine, theirs, weight, both):
+def output_body(place, conv_out, rec_out, columns, pieces, mine, theirs, weight, both):
     blocks = NX * NC
     step = blocks * CHUNK
     for z in range(NZ):
+        piece = pieces[z, : blocks * 24].reshape(blocks, 24, CH)
         at = z * step
-        piece = pieces[z]
         weight[at : at + step, :CH] = piece[:, :CHUNK].reshape(step, CH)
-        weight[at : at + step, CH:] = piece[:, CHUNK:].reshape(step, CH)
+        carried = columns[z, blocks * COLUMN_ROWS :].astype(f32)
+        last = jnp.concatenate([carried, pieces[z, blocks * 24 :].astype(f32)], axis=0)
+        second = jnp.concatenate(
+            [piece[:, CHUNK:].astype(f32), last.reshape(blocks, 8, CH)], axis=1
+        )
+        weight[at : at + step, CH:] = second.reshape(step, CH).astype(bf16)
     both[:, :CH] = conv_out[...]
     both[:, CH:] = rec_out[...]
     for core, out in ((place[3], mine), (1 - place[3], theirs)):
         rows = pl.ds(pl.multiple_of(core * HALF, HALF), HALF)
         out[...] = matmul(both[rows], weight[...], ((1,), (1,))).astype(bf16)
-
-
-def last_body(parts, out):
-    total = parts[0].astype(f32)
-    for y in range(1, NY):
-        total = total + parts[y].astype(f32)
-    out[...] = total.astype(bf16)
 
 
 def exchanged(x, axes):
@@ -326,14 +332,15 @@
     )(tokens, input_norm_gain.reshape(1, width))
     own = exchanged(copies, (X, Y)).reshape(NX * HALF, width)
     other = lax.ppermute(own, C, [(0, 1), (1, 0)])
-    columns = lax.all_gather(arrived[:, :COLUMN_ROWS], (ZH, ZL), axis=0, tiled=True)
-    out_pieces = to_everyone(arrived[:, COLUMN_ROWS : COLUMN_ROWS + OUT_ROWS], (ZH, ZL))
-    jumps = lax.dynamic_slice_in_dim(
-        arrived[:, COLUMN_ROWS + OUT_ROWS :], NC * lax.axis_index(X), NC, axis=0
-    )
+    along, rest_rows = kernel_call(
+        sort_body, (shape((248, CH), bf16), shape((200, CH), bf16)), [VMEM]
+    )(arrived)
+    columns = lax.all_gather(along, (ZH, ZL), axis=0)
+    out_pieces = to_everyone(rest_rows, (ZH, ZL))
+    piece = shape((ROWS, 2 * CH), bf16)
     projected = kernel_call(
         project_body,
-        shape((NX, ROWS, 2 * CH), bf16),
+        (piece, piece, piece, piece),
         [SMEM] + [VMEM] * 3,
         [pltpu.VMEM((width, 2 * CH), bf16)],
     )(place, own, other, columns)
@@ -354,7 +361,7 @@
             shape((HALO, 2 * CH), bf16),
         ),
         [SMEM] + [VMEM] * 6,
-    )(place, *pieces, margin, jumps)
+    )(place, *pieces, margin, arrived)
     chips = lax.all_gather(packed, X, axis=0)
 
     def total_of(parts, copies):
@@ -362,43 +369,42 @@
             total_body, shape((copies, STATE_ROWS, CH), bf16), [VMEM]
         )(parts)
 
-    slab_copies = total_of(chips, NQ)
-    slabs = exchanged(slab_copies, ZL)
-    quad_copies = total_of(slabs, NQ)
-    quads = exchanged(quad_copies, ZH)
+    slab_copies = total_of(chips, NZ)
+    slabs = exchanged(slab_copies, (ZH, ZL))
 
     blocks = NZ * NX
     halo = lax.ppermute(tail, (ZH, ZL, X), [(k, k + 1) for k in range(blocks - 1)])
     convolved, sums = kernel_call(
         conv_body,
-        (shape((ROWS, CH), bf16), shape((NC * NY, 8, ROWS), f32)),
+        (shape((ROWS, CH), bf16), shape((8, ROWS), f32)),
         [SMEM, VMEM, VMEM, VMEM],
         [pltpu.VMEM((HALO + ROWS, CH), f32)],
     )(place, rest, halo, depthwise_filter_taps)
-    all_sums = exchanged(sums, (C, Y))
-    conv_out = kernel_call(
-        channel_body, shape((ROWS, CH), bf16), [SMEM, VMEM, VMEM, VMEM, VMEM]
-    )(
+    sums = sums + lax.ppermute(sums, C, [(0, 1), (1, 0)])
+    all_sums = [sums]
+    for k in range(1, NY):
+        all_sums.append(lax.ppermute(sums, Y, [(y, (y + k) % NY) for y in range(NY)]))
+    conv_out = kernel_call(channel_body, shape((ROWS, CH), bf16), [SMEM] + [VMEM] * 7)(
         place,
         convolved,
-        all_sums,
+        *all_sums,
         channel_norm_gain.reshape(1, 2 * CH),
         channel_norm_bias.reshape(1, 2 * CH),
     )
     rec_out = kernel_call(
-        finish_body, shape((ROWS, CH), bf16), [SMEM] + [VMEM] * 7
-    )(place, quads, slabs, chips, inner, decayed, head_norm_gain.reshape(1, 2 * CH), rest)
+        finish_body, shape((ROWS, CH), bf16), [SMEM] + [VMEM] * 6
+    )(place, slabs, chips, inner, decayed, head_norm_gain.reshape(1, 2 * CH), rest)
 
     mine, theirs = kernel_call(
         output_body,
         (shape((HALF, width), bf16), shape((HALF, width), bf16)),
-        [SMEM] + [VMEM] * 3,
+        [SMEM] + [VMEM] * 4,
         [pltpu.VMEM((width, 2 * CH), bf16), pltpu.VMEM((ROWS, 2 * CH), bf16)],
-    )(place, conv_out, rec_out, out_pieces)
+    )(place, conv_out, rec_out, columns, out_pieces)
     given = lax.ppermute(theirs, C, [(0, 1), (1, 0)])
     pair_sum = (mine.astype(f32) + given.astype(f32)).astype(bf16)
     pieces = exchanged(pair_sum.reshape(NY, OWN, width), Y)
-    return kernel_call(last_body, shape((OWN, width), bf16), [VMEM])(pieces)
+    return pieces.astype(f32).sum(axis=0).astype(bf16)
 
 
 def solution(mesh):

time: 257 us -> 242 us (0.942)
  the two profiles are of different devices: /device:TPU:6 before, /device:TPU:96 now
where the time goes in v5:
time: 242 us; the launch traced here: 240 us
  blocking collectives  133 us (55%)
  waiting for transfers between devices  37.7 us (16%)
  starting transfers between devices  36.8 us (15%)
  Pallas kernels  24.9 us (10%)
  local copies, waits for them, and re-layouts  5.03 us (2%)
  other arithmetic  2.61 us (1%)
    all_to_all x3, blocking collectives, exchanged(): return lax.all_to_all(x, axes, split_axis=0, concat_axis=0, tiled=True)  81.3 us
    all_gather x1, blocking collectives, per_device(): columns = lax.all_gather(along, (ZH, ZL), axis=0)  39 us
    ppermute x1, waiting for transfers between devices, per_device(): lax.ppermute(tail, (ZH, ZL, X), [(k, k + 1) for k in range(blocks - 1)])  22.3 us
    all_gather x1, blocking collectives, per_device(): chips = lax.all_gather(packed, X, axis=0)  13 us
    ppermute x3, starting transfers between devices, per_device(): lax.ppermute(sums, Y, [(y, (y + k) % NY) for y in range(NY)])  9.82 us
    all_to_all x2, starting transfers between devices, exchanged(): return lax.all_to_all(x, axes, split_axis=0, concat_axis=0, tiled=True)  9.56 us
    ppermute x3, starting transfers between devices, per_device(): lax.ppermute(projected[k], X, [(x, (x + k) % NX) for x in range(NX)])  9.1 us
    all_to_all x2, waiting for transfers between devices, exchanged(): return lax.all_to_all(x, axes, split_axis=0, concat_axis=0, tiled=True)  5.41 us
  transfers between devices with their start and end apart: 12, of which 7 were waited for; matrix products, arithmetic and copies ran while one was open for 1% of the time, Pallas kernels for 4%

profile of v5, /device:TPU:96, one launch (start us, length us, event | category | flops | bytes accessed | tf_op | source)
XLA Modules:
  0.0 240.4 jit_solution(4664372436399580058)
XLA Ops:
  0.0 2.5 %shard_map.154 = bf16[16,32,2048]{2,1,0:T(8,128)(2,1)} custom-call(bf16[32,2048]{1,0:T(8,128)(2,1)} %tokens.1, f32[1,2048]{1,0:T(1,128)} %bitcast.23), custom_call_target="tpu_custom_call" | custom-call | tf_op jit(solution)/shard_map/pallas_call | solution.py:330
  2.5 35.3 %all_to_all.25 = bf16[16,32,2048]{2,1,0:T(8,128)(2,1)S(1)} all-to-all(bf16[16,32,2048]{2,1,0:T(8,128)(2,1)} %shard_map.154), channel_id=1, replica_groups=mesh['sp_0'=4,'sp_1'=4,'sp_2'=4,'sp_3'=2,'tp'=4] {'sp_2','tp'}, dimensions={0} | all-to-all | bytes 4194304 | tf_op jit(solution)/shard_map/all_to_all | solution.py:289
  41.2 3.4 %all-to-all-start.1 = ((bf16[8,64,128]{2,1,0:T(8,128)(2,1)}), bf16[8,64,128]{2,1,0:T(8,128)(2,1)S(1)}, u32[]{:S(2)}, u32[]{:S(2)}) async-start(bf16[8,64,128]{2,1,0:T(8,128)(2,1)} %shard_map.155), calls=%async_computation.1 | async-start | bytes 262144 | tf_op jit(solution)/shard_map/all_to_all | solution.py:289
  45.2 5.4 %all-to-all-done.1.arrived = bf16[8,64,128]{2,1,0:T(8,128)(2,1)S(1)} async-done(((bf16[8,64,128]{2,1,0:T(8,128)(2,1)}), bf16[8,64,128]{2,1,0:T(8,128)(2,1)S(1)}, u32[]{:S(2)}, u32[]{:S(2)}) %all-to-all-start.1) | async-done | bytes 131104 | tf_op jit(solution)/shard_map/all_to_all | solution.py:289
  52.9 39.0 %all-gather = bf16[3968,128]{1,0:T(8,128)(2,1)} all-gather(bf16[248,128]{1,0:T(8,128)(2,1)} %get-tuple-element.20), channel_id=2, replica_groups=mesh['sp_0'=4,'sp_1'=4,'sp_2'=4,'sp_3'=2,'tp'=4] {'sp_0','sp_1'}, dimensions={0}, use_global_device_ids=true | all-gather | bytes 1079296 | tf_op jit(solution)/shard_map/all_gather | solution.py:338
  91.9 4.5 %shard_map.157 = (bf16[256,256]{1,0:T(8,128)(2,1)}, bf16[256,256]{1,0:T(8,128)(2,1)}, bf16[256,256]{1,0:T(8,128)(2,1)}, bf16[256,256]{1,0:T(8,128)(2,1)}) custom-call(s32[5]{0:T(128)} %stack.23.place, bf16[512,2048]{1,0:T(8,128)(2,1)} %bitcast.19, bf16[512,2048]{1,0:T(8,128)(2,1)} %collective-permute-done.other, bf16[16,248,128]{2,1,0:T(8,128)(2,1)} %bitcast.16), custom_call_target="tpu_custom_call" | custom-call | tf_op jit(solution)/shard_map/pallas_call | solution.py:341
  96.4 2.6 %collective-permute-start.1 = (bf16[256,256]{1,0:T(8,128)(2,1)}, bf16[256,256]{1,0:T(8,128)(2,1)S(1)}, u32[]{:S(2)}, u32[]{:S(2)}) collective-permute-start(bf16[256,256]{1,0:T(8,128)(2,1)} %get-tuple-element.22), channel_id=1, source_target_pairs={{0,8},{8,16},{16,24},{24,0},{1,9},{9,17},{17,25},{25,1},{2,10},{10... | collective-permute-start | bytes 393224 | tf_op jit(solution)/shard_map/ppermute | solution.py:350
  99.0 3.9 %collective-permute-start.2 = (bf16[256,256]{1,0:T(8,128)(2,1)}, bf16[256,256]{1,0:T(8,128)(2,1)S(1)}, u32[]{:S(2)}, u32[]{:S(2)}) collective-permute-start(bf16[256,256]{1,0:T(8,128)(2,1)} %get-tuple-element.23), channel_id=1, source_target_pairs={{0,16},{8,24},{16,0},{24,8},{1,17},{9,25},{17,1},{25,9},{2,18},{10... | collective-permute-start | bytes 393224 | tf_op jit(solution)/shard_map/ppermute | solution.py:350
  102.9 2.6 %collective-permute-start.3 = (bf16[256,256]{1,0:T(8,128)(2,1)}, bf16[256,256]{1,0:T(8,128)(2,1)S(1)}, u32[]{:S(2)}, u32[]{:S(2)}) collective-permute-start(bf16[256,256]{1,0:T(8,128)(2,1)} %get-tuple-element.24), channel_id=1, source_target_pairs={{0,24},{8,0},{16,8},{24,16},{1,25},{9,1},{17,9},{25,17},{2,26},{10... | collective-permute-start | bytes 393224 | tf_op jit(solution)/shard_map/ppermute | solution.py:350
  107.5 2.6 %collective-permute-done.3.p3 = bf16[256,256]{1,0:T(8,128)(2,1)S(1)} collective-permute-done((bf16[256,256]{1,0:T(8,128)(2,1)}, bf16[256,256]{1,0:T(8,128)(2,1)S(1)}, u32[]{:S(2)}, u32[]{:S(2)}) %collective-permute-start.3) | collective-permute-done | bytes 131104 | tf_op jit(solution)/shard_map/ppermute | solution.py:350
  110.8 3.1 %shard_map.158 = (f32[256,128]{1,0:T(8,128)}, bf16[256,128]{1,0:T(8,128)(2,1)}, bf16[136,128]{1,0:T(8,128)(2,1)}, bf16[256,384]{1,0:T(8,128)(2,1)}, bf16[32,256]{1,0:T(8,128)(2,1)}) custom-call(s32[5]{0:T(128)} %stack.23.place, bf16[256,256]{1,0:T(8,128)(2,1)} %get-tuple-element.21.p0, bf16[256,256]{1,0:T(8,128)(2,1)} %copy-done.3, ...), custom_call_target="tpu_custom_call" | custom-call | tf_op jit(solution)/shard_map/pallas_call | solution.py:354
  114.0 13.0 %all-gather.1 = bf16[544,128]{1,0:T(8,128)(2,1)} all-gather(bf16[136,128]{1,0:T(8,128)(2,1)} %get-tuple-element.29), channel_id=3, replica_groups=mesh['sp_0'=4,'sp_1'=4,'sp_2'=4,'sp_3'=2,'tp'=4] {'sp_2'}, dimensions={0}, use_global_device_ids=true | all-gather | bytes 174080 | tf_op jit(solution)/shard_map/all_gather | solution.py:365
  128.7 32.3 %all_to_all.26.slabs = bf16[16,136,128]{2,1,0:T(8,128)(2,1)} all-to-all(bf16[16,136,128]{2,1,0:T(8,128)(2,1)} %shard_map.161), channel_id=1, replica_groups=mesh['sp_0'=4,'sp_1'=4,'sp_2'=4,'sp_3'=2,'tp'=4] {'sp_0','sp_1'}, dimensions={0} | all-to-all | bytes 1114112 | tf_op jit(solution)/shard_map/all_to_all | solution.py:289
  162.1 6.2 %all-to-all-start.3 = ((bf16[16,200,128]{2,1,0:T(8,128)(2,1)}), bf16[16,200,128]{2,1,0:T(8,128)(2,1)S(1)}, u32[]{:S(2)}, u32[]{:S(2)}) async-start(bf16[16,200,128]{2,1,0:T(8,128)(2,1)} %broadcast_in_dim.3), calls=%async_computation.3 | async-start | bytes 1638400 | tf_op jit(solution)/shard_map/all_to_all | solution.py:289
  168.3 2.6 %collective-permute-start.4 = (bf16[32,256]{1,0:T(8,128)(2,1)S(1)}, bf16[32,256]{1,0:T(8,128)(2,1)S(1)}, u32[]{:S(2)}, u32[]{:S(2)}) collective-permute-start(bf16[32,256]{1,0:T(8,128)(2,1)S(1)} %copy-done.12), channel_id=1, source_target_pairs={{0,8},{8,16},{16,24},{24,32},{32,40},{40,48},{48,56},{56,64},{64,7... | collective-permute-start | bytes 49160 | tf_op jit(solution)/shard_map/ppermute | solution.py:376
  170.8 22.3 %collective-permute-done.4.halo = bf16[32,256]{1,0:T(8,128)(2,1)S(1)} collective-permute-done((bf16[32,256]{1,0:T(8,128)(2,1)S(1)}, bf16[32,256]{1,0:T(8,128)(2,1)S(1)}, u32[]{:S(2)}, u32[]{:S(2)}) %collective-permute-start.4) | collective-permute-done | bytes 16416 | tf_op jit(solution)/shard_map/ppermute | solution.py:376
  193.7 2.2 shard_map.159
  199.9 2.2 collective-permute-start.6
  202.1 4.0 %collective-permute-start.7 = (f32[8,256]{1,0:T(8,128)S(1)}, f32[8,256]{1,0:T(8,128)S(1)}, u32[]{:S(2)}, u32[]{:S(2)}) collective-permute-start(f32[8,256]{1,0:T(8,128)S(1)} %add.6.s0), channel_id=1, source_target_pairs={{0,2},{1,3},{2,0},{3,1},{4,6},{5,7},{6,4},{7,5},{8,10},{9,11},{10,... | collective-permute-start | bytes 24584 | tf_op jit(solution)/shard_map/ppermute | solution.py:386
  206.2 3.6 %collective-permute-start.8 = (f32[8,256]{1,0:T(8,128)S(1)}, f32[8,256]{1,0:T(8,128)S(1)}, u32[]{:S(2)}, u32[]{:S(2)}) collective-permute-start(f32[8,256]{1,0:T(8,128)S(1)} %add.6.s0), channel_id=1, source_target_pairs={{0,3},{1,0},{2,1},{3,2},{4,7},{5,4},{6,5},{7,6},{8,11},{9,8},{10,9... | collective-permute-start | bytes 24584 | tf_op jit(solution)/shard_map/ppermute | solution.py:386
  214.3 2.4 shard_map.162.rec_out
  217.6 3.2 %shard_map.163 = (bf16[128,2048]{1,0:T(8,128)(2,1)}, bf16[128,2048]{1,0:T(8,128)(2,1)}) custom-call(s32[5]{0:T(128)} %stack.23.place, bf16[256,128]{1,0:T(8,128)(2,1)} %shard_map.160.conv_out, bf16[256,128]{1,0:T(8,128)(2,1)} %shard_map.162.rec_out, bf16[16,248,128]{2,1,0:T(8,128)(2,1)} %bitcast.17, bf16[16,200,128]{2,1,0:T(8,128)(2,1)} %copy-done.1), custom_call_target="tpu_custom_call" | custom-call | tf_op jit(solution)/shard_map/pallas_call | solution.py:398
  222.7 2.1 collective-permute-done.9
  226.0 13.7 %all_to_all.27 = bf16[4,32,2048]{2,1,0:T(8,128)(2,1)S(1)} all-to-all(bf16[4,32,2048]{2,1,0:T(8,128)(2,1)S(1)} %bitcast.20), channel_id=1, replica_groups=mesh['sp_0'=4,'sp_1'=4,'sp_2'=4,'sp_3'=2,'tp'=4] {'tp'}, dimensions={0} | all-to-all | bytes 1048576 | tf_op jit(solution)/shard_map/all_to_all | solution.py:289
  (46 shorter events, 25.6 us)
Async XLA Ops:
  37.8 54.1 %copy-start = (bf16[16,32,2048]{2,1,0:T(8,128)(2,1)}, bf16[16,32,2048]{2,1,0:T(8,128)(2,1)S(1)}, u32[]{:S(2)}) copy-start(bf16[16,32,2048]{2,1,0:T(8,128)(2,1)S(1)} %all_to_all.25) | copy-start | bytes 6291460
  37.8 54.1 %collective-permute-start = (bf16[512,2048]{1,0:T(8,128)(2,1)S(1)}, bf16[512,2048]{1,0:T(8,128)(2,1)}, u32[]{:S(2)}, u32[]{:S(2)}) collective-permute-start(bf16[512,2048]{1,0:T(8,128)(2,1)S(1)} %bitcast.18), channel_id=1, source_target_pairs={{0,4},{4,0},{1,5},{5,1},{2,6},{6,2},{3,7},{7,3},{8,12},{12,8},{9,1... | collective-permute-start | bytes 6291464 | tf_op jit(solution)/shard_map/ppermute | solution.py:334
  41.2 9.4 %all-to-all-start.1 = ((bf16[8,64,128]{2,1,0:T(8,128)(2,1)}), bf16[8,64,128]{2,1,0:T(8,128)(2,1)S(1)}, u32[]{:S(2)}, u32[]{:S(2)}) async-start(bf16[8,64,128]{2,1,0:T(8,128)(2,1)} %shard_map.155), calls=%async_computation.1 | async-start | bytes 262144 | tf_op jit(solution)/shard_map/all_to_all | solution.py:289
  50.7 0.7 copy-start.2
  96.4 64.7 %copy-start.6 = (bf16[200,128]{1,0:T(8,128)(2,1)S(1)}, bf16[200,128]{1,0:T(8,128)(2,1)}, u32[]{:S(2)}) copy-start(bf16[200,128]{1,0:T(8,128)(2,1)} %get-tuple-element.32) | copy-start | bytes 153604
  96.4 9.1 %collective-permute-start.1 = (bf16[256,256]{1,0:T(8,128)(2,1)}, bf16[256,256]{1,0:T(8,128)(2,1)S(1)}, u32[]{:S(2)}, u32[]{:S(2)}) collective-permute-start(bf16[256,256]{1,0:T(8,128)(2,1)} %get-tuple-element.22), channel_id=1, source_target_pairs={{0,8},{8,16},{16,24},{24,0},{1,9},{9,17},{17,25},{25,1},{2,10},{10... | collective-permute-start | bytes 393224 | tf_op jit(solution)/shard_map/ppermute | solution.py:350
  99.0 8.6 %collective-permute-start.2 = (bf16[256,256]{1,0:T(8,128)(2,1)}, bf16[256,256]{1,0:T(8,128)(2,1)S(1)}, u32[]{:S(2)}, u32[]{:S(2)}) collective-permute-start(bf16[256,256]{1,0:T(8,128)(2,1)} %get-tuple-element.23), channel_id=1, source_target_pairs={{0,16},{8,24},{16,0},{24,8},{1,17},{9,25},{17,1},{25,9},{2,18},{10... | collective-permute-start | bytes 393224 | tf_op jit(solution)/shard_map/ppermute | solution.py:350
  102.9 7.2 %collective-permute-start.3 = (bf16[256,256]{1,0:T(8,128)(2,1)}, bf16[256,256]{1,0:T(8,128)(2,1)S(1)}, u32[]{:S(2)}, u32[]{:S(2)}) collective-permute-start(bf16[256,256]{1,0:T(8,128)(2,1)} %get-tuple-element.24), channel_id=1, source_target_pairs={{0,24},{8,0},{16,8},{24,16},{1,25},{9,1},{17,9},{25,17},{2,26},{10... | collective-permute-start | bytes 393224 | tf_op jit(solution)/shard_map/ppermute | solution.py:350
  105.5 4.7 %copy-start.3 = (bf16[256,256]{1,0:T(8,128)(2,1)}, bf16[256,256]{1,0:T(8,128)(2,1)S(1)}, u32[]{:S(2)}) copy-start(bf16[256,256]{1,0:T(8,128)(2,1)S(1)} %collective-permute-done.1.p1) | copy-start | bytes 393220
  107.5 2.6 %copy-start.4 = (bf16[256,256]{1,0:T(8,128)(2,1)}, bf16[256,256]{1,0:T(8,128)(2,1)S(1)}, u32[]{:S(2)}) copy-start(bf16[256,256]{1,0:T(8,128)(2,1)S(1)} %collective-permute-done.2.p2) | copy-start | bytes 393220
  110.2 0.6 copy-start.5
  126.9 41.3 %copy-start.12 = (bf16[32,256]{1,0:T(8,128)(2,1)S(1)}, bf16[32,256]{1,0:T(8,128)(2,1)}, u32[]{:S(2)}) copy-start(bf16[32,256]{1,0:T(8,128)(2,1)} %get-tuple-element.26) | copy-start | bytes 49156
  162.1 54.6 %all-to-all-start.3 = ((bf16[16,200,128]{2,1,0:T(8,128)(2,1)}), bf16[16,200,128]{2,1,0:T(8,128)(2,1)S(1)}, u32[]{:S(2)}, u32[]{:S(2)}) async-start(bf16[16,200,128]{2,1,0:T(8,128)(2,1)} %broadcast_in_dim.3), calls=%async_computation.3 | async-start | bytes 1638400 | tf_op jit(solution)/shard_map/all_to_all | solution.py:289
  168.3 24.8 %collective-permute-start.4 = (bf16[32,256]{1,0:T(8,128)(2,1)S(1)}, bf16[32,256]{1,0:T(8,128)(2,1)S(1)}, u32[]{:S(2)}, u32[]{:S(2)}) collective-permute-start(bf16[32,256]{1,0:T(8,128)(2,1)S(1)} %copy-done.12), channel_id=1, source_target_pairs={{0,8},{8,16},{16,24},{24,32},{32,40},{40,48},{48,56},{56,64},{64,7... | collective-permute-start | bytes 49160 | tf_op jit(solution)/shard_map/ppermute | solution.py:376
  193.1 0.6 copy-start.8
  195.9 3.3 %collective-permute-start.5 = (f32[8,256]{1,0:T(8,128)}, f32[8,256]{1,0:T(8,128)S(1)}, u32[]{:S(2)}, u32[]{:S(2)}) collective-permute-start(f32[8,256]{1,0:T(8,128)} %get-tuple-element.28), channel_id=1, source_target_pairs={{0,4},{4,0},{1,5},{5,1},{2,6},{6,2},{3,7},{7,3},{8,12},{12,8},{9,1... | collective-permute-start | bytes 24584 | tf_op jit(solution)/shard_map/ppermute | solution.py:383
  199.9 11.8 %copy-start.7 = (f32[8,256]{1,0:T(8,128)}, f32[8,256]{1,0:T(8,128)S(1)}, u32[]{:S(2)}) copy-start(f32[8,256]{1,0:T(8,128)S(1)} %add.6.s0) | copy-start | bytes 24580
  199.9 9.8 %collective-permute-start.6 = (f32[8,256]{1,0:T(8,128)S(1)}, f32[8,256]{1,0:T(8,128)S(1)}, u32[]{:S(2)}, u32[]{:S(2)}) collective-permute-start(f32[8,256]{1,0:T(8,128)S(1)} %add.6.s0), channel_id=1, source_target_pairs={{0,1},{1,2},{2,3},{3,0},{4,5},{5,6},{6,7},{7,4},{8,9},{9,10},{10,1... | collective-permute-start | bytes 24584 | tf_op jit(solution)/shard_map/ppermute | solution.py:386
  202.1 7.7 %collective-permute-start.7 = (f32[8,256]{1,0:T(8,128)S(1)}, f32[8,256]{1,0:T(8,128)S(1)}, u32[]{:S(2)}, u32[]{:S(2)}) collective-permute-start(f32[8,256]{1,0:T(8,128)S(1)} %add.6.s0), channel_id=1, source_target_pairs={{0,2},{1,3},{2,0},{3,1},{4,6},{5,7},{6,4},{7,5},{8,10},{9,11},{10,... | collective-permute-start | bytes 24584 | tf_op jit(solution)/shard_map/ppermute | solution.py:386
  206.2 5.5 %collective-permute-start.8 = (f32[8,256]{1,0:T(8,128)S(1)}, f32[8,256]{1,0:T(8,128)S(1)}, u32[]{:S(2)}, u32[]{:S(2)}) collective-permute-start(f32[8,256]{1,0:T(8,128)S(1)} %add.6.s0), channel_id=1, source_target_pairs={{0,3},{1,0},{2,1},{3,2},{4,7},{5,4},{6,5},{7,6},{8,11},{9,8},{10,9... | collective-permute-start | bytes 24584 | tf_op jit(solution)/shard_map/ppermute | solution.py:386
  209.8 2.0 copy-start.9
  209.8 1.9 copy-start.10
  216.7 0.9 copy-start.1
  220.8 4.0 %collective-permute-start.9 = (bf16[128,2048]{1,0:T(8,128)(2,1)}, bf16[128,2048]{1,0:T(8,128)(2,1)S(1)}, u32[]{:S(2)}, u32[]{:S(2)}) collective-permute-start(bf16[128,2048]{1,0:T(8,128)(2,1)} %get-tuple-element.34), channel_id=1, source_target_pairs={{0,4},{4,0},{1,5},{5,1},{2,6},{6,2},{3,7},{7,3},{8,12},{12,8},{9,1... | collective-permute-start | bytes 1572872 | tf_op jit(solution)/shard_map/ppermute | solution.py:404
  (1 other events, 0.6 us)

commit v6 on v4

--- a/solution.py
+++ b/solution.py
@@ -18,7 +18,7 @@
 BLOCK = 64
 TAPS = 31
 HALO = 32
-STATE_ROWS = 136
+STATE_ROWS = 40
 HALF = 128
 CHUNK = 16
 COLUMN_ROWS = 24
@@ -111,48 +111,32 @@
         turned = pltpu.roll(packed, CH // 2, 1).reshape(blocks, 8, CH)
         both = jnp.concatenate([packed.reshape(blocks, 8, CH), turned], axis=1)
         weight[at : at + step, CH:] = both.reshape(step, CH).astype(bf16)
-    for k in range(NX):
-        x = lax.rem(place[2] + k, NX)
-        rows = pl.ds(pl.multiple_of(x * HALF, HALF), HALF)
+    for x in range(NX):
+        rows = slice(x * HALF, (x + 1) * HALF)
         for core, tokens in ((c, own), (1 - c, other)):
             to = pl.ds(pl.multiple_of(core * HALF, HALF), HALF)
-            out[k, to] = matmul(tokens[rows], weight[...], ((1,), (0,))).astype(bf16)
-
-
-def source(pieces, place, x, second):
-    slot = lax.rem(place[2] - x + NX, NX)
-    at = slice(CH, 2 * CH) if second else slice(0, CH)
-    value = pieces[0][:, at].astype(f32)
-    for k in range(1, NX):
-        value = jnp.where(slot == k, pieces[k][:, at].astype(f32), value)
-    return value
-
-
-def joined(pieces, place, x):
+            out[x, to] = matmul(tokens[rows], weight[...], ((1,), (0,))).astype(bf16)
+
+
+def joined(pieces, x):
     lane = lax.broadcasted_iota(jnp.int32, (ROWS, CH), 1)
-    return jnp.where(
-        lane < CH // 2, source(pieces, place, x, True), source(pieces, place, x + 1, True)
-    )
-
-
-def local_body(place, p0, p1, p2, p3, margin, jumps, inner, decayed, packed, rest, tail):
+    first, second = (pieces[k, :, CH:].astype(f32) for k in (x, x + 1))
+    return jnp.where(lane < CH // 2, first, second)
+
+
+def local_body(place, pieces, margin, arrived, inner, decayed, packed, rest, tail):
     c = place[3]
-    pieces = (p0, p1, p2, p3)
-    jump = jnp.concatenate(
-        [
-            jumps[k, :1].astype(f32) + jumps[k, 1:2].astype(f32)
-            for k in range(NC)
-        ],
-        axis=1,
-    )
+    at = COLUMN_ROWS + OUT_ROWS
+    rows = [arrived[NC * place[2] + k, at : at + 8].astype(f32) for k in range(NC)]
+    jump = jnp.concatenate([r[:1] + r[1:2] for r in rows], axis=1)
     bound = own_half(margin[...], c)
-    queries = silu(source(pieces, place, 0, False))
-    keys = bound * sigmoid(-joined(pieces, place, 0))
-    inputs = source(pieces, place, 1, False).astype(bf16)
+    queries = silu(pieces[0, :, :CH].astype(f32))
+    keys = bound * sigmoid(-joined(pieces, 0))
+    inputs = pieces[1, :, :CH]
     others = (
-        source(pieces, place, 2, False),
-        joined(pieces, place, 2),
-        source(pieces, place, 3, False),
+        pieces[2, :, :CH].astype(f32),
+        joined(pieces, 2),
+        pieces[3, :, :CH].astype(f32),
     )
     for k, value in enumerate(others):
         rest[:, k * CH : (k + 1) * CH] = value.astype(bf16)
@@ -182,40 +166,50 @@
         decayed[at] = (scaled * jnp.exp(before)).astype(bf16)
         state = state * jnp.exp(final) + matmul(inputs[at], final_keys, ((0,), (0,)))
         before = before + final
-    pack(packed, state, before)
-
-
-def pack(ref, state, decay):
+    high = before.astype(bf16)
+    low = (before - high.astype(f32)).astype(bf16)
+    first = lax.broadcasted_iota(jnp.int32, (8, CH), 0)
+    tail = jnp.where(first == 0, high.astype(f32), jnp.where(first == 1, low.astype(f32), 0.0))
+    for x in range(NX):
+        packed[x, :OWN] = state[x * OWN : (x + 1) * OWN].astype(bf16)
+        packed[x, OWN:] = tail.astype(bf16)
+
+
+def unpacked(block):
+    wide = block.astype(f32)
+    return wide[OWN : OWN + 1] + wide[OWN + 1 : OWN + 2], wide[:OWN]
+
+
+def slab_body(parts, total):
+    state = jnp.zeros((OWN, CH), f32)
+    decay = jnp.zeros((1, CH), f32)
+    for x in range(NX):
+        step, add = unpacked(parts[x])
+        state = state * jnp.exp(step) + add
+        decay = decay + step
     high = decay.astype(bf16).astype(f32)
     low = decay - high
     first = lax.broadcasted_iota(jnp.int32, (8, CH), 0)
-    ref[:CH] = state.astype(bf16)
-    ref[CH:] = jnp.where(first == 0, high, jnp.where(first == 1, low, 0.0)).astype(bf16)
-
-
-def unpacked(block):
-    wide = block.astype(f32)
-    return wide[CH : CH + 1] + wide[CH + 1 : CH + 2], wide[:CH]
-
-
-def total_body(parts, total):
-    state = jnp.zeros((CH, CH), f32)
-    decay = jnp.zeros((1, CH), f32)
-    for k in range(NQ):
-        step, add = unpacked(parts[k])
+    tail = jnp.where(first == 0, high, jnp.where(first == 1, low, 0.0)).astype(bf16)
+    for z in range(NZ):
+        total[z, :OWN] = state.astype(bf16)
+        total[z, OWN:] = tail
+
+
+def prefix_body(place, slabs, parts, starts):
+    mine = NQ * place[0] + place[1]
+    state = jnp.zeros((OWN, CH), f32)
+    for z in range(NZ):
+        step, add = unpacked(slabs[z])
+        state = jnp.where(z < mine, state * jnp.exp(step) + add, state)
+    for x in range(NX):
+        starts[x] = state.astype(bf16)
+        step, add = unpacked(parts[x])
         state = state * jnp.exp(step) + add
-        decay = decay + step
-    for k in range(total.shape[0]):
-        pack(total.at[k], state, decay)
-
-
-def finish_body(place, quads, slabs, chips, inner, decayed, gain, rest, out):
-    state = jnp.zeros((CH, CH), f32)
-    for level, parts in enumerate((quads, slabs, chips)):
-        for k in range(NQ):
-            step, add = unpacked(parts[k])
-            state = jnp.where(k < place[level], state * jnp.exp(step) + add, state)
-    recurrent = inner[...] + matmul(decayed[...], state.astype(bf16), ((1,), (1,)))
+
+
+def finish_body(place, inner, decayed, start, gain, rest, out):
+    recurrent = inner[...] + matmul(decayed[...], start[...], ((1,), (1,)))
     scale = lax.rsqrt(jnp.mean(recurrent * recurrent, axis=1, keepdims=True) + norm_eps)
     gate = silu(rest[:, 2 * CH :].astype(f32))
     out[...] = (recurrent * scale * own_half(gain[...], place[3]) * gate).astype(bf16)
@@ -272,20 +266,8 @@
         out[...] = matmul(both[rows], weight[...], ((1,), (1,))).astype(bf16)
 
 
-def last_body(parts, out):
-    total = parts[0].astype(f32)
-    for y in range(1, NY):
-        total = total + parts[y].astype(f32)
-    out[...] = total.astype(bf16)
-
-
 def exchanged(x, axes):
     return lax.all_to_all(x, axes, split_axis=0, concat_axis=0, tiled=True)
-
-
-def to_everyone(x, axes):
-    copies = jnp.broadcast_to(x, (lax.axis_size(axes), *x.shape))
-    return exchanged(copies, axes)
 
 
 def per_device(
@@ -327,9 +309,8 @@
     own = exchanged(copies, (X, Y)).reshape(NX * HALF, width)
     other = lax.ppermute(own, C, [(0, 1), (1, 0)])
     columns = lax.all_gather(arrived[:, :COLUMN_ROWS], (ZH, ZL), axis=0, tiled=True)
-    out_pieces = to_everyone(arrived[:, COLUMN_ROWS : COLUMN_ROWS + OUT_ROWS], (ZH, ZL))
-    jumps = lax.dynamic_slice_in_dim(
-        arrived[:, COLUMN_ROWS + OUT_ROWS :], NC * lax.axis_index(X), NC, axis=0
+    out_pieces = lax.all_gather(
+        arrived[:, COLUMN_ROWS : COLUMN_ROWS + OUT_ROWS], (ZH, ZL), axis=0
     )
     projected = kernel_call(
         project_body,
@@ -337,11 +318,7 @@
         [SMEM] + [VMEM] * 3,
         [pltpu.VMEM((width, 2 * CH), bf16)],
     )(place, own, other, columns)
-    pieces = [projected[0]]
-    for k in range(1, NX):
-        pieces.append(
-            lax.ppermute(projected[k], X, [(x, (x + k) % NX) for x in range(NX)])
-        )
+    pieces = exchanged(projected, X)
 
     margin = forget_floor_margin.reshape(1, 2 * CH)
     inner, decayed, packed, rest, tail = kernel_call(
@@ -349,23 +326,21 @@
         (
             shape((ROWS, CH), f32),
             shape((ROWS, CH), bf16),
-            shape((STATE_ROWS, CH), bf16),
+            shape((NX, STATE_ROWS, CH), bf16),
             shape((ROWS, 3 * CH), bf16),
             shape((HALO, 2 * CH), bf16),
         ),
-        [SMEM] + [VMEM] * 6,
-    )(place, *pieces, margin, jumps)
-    chips = lax.all_gather(packed, X, axis=0)
-
-    def total_of(parts, copies):
-        return kernel_call(
-            total_body, shape((copies, STATE_ROWS, CH), bf16), [VMEM]
-        )(parts)
-
-    slab_copies = total_of(chips, NQ)
-    slabs = exchanged(slab_copies, ZL)
-    quad_copies = total_of(slabs, NQ)
-    quads = exchanged(quad_copies, ZH)
+        [SMEM] + [VMEM] * 3,
+    )(place, pieces, margin, arrived)
+    parts = exchanged(packed, X)
+    slab_copies = kernel_call(
+        slab_body, shape((NZ, STATE_ROWS, CH), bf16), [VMEM]
+    )(parts)
+    slabs = exchanged(slab_copies, (ZH, ZL))
+    starts = kernel_call(
+        prefix_body, shape((NX, OWN, CH), bf16), [SMEM, VMEM, VMEM]
+    )(place, slabs, parts)
+    start = exchanged(starts, X).reshape(CH, CH)
 
     blocks = NZ * NX
     halo = lax.ppermute(tail, (ZH, ZL, X), [(k, k + 1) for k in range(blocks - 1)])
@@ -376,9 +351,7 @@
         [pltpu.VMEM((HALO + ROWS, CH), f32)],
     )(place, rest, halo, depthwise_filter_taps)
     all_sums = exchanged(sums, (C, Y))
-    conv_out = kernel_call(
-        channel_body, shape((ROWS, CH), bf16), [SMEM, VMEM, VMEM, VMEM, VMEM]
-    )(
+    conv_out = kernel_call(channel_body, shape((ROWS, CH), bf16), [SMEM] + [VMEM] * 4)(
         place,
         convolved,
         all_sums,
@@ -386,8 +359,8 @@
         channel_norm_bias.reshape(1, 2 * CH),
     )
     rec_out = kernel_call(
-        finish_body, shape((ROWS, CH), bf16), [SMEM] + [VMEM] * 7
-    )(place, quads, slabs, chips, inner, decayed, head_norm_gain.reshape(1, 2 * CH), rest)
+        finish_body, shape((ROWS, CH), bf16), [SMEM] + [VMEM] * 5
+    )(place, inner, decayed, start, head_norm_gain.reshape(1, 2 * CH), rest)
 
     mine, theirs = kernel_call(
         output_body,
@@ -398,7 +371,7 @@
     given = lax.ppermute(theirs, C, [(0, 1), (1, 0)])
     pair_sum = (mine.astype(f32) + given.astype(f32)).astype(bf16)
     pieces = exchanged(pair_sum.reshape(NY, OWN, width), Y)
-    return kernel_call(last_body, shape((OWN, width), bf16), [VMEM])(pieces)
+    return pieces.astype(f32).sum(axis=0).astype(bf16)
 
 
 def solution(mesh):

time: 257 us -> 202 us (0.79)
  waiting for transfers between devices: 76.6 us -> 12.4 us
  blocking collectives: 102 us -> 120 us
  starting transfers between devices: 40.4 us -> 25.1 us
  between operations: 0.13 us -> 13.5 us
  local copies, waits for them, and re-layouts: 6.5 us -> 2.53 us
    all_to_all x5 -> x3, waiting for transfers between devices: 68.4 us -> 8.63 us  [exchanged(): return lax.all_to_all(x, axes, split_axis=0, concat_axis=0, tiled=True)]
    all_to_all x2 -> x5, blocking collectives: 46.9 us -> 77 us  [exchanged(): return lax.all_to_all(x, axes, split_axis=0, concat_axis=0, tiled=True)]
    all_gather x1 -> x0, blocking collectives: 13 us -> none  [per_device(): chips = lax.all_gather(packed, X, axis=0)]
    ppermute x3 -> x0, starting transfers between devices: 9.23 us -> none  [per_device(): lax.ppermute(projected[k], X, [(x, (x + k) % NX) for x in range(NX)])]
    all_to_all x5 -> x3, starting transfers between devices: 22.7 us -> 15.9 us  [exchanged(): return lax.all_to_all(x, axes, split_axis=0, concat_axis=0, tiled=True)]
    ppermute x3 -> x0, waiting for transfers between devices: 4.51 us -> none  [per_device(): lax.ppermute(projected[k], X, [(x, (x + k) % NX) for x in range(NX)])]
    pallas_call x5 -> x4, Pallas kernels: 9.24 us -> 7.06 us  [the longest x1 2 us: per_device(): kernel_call(channel_body, shape((ROWS, CH), bf16), [SMEM] + [VMEM] * 4)]
  transfers between devices with their start and end apart: 11 -> 7, of which waited for: 8 -> 5; matrix products, arithmetic and copies ran while one was open for 0% -> 1% of each run, Pallas kernels for 4% -> 9%
where the time goes in v6:
time: 202 us; the launch traced here: 199 us
  blocking collectives  120 us (59%)
  starting transfers between devices  25.1 us (12%)
  Pallas kernels  23.9 us (12%)
  between operations  13.5 us (7%)
  waiting for transfers between devices  12.4 us (6%)
  local copies, waits for them, and re-layouts  2.53 us (1%)
    all_to_all x5, blocking collectives, exchanged(): return lax.all_to_all(x, axes, split_axis=0, concat_axis=0, tiled=True)  77 us
    all_gather x1, blocking collectives, per_device(): lax.all_gather(arrived[:, :COLUMN_ROWS], (ZH, ZL), axis=0, tiled=True)  42.7 us
    all_to_all x3, starting transfers between devices, exchanged(): return lax.all_to_all(x, axes, split_axis=0, concat_axis=0, tiled=True)  15.9 us
    all_to_all x3, waiting for transfers between devices, exchanged(): return lax.all_to_all(x, axes, split_axis=0, concat_axis=0, tiled=True)  8.63 us
    ppermute x1, starting transfers between devices, per_device(): lax.ppermute(tail, (ZH, ZL, X), [(k, k + 1) for k in range(blocks - 1)])  5.33 us
    pallas_call x1, Pallas kernels, per_device(): kernel_call(project_body, shape((NX, ROWS, 2 * CH), bf16), [SMEM] + [VMEM...  4.56 us
  transfers between devices with their start and end apart: 7, of which 5 were waited for; matrix products, arithmetic and copies ran while one was open for 1% of the time, Pallas kernels for 9%

profile of v6, /device:TPU:6, one launch (start us, length us, event | category | flops | bytes accessed | tf_op | source)
XLA Modules:
  0.0 198.9 jit_solution(13382662136353138021)
XLA Ops:
  6.5 2.5 %shard_map.154 = bf16[16,32,2048]{2,1,0:T(8,128)(2,1)} custom-call(bf16[32,2048]{1,0:T(8,128)(2,1)} %tokens.1, f32[1,2048]{1,0:T(1,128)} %bitcast.21), custom_call_target="tpu_custom_call" | custom-call | tf_op jit(solution)/shard_map/pallas_call | solution.py:306
  9.0 33.7 %all_to_all.40 = bf16[16,32,2048]{2,1,0:T(8,128)(2,1)S(1)} all-to-all(bf16[16,32,2048]{2,1,0:T(8,128)(2,1)} %shard_map.154), channel_id=1, replica_groups=mesh['sp_0'=4,'sp_1'=4,'sp_2'=4,'sp_3'=2,'tp'=4] {'sp_2','tp'}, dimensions={0} | all-to-all | bytes 4194304 | tf_op jit(solution)/shard_map/all_to_all | solution.py:270
  42.8 1.9 collective-permute-start
  46.2 9.4 %all_to_all.41.arrived = bf16[8,64,128]{2,1,0:T(8,128)(2,1)S(1)} all-to-all(bf16[8,64,128]{2,1,0:T(8,128)(2,1)} %shard_map.155), channel_id=1, replica_groups=mesh['sp_0'=4,'sp_1'=4,'sp_2'=4,'sp_3'=2,'tp'=4] {'sp_2','sp_3'}, dimensions={0} | all-to-all | bytes 262144 | tf_op jit(solution)/shard_map/all_to_all | solution.py:270
  57.0 42.7 %all_gather.9.columns = bf16[128,24,128]{2,1,0:T(8,128)(2,1)} all-gather(bf16[8,24,128]{2,1,0:T(8,128)(2,1)S(1)} %slice.8), channel_id=1, replica_groups=mesh['sp_0'=4,'sp_1'=4,'sp_2'=4,'sp_3'=2,'tp'=4] {'sp_0','sp_1'}, dimensions={0}, use_global_device_ids=true | all-gather | bytes 835584 | tf_op jit(solution)/shard_map/all_gather | solution.py:311
  99.7 4.6 %shard_map.156 = bf16[4,256,256]{2,1,0:T(8,128)(2,1)} custom-call(s32[5]{0:T(128)} %stack.23.place, bf16[512,2048]{1,0:T(8,128)(2,1)} %bitcast.17, bf16[512,2048]{1,0:T(8,128)(2,1)} %collective-permute-done.other, bf16[128,24,128]{2,1,0:T(8,128)(2,1)} %all_gather.9.columns), custom_call_target="tpu_custom_call" | custom-call | tf_op jit(solution)/shard_map/pallas_call | solution.py:315
  104.2 12.0 %all_to_all.42.pieces = bf16[4,256,256]{2,1,0:T(8,128)(2,1)} all-to-all(bf16[4,256,256]{2,1,0:T(8,128)(2,1)} %shard_map.156), channel_id=1, replica_groups=mesh['sp_0'=4,'sp_1'=4,'sp_2'=4,'sp_3'=2,'tp'=4] {'sp_2'}, dimensions={0} | all-to-all | bytes 1048576 | tf_op jit(solution)/shard_map/all_to_all | solution.py:270
  116.2 3.0 %shard_map.157 = (f32[256,128]{1,0:T(8,128)}, bf16[256,128]{1,0:T(8,128)(2,1)}, bf16[4,40,128]{2,1,0:T(8,128)(2,1)}, bf16[256,384]{1,0:T(8,128)(2,1)}, bf16[32,256]{1,0:T(8,128)(2,1)}) custom-call(s32[5]{0:T(128)} %stack.23.place, bf16[4,256,256]{2,1,0:T(8,128)(2,1)} %all_to_all.42.pieces, f32[1,256]{1,0:T(1,128)} %bitcast.24, bf16[8,64,128]{2,1,0:T(8,128)(2,1)} %copy-done.1), custom_call_target="tpu_custom_call" | custom-call | tf_op jit(solution)/shard_map/pallas_call | solution.py:324
  119.2 9.4 %all_to_all.43.parts = bf16[4,40,128]{2,1,0:T(8,128)(2,1)} all-to-all(bf16[4,40,128]{2,1,0:T(8,128)(2,1)} %get-tuple-element.20), channel_id=1, replica_groups=mesh['sp_0'=4,'sp_1'=4,'sp_2'=4,'sp_3'=2,'tp'=4] {'sp_2'}, dimensions={0} | all-to-all | bytes 81920 | tf_op jit(solution)/shard_map/all_to_all | solution.py:270
  130.1 7.3 %all-to-all-start.5 = ((bf16[16,40,128]{2,1,0:T(8,128)(2,1)}), bf16[16,40,128]{2,1,0:T(8,128)(2,1)S(1)}, u32[]{:S(2)}, u32[]{:S(2)}) async-start(bf16[16,40,128]{2,1,0:T(8,128)(2,1)} %shard_map.160), calls=%async_computation.5 | async-start | bytes 327680 | tf_op jit(solution)/shard_map/all_to_all | solution.py:270
  137.4 5.3 %collective-permute-start.1 = (bf16[32,256]{1,0:T(8,128)(2,1)}, bf16[32,256]{1,0:T(8,128)(2,1)S(1)}, u32[]{:S(2)}, u32[]{:S(2)}) collective-permute-start(bf16[32,256]{1,0:T(8,128)(2,1)} %get-tuple-element.15), channel_id=1, source_target_pairs={{0,8},{8,16},{16,24},{24,32},{32,40},{40,48},{48,56},{56,64},{64,7... | collective-permute-start | bytes 49160 | tf_op jit(solution)/shard_map/ppermute | solution.py:346
  142.8 1.6 collective-permute-done.1.halo
  145.0 2.3 %shard_map.158 = (bf16[256,128]{1,0:T(8,128)(2,1)}, f32[8,8,256]{2,1,0:T(8,128)}) custom-call(s32[5]{0:T(128)} %stack.23.place, bf16[256,384]{1,0:T(8,128)(2,1)} %get-tuple-element.14.rest, bf16[32,256]{1,0:T(8,128)(2,1)} %copy-done.5, f32[31,256]{1,0:T(8,128)} %taps.1), custom_call_target="tpu_custom_call" | custom-call | tf_op jit(solution)/shard_map/pallas_call | solution.py:347
  147.2 3.5 %all-to-all-done.5.slabs = bf16[16,40,128]{2,1,0:T(8,128)(2,1)S(1)} async-done(((bf16[16,40,128]{2,1,0:T(8,128)(2,1)}), bf16[16,40,128]{2,1,0:T(8,128)(2,1)S(1)}, u32[]{:S(2)}, u32[]{:S(2)}) %all-to-all-start.5) | async-done | bytes 163872 | tf_op jit(solution)/shard_map/all_to_all | solution.py:270
  150.8 3.3 %all-to-all-start.3 = ((f32[8,8,256]{2,1,0:T(8,128)}), f32[8,8,256]{2,1,0:T(8,128)S(1)}, u32[]{:S(2)}, u32[]{:S(2)}) async-start(f32[8,8,256]{2,1,0:T(8,128)} %get-tuple-element.17), calls=%async_computation.3 | async-start | bytes 131072 | tf_op jit(solution)/shard_map/all_to_all | solution.py:270
  154.2 1.6 shard_map.161
  155.8 3.7 %all-to-all-done.3.sums = f32[8,8,256]{2,1,0:T(8,128)S(1)} async-done(((f32[8,8,256]{2,1,0:T(8,128)}), f32[8,8,256]{2,1,0:T(8,128)S(1)}, u32[]{:S(2)}, u32[]{:S(2)}) %all-to-all-start.3) | async-done | bytes 65568 | tf_op jit(solution)/shard_map/all_to_all | solution.py:270
  159.5 5.3 %all-to-all-start.6 = ((bf16[4,32,128]{2,1,0:T(8,128)(2,1)}), bf16[4,32,128]{2,1,0:T(8,128)(2,1)S(1)}, u32[]{:S(2)}, u32[]{:S(2)}) async-start(bf16[4,32,128]{2,1,0:T(8,128)(2,1)} %shard_map.161), calls=%async_computation.6 | async-start | bytes 65536 | tf_op jit(solution)/shard_map/all_to_all | solution.py:270
  164.8 2.0 %shard_map.159.conv_out = bf16[256,128]{1,0:T(8,128)(2,1)} custom-call(s32[5]{0:T(128)} %stack.23.place, bf16[256,128]{1,0:T(8,128)(2,1)} %get-tuple-element.16.values, f32[8,8,256]{2,1,0:T(8,128)} %copy-done.3, f32[1,256]{1,0:T(1,128)} %bitcast.25, f32[1,256]{1,0:T(1,128)} %bitcast.26), custom_call_target="tpu_custom_call" | custom-call | tf_op jit(solution)/shard_map/pallas_call | solution.py:354
  168.8 2.0 shard_map.162.rec_out
  170.8 3.0 %shard_map.163 = (bf16[128,2048]{1,0:T(8,128)(2,1)}, bf16[128,2048]{1,0:T(8,128)(2,1)}) custom-call(s32[5]{0:T(128)} %stack.23.place, bf16[256,128]{1,0:T(8,128)(2,1)} %shard_map.159.conv_out, bf16[256,128]{1,0:T(8,128)(2,1)} %shard_map.162.rec_out, bf16[16,8,32,128]{3,2,1,0:T(8,128)(2,1)} %bitcast.19), custom_call_target="tpu_custom_call" | custom-call | tf_op jit(solution)/shard_map/pallas_call | solution.py:365
  173.7 1.9 collective-permute-start.2
  175.6 2.1 %collective-permute-done.2 = bf16[128,2048]{1,0:T(8,128)(2,1)S(1)} collective-permute-done((bf16[128,2048]{1,0:T(8,128)(2,1)}, bf16[128,2048]{1,0:T(8,128)(2,1)S(1)}, u32[]{:S(2)}, u32[]{:S(2)}) %collective-permute-start.2) | collective-permute-done | bytes 524320 | tf_op jit(solution)/shard_map/ppermute | solution.py:371
  178.9 12.5 %all_to_all.44 = bf16[4,32,2048]{2,1,0:T(8,128)(2,1)S(1)} all-to-all(bf16[4,32,2048]{2,1,0:T(8,128)(2,1)S(1)} %bitcast.18), channel_id=1, replica_groups=mesh['sp_0'=4,'sp_1'=4,'sp_2'=4,'sp_3'=2,'tp'=4] {'tp'}, dimensions={0} | all-to-all | bytes 1048576 | tf_op jit(solution)/shard_map/all_to_all | solution.py:270
  (24 shorter events, 8.9 us)
Async XLA Ops:
  6.5 164.2 %all-gather.3.cloned.1.call-start = ((), (), s32[]{:S(2)}) async-start(), calls=%async_computation.8 | async-start | bytes 1114112 | tf_op jit(solution)/shard_map/all_gather | solution.py:312
  42.8 56.9 %copy-start = (bf16[16,32,2048]{2,1,0:T(8,128)(2,1)}, bf16[16,32,2048]{2,1,0:T(8,128)(2,1)S(1)}, u32[]{:S(2)}) copy-start(bf16[16,32,2048]{2,1,0:T(8,128)(2,1)S(1)} %all_to_all.40) | copy-start | bytes 6291460
  42.8 56.9 %collective-permute-start = (bf16[512,2048]{1,0:T(8,128)(2,1)S(1)}, bf16[512,2048]{1,0:T(8,128)(2,1)}, u32[]{:S(2)}, u32[]{:S(2)}) collective-permute-start(bf16[512,2048]{1,0:T(8,128)(2,1)S(1)} %bitcast.16), channel_id=1, source_target_pairs={{0,4},{4,0},{1,5},{5,1},{2,6},{6,2},{3,7},{7,3},{8,12},{12,8},{9,1... | collective-permute-start | bytes 6291464 | tf_op jit(solution)/shard_map/ppermute | solution.py:310
  55.7 48.6 %copy-start.1 = (bf16[8,64,128]{2,1,0:T(8,128)(2,1)}, bf16[8,64,128]{2,1,0:T(8,128)(2,1)S(1)}, u32[]{:S(2)}) copy-start(bf16[8,64,128]{2,1,0:T(8,128)(2,1)S(1)} %all_to_all.41.arrived) | copy-start | bytes 393220
  130.1 20.7 %all-to-all-start.5 = ((bf16[16,40,128]{2,1,0:T(8,128)(2,1)}), bf16[16,40,128]{2,1,0:T(8,128)(2,1)S(1)}, u32[]{:S(2)}, u32[]{:S(2)}) async-start(bf16[16,40,128]{2,1,0:T(8,128)(2,1)} %shard_map.160), calls=%async_computation.5 | async-start | bytes 327680 | tf_op jit(solution)/shard_map/all_to_all | solution.py:270
  137.4 7.0 %collective-permute-start.1 = (bf16[32,256]{1,0:T(8,128)(2,1)}, bf16[32,256]{1,0:T(8,128)(2,1)S(1)}, u32[]{:S(2)}, u32[]{:S(2)}) collective-permute-start(bf16[32,256]{1,0:T(8,128)(2,1)} %get-tuple-element.15), channel_id=1, source_target_pairs={{0,8},{8,16},{16,24},{24,32},{32,40},{40,48},{48,56},{56,64},{64,7... | collective-permute-start | bytes 49160 | tf_op jit(solution)/shard_map/ppermute | solution.py:346
  144.4 0.6 copy-start.5
  150.8 3.4 %copy-start.2 = (bf16[16,40,128]{2,1,0:T(8,128)(2,1)}, bf16[16,40,128]{2,1,0:T(8,128)(2,1)S(1)}, u32[]{:S(2)}) copy-start(bf16[16,40,128]{2,1,0:T(8,128)(2,1)S(1)} %all-to-all-done.5.slabs) | copy-start | bytes 491524
  150.8 8.7 %all-to-all-start.3 = ((f32[8,8,256]{2,1,0:T(8,128)}), f32[8,8,256]{2,1,0:T(8,128)S(1)}, u32[]{:S(2)}, u32[]{:S(2)}) async-start(f32[8,8,256]{2,1,0:T(8,128)} %get-tuple-element.17), calls=%async_computation.3 | async-start | bytes 131072 | tf_op jit(solution)/shard_map/all_to_all | solution.py:270
  159.5 5.3 %copy-start.3 = (f32[8,8,256]{2,1,0:T(8,128)}, f32[8,8,256]{2,1,0:T(8,128)S(1)}, u32[]{:S(2)}) copy-start(f32[8,8,256]{2,1,0:T(8,128)S(1)} %all-to-all-done.3.sums) | copy-start | bytes 196612
  159.5 8.7 %all-to-all-start.6 = ((bf16[4,32,128]{2,1,0:T(8,128)(2,1)}), bf16[4,32,128]{2,1,0:T(8,128)(2,1)S(1)}, u32[]{:S(2)}, u32[]{:S(2)}) async-start(bf16[4,32,128]{2,1,0:T(8,128)(2,1)} %shard_map.161), calls=%async_computation.6 | async-start | bytes 65536 | tf_op jit(solution)/shard_map/all_to_all | solution.py:270
  168.2 0.6 copy-start.4
  173.7 4.0 %collective-permute-start.2 = (bf16[128,2048]{1,0:T(8,128)(2,1)}, bf16[128,2048]{1,0:T(8,128)(2,1)S(1)}, u32[]{:S(2)}, u32[]{:S(2)}) collective-permute-start(bf16[128,2048]{1,0:T(8,128)(2,1)} %get-tuple-element.22), channel_id=1, source_target_pairs={{0,4},{4,0},{1,5},{5,1},{2,6},{6,2},{3,7},{7,3},{8,12},{12,8},{9,1... | collective-permute-start | bytes 1572872 | tf_op jit(solution)/shard_map/ppermute | solution.py:371
Sparse Core Ops, SparseCore 0:
  56.5 73.1 all-gather.2

commit v7 on v6

--- a/solution.py
+++ b/solution.py
@@ -99,8 +99,7 @@
         out[k] = normed
 
 
-def project_body(place, own, other, columns, out, weight):
-    c = place[3]
+def weight_body(own, columns, half, weight):
     blocks = NX * NC
     step = blocks * CHUNK
     for z in range(NZ):
@@ -111,53 +110,87 @@
         turned = pltpu.roll(packed, CH // 2, 1).reshape(blocks, 8, CH)
         both = jnp.concatenate([packed.reshape(blocks, 8, CH), turned], axis=1)
         weight[at : at + step, CH:] = both.reshape(step, CH).astype(bf16)
+    half[...] = matmul(own[...], weight[...], ((1,), (0,))).astype(bf16)
+
+
+def project_body(place, other, half, weight, out):
+    c = place[3]
+    even = lax.rem(place[2], 2) == 0
+    result = matmul(other[...], weight[...], ((1,), (0,))).astype(bf16)
+    lane = lax.broadcasted_iota(jnp.int32, (HALF, CH), 1)
+    keep = (lane < CH // 2) == even
     for x in range(NX):
         rows = slice(x * HALF, (x + 1) * HALF)
-        for core, tokens in ((c, own), (1 - c, other)):
-            to = pl.ds(pl.multiple_of(core * HALF, HALF), HALF)
-            out[x, to] = matmul(tokens[rows], weight[...], ((1,), (0,))).astype(bf16)
+        mine, theirs = half[rows], result[rows]
+        out[x, pl.ds(pl.multiple_of(c * HALF, HALF), HALF)] = mine[:, :CH]
+        out[x, pl.ds(pl.multiple_of((1 - c) * HALF, HALF), HALF)] = theirs[:, :CH]
+        mine, theirs = mine[:, CH:].astype(f32), theirs[:, CH:].astype(f32)
+        early = jnp.where(c == 0, mine, theirs)
+        late = jnp.where(c == 0, theirs, mine)
+        out[x, ROWS:] = jnp.where(keep, early, pltpu.roll(late, CH // 2, 1)).astype(bf16)
 
 
 def joined(pieces, x):
-    lane = lax.broadcasted_iota(jnp.int32, (ROWS, CH), 1)
-    first, second = (pieces[k, :, CH:].astype(f32) for k in (x, x + 1))
-    return jnp.where(lane < CH // 2, first, second)
-
-
-def local_body(place, pieces, margin, arrived, inner, decayed, packed, rest, tail):
-    c = place[3]
+    lane = lax.broadcasted_iota(jnp.int32, (HALF, CH), 1)
+    first, second = (pieces[k, ROWS:].astype(f32) for k in (x, x + 1))
+    early = jnp.where(lane < CH // 2, first, second)
+    late = pltpu.roll(jnp.where(lane < CH // 2, second, first), CH // 2, 1)
+    return jnp.concatenate([early, late], axis=0)
+
+
+def gates_of(pieces, margin, arrived, place):
     at = COLUMN_ROWS + OUT_ROWS
     rows = [arrived[NC * place[2] + k, at : at + 8].astype(f32) for k in range(NC)]
     jump = jnp.concatenate([r[:1] + r[1:2] for r in rows], axis=1)
-    bound = own_half(margin[...], c)
-    queries = silu(pieces[0, :, :CH].astype(f32))
-    keys = bound * sigmoid(-joined(pieces, 0))
-    inputs = pieces[1, :, :CH]
-    others = (
-        pieces[2, :, :CH].astype(f32),
-        joined(pieces, 2),
-        pieces[3, :, :CH].astype(f32),
-    )
-    for k, value in enumerate(others):
-        rest[:, k * CH : (k + 1) * CH] = value.astype(bf16)
-        if k < 2:
-            tail[:, k * CH : (k + 1) * CH] = value[ROWS - HALO :].astype(bf16)
+    keys = own_half(margin[...], place[3]) * sigmoid(-joined(pieces, 0))
     log_forget = jnp.log1p(-keys)
     row = lax.broadcasted_iota(jnp.int32, (BLOCK, BLOCK), 0)
     col = lax.broadcasted_iota(jnp.int32, (BLOCK, BLOCK), 1)
     causal = row >= col
     lower = jnp.where(causal, 1.0, 0.0)
+    running = []
+    for n in range(ROWS // BLOCK):
+        jumps = jump[:, n * BLOCK : (n + 1) * BLOCK]
+        jumped = jnp.sum(jnp.where(causal, jumps, 0.0), axis=1, keepdims=True)
+        part = log_forget[n * BLOCK : (n + 1) * BLOCK]
+        running.append(matmul(lower, part, ((1,), (0,)), HIGH) + jumped)
+    return keys, running, causal
+
+
+def state_body(place, pieces, margin, arrived, packed, tail):
+    keys, running, _ = gates_of(pieces, margin, arrived, place)
+    inputs = pieces[1, :ROWS]
+    state = jnp.zeros((CH, CH), f32)
+    decay = jnp.zeros((1, CH), f32)
+    for n in range(ROWS // BLOCK):
+        at = slice(n * BLOCK, (n + 1) * BLOCK)
+        final = running[n][BLOCK - 1 : BLOCK]
+        final_keys = (keys[at] * jnp.exp(final - running[n])).astype(bf16)
+        state = state * jnp.exp(final) + matmul(inputs[at], final_keys, ((0,), (0,)))
+        decay = decay + final
+    high = decay.astype(bf16).astype(f32)
+    low = decay - high
+    first = lax.broadcasted_iota(jnp.int32, (8, CH), 0)
+    sent = jnp.where(first == 0, high, jnp.where(first == 1, low, 0.0)).astype(bf16)
+    for x in range(NX):
+        packed[x, :OWN] = state[x * OWN : (x + 1) * OWN].astype(bf16)
+        packed[x, OWN:] = sent
+    tail[:, :CH] = pieces[2, ROWS - HALO : ROWS]
+    tail[:, CH:] = joined(pieces, 2)[ROWS - HALO :].astype(bf16)
+
+
+def local_body(place, pieces, margin, arrived, inner, decayed):
+    keys, running, causal = gates_of(pieces, margin, arrived, place)
+    queries = silu(pieces[0, :ROWS].astype(f32))
+    inputs = pieces[1, :ROWS]
     state = jnp.zeros((CH, CH), f32)
     before = jnp.zeros((1, CH), f32)
     for n in range(ROWS // BLOCK):
         at = slice(n * BLOCK, (n + 1) * BLOCK)
-        jumps = jump[:, n * BLOCK : (n + 1) * BLOCK]
-        jumped = jnp.sum(jnp.where(causal, jumps, 0.0), axis=1, keepdims=True)
-        running = matmul(lower, log_forget[at], ((1,), (0,)), HIGH) + jumped
-        final = running[BLOCK - 1 : BLOCK]
-        scaled = queries[at] * jnp.exp(running)
-        scaled_keys = (keys[at] * jnp.exp(-running)).astype(bf16)
-        final_keys = (keys[at] * jnp.exp(final - running)).astype(bf16)
+        final = running[n][BLOCK - 1 : BLOCK]
+        scaled = queries[at] * jnp.exp(running[n])
+        scaled_keys = (keys[at] * jnp.exp(-running[n])).astype(bf16)
+        final_keys = (keys[at] * jnp.exp(final - running[n])).astype(bf16)
         scores = matmul(scaled.astype(bf16), scaled_keys, ((1,), (1,)))
         scores = jnp.where(causal, scores, 0.0).astype(bf16)
         inner[at] = matmul(scores, inputs[at], ((1,), (0,))) + matmul(
@@ -166,13 +199,6 @@
         decayed[at] = (scaled * jnp.exp(before)).astype(bf16)
         state = state * jnp.exp(final) + matmul(inputs[at], final_keys, ((0,), (0,)))
         before = before + final
-    high = before.astype(bf16)
-    low = (before - high.astype(f32)).astype(bf16)
-    first = lax.broadcasted_iota(jnp.int32, (8, CH), 0)
-    tail = jnp.where(first == 0, high.astype(f32), jnp.where(first == 1, low.astype(f32), 0.0))
-    for x in range(NX):
-        packed[x, :OWN] = state[x * OWN : (x + 1) * OWN].astype(bf16)
-        packed[x, OWN:] = tail.astype(bf16)
 
 
 def unpacked(block):
@@ -196,29 +222,33 @@
         total[z, OWN:] = tail
 
 
-def prefix_body(place, slabs, parts, starts):
+def bridge_body(place, slabs, parts, sums, out):
     mine = NQ * place[0] + place[1]
+    own = NY * place[3] + place[4]
     state = jnp.zeros((OWN, CH), f32)
     for z in range(NZ):
         step, add = unpacked(slabs[z])
         state = jnp.where(z < mine, state * jnp.exp(step) + add, state)
+    row = lax.broadcasted_iota(jnp.int32, (8, CH), 0)
+    packed = []
+    for k in range(2):
+        value = sums[:, k * CH : (k + 1) * CH]
+        high = value.astype(bf16).astype(f32)
+        middle = (value - high).astype(bf16).astype(f32)
+        low = value - high - middle
+        packed.append(jnp.where(row < 2, high, jnp.where(row < 4, middle, low)))
+    packed = jnp.concatenate([*packed, jnp.zeros((16, CH), f32)], axis=0)
     for x in range(NX):
-        starts[x] = state.astype(bf16)
+        for k in range(NC * NY):
+            out[x * NC * NY + k] = jnp.where(k == own, state, packed).astype(bf16)
         step, add = unpacked(parts[x])
         state = state * jnp.exp(step) + add
 
 
-def finish_body(place, inner, decayed, start, gain, rest, out):
-    recurrent = inner[...] + matmul(decayed[...], start[...], ((1,), (1,)))
-    scale = lax.rsqrt(jnp.mean(recurrent * recurrent, axis=1, keepdims=True) + norm_eps)
-    gate = silu(rest[:, 2 * CH :].astype(f32))
-    out[...] = (recurrent * scale * own_half(gain[...], place[3]) * gate).astype(bf16)
-
-
-def conv_body(place, rest, halo, taps, out, sums, gated):
+def conv_body(place, pieces, halo, taps, out, sums, gated):
     rim = halo[...].astype(f32)
     gated[:HALO] = rim[:, :CH] * sigmoid(rim[:, CH:])
-    gated[HALO:] = rest[:, :CH].astype(f32) * sigmoid(rest[:, CH : 2 * CH].astype(f32))
+    gated[HALO:] = pieces[2, :ROWS].astype(f32) * sigmoid(joined(pieces, 2))
     own_taps = own_half(taps[...], place[3])
     for n in range(ROWS // BLOCK):
         total = jnp.zeros((BLOCK, CH), f32)
@@ -231,27 +261,10 @@
     first_sum = matmul(ones, values, ((1,), (1,)), HIGH)
     second_sum = matmul(ones, values * values, ((1,), (1,)), HIGH)
     row = lax.broadcasted_iota(jnp.int32, (8, ROWS), 0)
-    both_sums = jnp.where(row == 0, first_sum, second_sum)
-    for k in range(NC * NY):
-        sums[k] = both_sums
-
-
-def channel_body(place, values, sums, gain, bias, out):
-    total = sums[0]
-    for k in range(1, NC * NY):
-        total = total + sums[k]
-    row = lax.broadcasted_iota(jnp.int32, (8, CH), 0)
-    pick_first = jnp.where(row == 0, 1.0 / CONV_CH, 0.0)
-    pick_second = jnp.where(row == 1, 1.0 / CONV_CH, 0.0)
-    mean = matmul(total, pick_first, ((0,), (0,)), HIGH)
-    variance = matmul(total, pick_second, ((0,), (0,)), HIGH) - mean * mean
-    shifted = (values[...].astype(f32) - mean) * lax.rsqrt(variance + layer_eps)
-    out[...] = silu(
-        shifted * own_half(gain[...], place[3]) + own_half(bias[...], place[3])
-    ).astype(bf16)
-
-
-def output_body(place, conv_out, rec_out, pieces, mine, theirs, weight, both):
+    sums[...] = jnp.where(row % 2 == 0, first_sum, second_sum)
+
+
+def order_body(pieces, weight):
     blocks = NX * NC
     step = blocks * CHUNK
     for z in range(NZ):
@@ -259,9 +272,34 @@
         piece = pieces[z]
         weight[at : at + step, :CH] = piece[:, :CHUNK].reshape(step, CH)
         weight[at : at + step, CH:] = piece[:, CHUNK:].reshape(step, CH)
-    both[:, :CH] = conv_out[...]
-    both[:, CH:] = rec_out[...]
-    for core, out in ((place[3], mine), (1 - place[3], theirs)):
+
+
+def tail_body(
+    place, joint, sums, values, gain, bias, inner, decayed, head_gain, pieces, weight, mine, theirs, both
+):
+    c = place[3]
+    group = NC * NY
+    own = NY * c + place[4]
+    total = jnp.zeros((8, ROWS), f32)
+    for k in range(group):
+        piece = joint[group * place[2] + k].astype(f32)
+        part = jnp.concatenate([piece[:8], piece[8:16]], axis=1)
+        total = total + jnp.where(k == own, 0.0, part)
+    row = lax.broadcasted_iota(jnp.int32, (8, ROWS), 0)
+    total = total + jnp.where(row < 2, sums[...], 0.0)
+    row = lax.broadcasted_iota(jnp.int32, (8, CH), 0)
+    pick_first = jnp.where((row < 6) & (row % 2 == 0), 1.0 / CONV_CH, 0.0)
+    pick_second = jnp.where((row < 6) & (row % 2 == 1), 1.0 / CONV_CH, 0.0)
+    mean = matmul(total, pick_first, ((0,), (0,)), HIGH)
+    variance = matmul(total, pick_second, ((0,), (0,)), HIGH) - mean * mean
+    shifted = (values[...].astype(f32) - mean) * lax.rsqrt(variance + layer_eps)
+    both[:, :CH] = silu(shifted * own_half(gain[...], c) + own_half(bias[...], c)).astype(bf16)
+    start = jnp.concatenate([joint[group * x + own] for x in range(NX)], axis=0)
+    recurrent = inner[...] + matmul(decayed[...], start, ((1,), (1,)))
+    scale = lax.rsqrt(jnp.mean(recurrent * recurrent, axis=1, keepdims=True) + norm_eps)
+    gate = silu(pieces[3, :ROWS].astype(f32))
+    both[:, CH:] = (recurrent * scale * own_half(head_gain[...], c) * gate).astype(bf16)
+    for core, out in ((c, mine), (1 - c, theirs)):
         rows = pl.ds(pl.multiple_of(core * HALF, HALF), HALF)
         out[...] = matmul(both[rows], weight[...], ((1,), (1,))).astype(bf16)
 
@@ -312,24 +350,25 @@
     out_pieces = lax.all_gather(
         arrived[:, COLUMN_ROWS : COLUMN_ROWS + OUT_ROWS], (ZH, ZL), axis=0
     )
+    half, weight = kernel_call(
+        weight_body,
+        (shape((NX * HALF, 2 * CH), bf16), shape((width, 2 * CH), bf16)),
+        [VMEM] * 2,
+    )(own, columns)
     projected = kernel_call(
-        project_body,
-        shape((NX, ROWS, 2 * CH), bf16),
+        project_body, shape((NX, ROWS + HALF, CH), bf16), [SMEM] + [VMEM] * 3
+    )(place, other, half, weight)
+    pieces = exchanged(projected, X)
+
+    margin = forget_floor_margin.reshape(1, 2 * CH)
+    packed, tail = kernel_call(
+        state_body,
+        (shape((NX, STATE_ROWS, CH), bf16), shape((HALO, 2 * CH), bf16)),
         [SMEM] + [VMEM] * 3,
-        [pltpu.VMEM((width, 2 * CH), bf16)],
-    )(place, own, other, columns)
-    pieces = exchanged(projected, X)
-
-    margin = forget_floor_margin.reshape(1, 2 * CH)
-    inner, decayed, packed, rest, tail = kernel_call(
+    )(place, pieces, margin, arrived)
+    inner, decayed = kernel_call(
         local_body,
-        (
-            shape((ROWS, CH), f32),
-            shape((ROWS, CH), bf16),
-            shape((NX, STATE_ROWS, CH), bf16),
-            shape((ROWS, 3 * CH), bf16),
-            shape((HALO, 2 * CH), bf16),
-        ),
+        (shape((ROWS, CH), f32), shape((ROWS, CH), bf16)),
         [SMEM] + [VMEM] * 3,
     )(place, pieces, margin, arrived)
     parts = exchanged(packed, X)
@@ -337,37 +376,39 @@
         slab_body, shape((NZ, STATE_ROWS, CH), bf16), [VMEM]
     )(parts)
     slabs = exchanged(slab_copies, (ZH, ZL))
-    starts = kernel_call(
-        prefix_body, shape((NX, OWN, CH), bf16), [SMEM, VMEM, VMEM]
-    )(place, slabs, parts)
-    start = exchanged(starts, X).reshape(CH, CH)
-
     blocks = NZ * NX
     halo = lax.ppermute(tail, (ZH, ZL, X), [(k, k + 1) for k in range(blocks - 1)])
     convolved, sums = kernel_call(
         conv_body,
-        (shape((ROWS, CH), bf16), shape((NC * NY, 8, ROWS), f32)),
+        (shape((ROWS, CH), bf16), shape((8, ROWS), f32)),
         [SMEM, VMEM, VMEM, VMEM],
         [pltpu.VMEM((HALO + ROWS, CH), f32)],
-    )(place, rest, halo, depthwise_filter_taps)
-    all_sums = exchanged(sums, (C, Y))
-    conv_out = kernel_call(channel_body, shape((ROWS, CH), bf16), [SMEM] + [VMEM] * 4)(
+    )(place, pieces, halo, depthwise_filter_taps)
+    bridge = kernel_call(
+        bridge_body, shape((NX * NC * NY, OWN, CH), bf16), [SMEM] + [VMEM] * 3
+    )(place, slabs, parts, sums)
+    joint = exchanged(bridge, (X, C, Y))
+    out_weight = kernel_call(order_body, shape((width, 2 * CH), bf16), [VMEM])(
+        out_pieces
+    )
+    mine, theirs = kernel_call(
+        tail_body,
+        (shape((HALF, width), bf16), shape((HALF, width), bf16)),
+        [SMEM] + [VMEM] * 10,
+        [pltpu.VMEM((ROWS, 2 * CH), bf16)],
+    )(
         place,
+        joint,
+        sums,
         convolved,
-        all_sums,
         channel_norm_gain.reshape(1, 2 * CH),
         channel_norm_bias.reshape(1, 2 * CH),
-    )
-    rec_out = kernel_call(
-        finish_body, shape((ROWS, CH), bf16), [SMEM] + [VMEM] * 5
-    )(place, inner, decayed, start, head_norm_gain.reshape(1, 2 * CH), rest)
-
-    mine, theirs = kernel_call(
-        output_body,
-        (shape((HALF, width), bf16), shape((HALF, width), bf16)),
-        [SMEM] + [VMEM] * 3,
-        [pltpu.VMEM((width, 2 * CH), bf16), pltpu.VMEM((ROWS, 2 * CH), bf16)],
-    )(place, conv_out, rec_out, out_pieces)
+        inner,
+        decayed,
+        head_norm_gain.reshape(1, 2 * CH),
+        pieces,
+        out_weight,
+    )
     given = lax.ppermute(theirs, C, [(0, 1), (1, 0)])
     pair_sum = (mine.astype(f32) + given.astype(f32)).astype(bf16)
     pieces = exchanged(pair_sum.reshape(NY, OWN, width), Y)

time: 202 us -> 200 us (0.990)
  Pallas kernels: 23.9 us -> 27.2 us
  waiting for transfers between devices: 12.4 us -> 9.38 us
  starting transfers between devices: 25.1 us -> 22.8 us
    pallas_call x7 -> x8, Pallas kernels: 18.4 us -> 21.7 us  [the longest x1 3.76 us: per_device(): kernel_call(tail_body, (shape((HALF, width), bf16), shape((HALF, width),...]
    all_to_all x3 -> x2, waiting for transfers between devices: 8.63 us -> 5.73 us  [exchanged(): return lax.all_to_all(x, axes, split_axis=0, concat_axis=0, tiled=True)]
    all_to_all x3 -> x2, starting transfers between devices: 15.9 us -> 13.5 us  [exchanged(): return lax.all_to_all(x, axes, split_axis=0, concat_axis=0, tiled=True)]
  transfers between devices with their start and end apart: 7 -> 6, of which waited for: 5 -> 4; matrix products, arithmetic and copies ran while one was open for 1% -> 1% of each run, Pallas kernels for 9% -> 11%
where the time goes in v7:
time: 200 us; the launch traced here: 197 us
  blocking collectives  119 us (60%)
  Pallas kernels  27.2 us (14%)
  starting transfers between devices  22.8 us (11%)
  between operations  13.5 us (7%)
  waiting for transfers between devices  9.38 us (5%)
  local copies, waits for them, and re-layouts  3.23 us (2%)
    all_to_all x5, blocking collectives, exchanged(): return lax.all_to_all(x, axes, split_axis=0, concat_axis=0, tiled=True)  76.2 us
    all_gather x1, blocking collectives, per_device(): lax.all_gather(arrived[:, :COLUMN_ROWS], (ZH, ZL), axis=0, tiled=True)  42.8 us
    all_to_all x2, starting transfers between devices, exchanged(): return lax.all_to_all(x, axes, split_axis=0, concat_axis=0, tiled=True)  13.5 us
    all_to_all x2, waiting for transfers between devices, exchanged(): return lax.all_to_all(x, axes, split_axis=0, concat_axis=0, tiled=True)  5.73 us
    ppermute x1, starting transfers between devices, per_device(): lax.ppermute(tail, (ZH, ZL, X), [(k, k + 1) for k in range(blocks - 1)])  5.33 us
  transfers between devices with their start and end apart: 6, of which 4 were waited for; matrix products, arithmetic and copies ran while one was open for 1% of the time, Pallas kernels for 11%

profile of v7, /device:TPU:6, one launch (start us, length us, event | category | flops | bytes accessed | tf_op | source)
XLA Modules:
  0.0 196.9 jit_solution(8537881348491399705)
XLA Ops:
  6.5 2.5 %shard_map.154 = bf16[16,32,2048]{2,1,0:T(8,128)(2,1)} custom-call(bf16[32,2048]{1,0:T(8,128)(2,1)} %tokens.1, f32[1,2048]{1,0:T(1,128)} %bitcast.19), custom_call_target="tpu_custom_call" | custom-call | tf_op jit(solution)/shard_map/pallas_call | solution.py:344
  9.0 33.7 %all_to_all.35 = bf16[16,32,2048]{2,1,0:T(8,128)(2,1)S(1)} all-to-all(bf16[16,32,2048]{2,1,0:T(8,128)(2,1)} %shard_map.154), channel_id=1, replica_groups=mesh['sp_0'=4,'sp_1'=4,'sp_2'=4,'sp_3'=2,'tp'=4] {'sp_2','tp'}, dimensions={0} | all-to-all | bytes 4194304 | tf_op jit(solution)/shard_map/all_to_all | solution.py:308
  42.8 1.9 collective-permute-start
  46.2 9.4 %all_to_all.36.arrived = bf16[8,64,128]{2,1,0:T(8,128)(2,1)S(1)} all-to-all(bf16[8,64,128]{2,1,0:T(8,128)(2,1)} %shard_map.155), channel_id=1, replica_groups=mesh['sp_0'=4,'sp_1'=4,'sp_2'=4,'sp_3'=2,'tp'=4] {'sp_2','sp_3'}, dimensions={0} | all-to-all | bytes 262144 | tf_op jit(solution)/shard_map/all_to_all | solution.py:308
  57.0 42.8 %all_gather.9.columns = bf16[128,24,128]{2,1,0:T(8,128)(2,1)} all-gather(bf16[8,24,128]{2,1,0:T(8,128)(2,1)S(1)} %slice.8), channel_id=1, replica_groups=mesh['sp_0'=4,'sp_1'=4,'sp_2'=4,'sp_3'=2,'tp'=4] {'sp_0','sp_1'}, dimensions={0}, use_global_device_ids=true | all-gather | bytes 835584 | tf_op jit(solution)/shard_map/all_gather | solution.py:349
  99.7 3.3 %shard_map.156 = (bf16[512,256]{1,0:T(8,128)(2,1)}, bf16[2048,256]{1,0:T(8,128)(2,1)}) custom-call(bf16[512,2048]{1,0:T(8,128)(2,1)} %bitcast.16, bf16[128,24,128]{2,1,0:T(8,128)(2,1)} %all_gather.9.columns), custom_call_target="tpu_custom_call" | custom-call | tf_op jit(solution)/shard_map/pallas_call | solution.py:353
  103.1 3.5 %shard_map.157 = bf16[4,384,128]{2,1,0:T(8,128)(2,1)} custom-call(s32[5]{0:T(128)} %stack.23.place, bf16[512,2048]{1,0:T(8,128)(2,1)} %collective-permute-done.other, bf16[512,256]{1,0:T(8,128)(2,1)} %get-tuple-element.15.half, bf16[2048,256]{1,0:T(8,128)(2,1)} %get-tuple-element.16.weight), custom_call_target="tpu_custom_call" | custom-call | tf_op jit(solution)/shard_map/pallas_call | solution.py:358
  106.6 11.2 %all_to_all.37.pieces = bf16[4,384,128]{2,1,0:T(8,128)(2,1)} all-to-all(bf16[4,384,128]{2,1,0:T(8,128)(2,1)} %shard_map.157), channel_id=1, replica_groups=mesh['sp_0'=4,'sp_1'=4,'sp_2'=4,'sp_3'=2,'tp'=4] {'sp_2'}, dimensions={0} | all-to-all | bytes 786432 | tf_op jit(solution)/shard_map/all_to_all | solution.py:308
  117.8 2.1 %shard_map.158 = (bf16[4,40,128]{2,1,0:T(8,128)(2,1)}, bf16[32,256]{1,0:T(8,128)(2,1)}) custom-call(s32[5]{0:T(128)} %stack.23.place, bf16[4,384,128]{2,1,0:T(8,128)(2,1)} %all_to_all.37.pieces, f32[1,256]{1,0:T(1,128)} %bitcast.22, bf16[8,64,128]{2,1,0:T(8,128)(2,1)} %copy-done.1), custom_call_target="tpu_custom_call" | custom-call | tf_op jit(solution)/shard_map/pallas_call | solution.py:364
  119.9 9.4 %all_to_all.38.parts = bf16[4,40,128]{2,1,0:T(8,128)(2,1)} all-to-all(bf16[4,40,128]{2,1,0:T(8,128)(2,1)} %get-tuple-element.17), channel_id=1, replica_groups=mesh['sp_0'=4,'sp_1'=4,'sp_2'=4,'sp_3'=2,'tp'=4] {'sp_2'}, dimensions={0} | all-to-all | bytes 81920 | tf_op jit(solution)/shard_map/all_to_all | solution.py:308
  130.8 7.2 %all-to-all-start.4 = ((bf16[16,40,128]{2,1,0:T(8,128)(2,1)}), bf16[16,40,128]{2,1,0:T(8,128)(2,1)S(1)}, u32[]{:S(2)}, u32[]{:S(2)}) async-start(bf16[16,40,128]{2,1,0:T(8,128)(2,1)} %shard_map.159), calls=%async_computation.4 | async-start | bytes 327680 | tf_op jit(solution)/shard_map/all_to_all | solution.py:308
  138.1 5.3 %collective-permute-start.1 = (bf16[32,256]{1,0:T(8,128)(2,1)}, bf16[32,256]{1,0:T(8,128)(2,1)S(1)}, u32[]{:S(2)}, u32[]{:S(2)}) collective-permute-start(bf16[32,256]{1,0:T(8,128)(2,1)} %get-tuple-element.18), channel_id=1, source_target_pairs={{0,8},{8,16},{16,24},{24,32},{32,40},{40,48},{48,56},{56,64},{64,7... | collective-permute-start | bytes 49160 | tf_op jit(solution)/shard_map/ppermute | solution.py:380
  143.4 1.6 collective-permute-done.1.halo
  145.6 2.3 %shard_map.160 = (bf16[256,128]{1,0:T(8,128)(2,1)}, f32[8,256]{1,0:T(8,128)}) custom-call(s32[5]{0:T(128)} %stack.23.place, bf16[4,384,128]{2,1,0:T(8,128)(2,1)} %all_to_all.37.pieces, bf16[32,256]{1,0:T(8,128)(2,1)} %copy-done.4, f32[31,256]{1,0:T(8,128)} %taps.1), custom_call_target="tpu_custom_call" | custom-call | tf_op jit(solution)/shard_map/pallas_call | solution.py:381
  148.0 3.5 %all-to-all-done.4.slabs = bf16[16,40,128]{2,1,0:T(8,128)(2,1)S(1)} async-done(((bf16[16,40,128]{2,1,0:T(8,128)(2,1)}), bf16[16,40,128]{2,1,0:T(8,128)(2,1)S(1)}, u32[]{:S(2)}, u32[]{:S(2)}) %all-to-all-start.4) | async-done | bytes 163872 | tf_op jit(solution)/shard_map/all_to_all | solution.py:308
  152.1 1.8 shard_map.161
  153.8 6.3 %all-to-all-start.5 = ((bf16[32,32,128]{2,1,0:T(8,128)(2,1)}), bf16[32,32,128]{2,1,0:T(8,128)(2,1)S(1)}, u32[]{:S(2)}, u32[]{:S(2)}) async-start(bf16[32,32,128]{2,1,0:T(8,128)(2,1)} %shard_map.161), calls=%async_computation.5 | async-start | bytes 524288 | tf_op jit(solution)/shard_map/all_to_all | solution.py:308
  160.2 2.3 %shard_map.163.weight = bf16[2048,256]{1,0:T(8,128)(2,1)} custom-call(bf16[16,8,32,128]{3,2,1,0:T(8,128)(2,1)} %bitcast.18), custom_call_target="tpu_custom_call" | custom-call | tf_op jit(solution)/shard_map/pallas_call | solution.py:391
  162.5 2.5 %shard_map.162 = (f32[256,128]{1,0:T(8,128)}, bf16[256,128]{1,0:T(8,128)(2,1)}) custom-call(s32[5]{0:T(128)} %stack.23.place, bf16[4,384,128]{2,1,0:T(8,128)(2,1)} %all_to_all.37.pieces, f32[1,256]{1,0:T(1,128)} %bitcast.23, bf16[8,64,128]{2,1,0:T(8,128)(2,1)} %copy-done.1), custom_call_target="tpu_custom_call" | custom-call | tf_op jit(solution)/shard_map/pallas_call | solution.py:369
  165.0 2.3 %all-to-all-done.5.joint = bf16[32,32,128]{2,1,0:T(8,128)(2,1)S(1)} async-done(((bf16[32,32,128]{2,1,0:T(8,128)(2,1)}), bf16[32,32,128]{2,1,0:T(8,128)(2,1)S(1)}, u32[]{:S(2)}, u32[]{:S(2)}) %all-to-all-start.5) | async-done | bytes 262176 | tf_op jit(solution)/shard_map/all_to_all | solution.py:308
  168.0 3.8 %shard_map.164 = (bf16[128,2048]{1,0:T(8,128)(2,1)}, bf16[128,2048]{1,0:T(8,128)(2,1)}) custom-call(s32[5]{0:T(128)} %stack.23.place, bf16[32,32,128]{2,1,0:T(8,128)(2,1)} %copy-done.2, f32[8,256]{1,0:T(8,128)} %get-tuple-element.19.sums, bf16[256,128]{1,0:T(8,128)(2,1)} %get-tuple-element.20.values, f32[1,256]{1,0:T(1,128)} %bitcast.24, f32[1,256]{1,0:T(1,128)} %bitcast.25, ...), custom_call_target="tpu_custom_call" | custom-call | tf_op jit(solution)/shard_map/pallas_call | solution.py:394
  171.7 2.0 %collective-permute-start.2 = (bf16[128,2048]{1,0:T(8,128)(2,1)}, bf16[128,2048]{1,0:T(8,128)(2,1)S(1)}, u32[]{:S(2)}, u32[]{:S(2)}) collective-permute-start(bf16[128,2048]{1,0:T(8,128)(2,1)} %get-tuple-element.24), channel_id=1, source_target_pairs={{0,4},{4,0},{1,5},{5,1},{2,6},{6,2},{3,7},{7,3},{8,12},{12,8},{9,1... | collective-permute-start | bytes 1572872 | tf_op jit(solution)/shard_map/ppermute | solution.py:412
  173.8 2.0 %collective-permute-done.2 = bf16[128,2048]{1,0:T(8,128)(2,1)S(1)} collective-permute-done((bf16[128,2048]{1,0:T(8,128)(2,1)}, bf16[128,2048]{1,0:T(8,128)(2,1)S(1)}, u32[]{:S(2)}, u32[]{:S(2)}) %collective-permute-start.2) | collective-permute-done | bytes 524320 | tf_op jit(solution)/shard_map/ppermute | solution.py:412
  176.9 12.5 %all_to_all.39 = bf16[4,32,2048]{2,1,0:T(8,128)(2,1)S(1)} all-to-all(bf16[4,32,2048]{2,1,0:T(8,128)(2,1)S(1)} %bitcast.17), channel_id=1, replica_groups=mesh['sp_0'=4,'sp_1'=4,'sp_2'=4,'sp_3'=2,'tp'=4] {'tp'}, dimensions={0} | all-to-all | bytes 1048576 | tf_op jit(solution)/shard_map/all_to_all | solution.py:308
  (21 shorter events, 8.2 us)
Async XLA Ops:
  6.5 153.6 %all-gather.3.cloned.1.call-start = ((), (), s32[]{:S(2)}) async-start(), calls=%async_computation.7 | async-start | bytes 1114112 | tf_op jit(solution)/shard_map/all_gather | solution.py:350
  42.8 57.0 %copy-start = (bf16[16,32,2048]{2,1,0:T(8,128)(2,1)}, bf16[16,32,2048]{2,1,0:T(8,128)(2,1)S(1)}, u32[]{:S(2)}) copy-start(bf16[16,32,2048]{2,1,0:T(8,128)(2,1)S(1)} %all_to_all.35) | copy-start | bytes 6291460
  42.8 60.3 %collective-permute-start = (bf16[512,2048]{1,0:T(8,128)(2,1)S(1)}, bf16[512,2048]{1,0:T(8,128)(2,1)}, u32[]{:S(2)}, u32[]{:S(2)}) collective-permute-start(bf16[512,2048]{1,0:T(8,128)(2,1)S(1)} %bitcast.15), channel_id=1, source_target_pairs={{0,4},{4,0},{1,5},{5,1},{2,6},{6,2},{3,7},{7,3},{8,12},{12,8},{9,1... | collective-permute-start | bytes 6291464 | tf_op jit(solution)/shard_map/ppermute | solution.py:348
  55.7 50.9 %copy-start.1 = (bf16[8,64,128]{2,1,0:T(8,128)(2,1)}, bf16[8,64,128]{2,1,0:T(8,128)(2,1)S(1)}, u32[]{:S(2)}) copy-start(bf16[8,64,128]{2,1,0:T(8,128)(2,1)S(1)} %all_to_all.36.arrived) | copy-start | bytes 393220
  130.8 20.6 %all-to-all-start.4 = ((bf16[16,40,128]{2,1,0:T(8,128)(2,1)}), bf16[16,40,128]{2,1,0:T(8,128)(2,1)S(1)}, u32[]{:S(2)}, u32[]{:S(2)}) async-start(bf16[16,40,128]{2,1,0:T(8,128)(2,1)} %shard_map.159), calls=%async_computation.4 | async-start | bytes 327680 | tf_op jit(solution)/shard_map/all_to_all | solution.py:308
  138.1 7.0 %collective-permute-start.1 = (bf16[32,256]{1,0:T(8,128)(2,1)}, bf16[32,256]{1,0:T(8,128)(2,1)S(1)}, u32[]{:S(2)}, u32[]{:S(2)}) collective-permute-start(bf16[32,256]{1,0:T(8,128)(2,1)} %get-tuple-element.18), channel_id=1, source_target_pairs={{0,8},{8,16},{16,24},{24,32},{32,40},{40,48},{48,56},{56,64},{64,7... | collective-permute-start | bytes 49160 | tf_op jit(solution)/shard_map/ppermute | solution.py:380
  145.0 0.6 copy-start.4
  151.4 0.7 copy-start.3
  153.8 13.4 %all-to-all-start.5 = ((bf16[32,32,128]{2,1,0:T(8,128)(2,1)}), bf16[32,32,128]{2,1,0:T(8,128)(2,1)S(1)}, u32[]{:S(2)}, u32[]{:S(2)}) async-start(bf16[32,32,128]{2,1,0:T(8,128)(2,1)} %shard_map.161), calls=%async_computation.5 | async-start | bytes 524288 | tf_op jit(solution)/shard_map/all_to_all | solution.py:308
  167.3 0.7 copy-start.2
  171.7 4.0 %collective-permute-start.2 = (bf16[128,2048]{1,0:T(8,128)(2,1)}, bf16[128,2048]{1,0:T(8,128)(2,1)S(1)}, u32[]{:S(2)}, u32[]{:S(2)}) collective-permute-start(bf16[128,2048]{1,0:T(8,128)(2,1)} %get-tuple-element.24), channel_id=1, source_target_pairs={{0,4},{4,0},{1,5},{5,1},{2,6},{6,2},{3,7},{7,3},{8,12},{12,8},{9,1... | collective-permute-start | bytes 1572872 | tf_op jit(solution)/shard_map/ppermute | solution.py:412
Sparse Core Ops, SparseCore 0:
  56.5 73.1 all-gather.2

commit v8 on v7

--- a/solution.py
+++ b/solution.py
@@ -19,6 +19,7 @@
 TAPS = 31
 HALO = 32
 STATE_ROWS = 40
+LIMIT = 16 * 2**20
 HALF = 128
 CHUNK = 16
 COLUMN_ROWS = 24
@@ -34,14 +35,24 @@
 SMEM = pl.BlockSpec(memory_space=pltpu.SMEM)
 
 
-def kernel_call(body, out, specs, scratch=()):
-    return pl.pallas_call(
+def in_vmem(value, spec):
+    if spec is SMEM or not isinstance(value, jax.Array):
+        return value
+    return pltpu.with_memory_space_constraint(value, pltpu.VMEM)
+
+
+def kernel_call(body, out, specs, scratch=(), near=True):
+    call = pl.pallas_call(
         body,
-        out_shape=out,
+        out_shape=jax.tree.map(lambda o: pltpu.VMEM(o.shape, o.dtype), out) if near else out,
         in_specs=specs,
         out_specs=jax.tree.map(lambda _: VMEM, out),
         scratch_shapes=scratch,
-    )
+        compiler_params=pltpu.CompilerParams(vmem_limit_bytes=LIMIT if near else None),
+    )
+    if not near:
+        return call
+    return lambda *args: call(*[in_vmem(a, s) for a, s in zip(args, specs)])
 
 
 def shape(dims, dtype):
@@ -329,7 +340,9 @@
     place = jnp.stack([lax.axis_index(a) for a in SP_TP]).astype(jnp.int32)
     width = tokens.shape[1]
 
-    payload = kernel_call(pack_body, shape((NX * NC, SENT_ROWS, CH), bf16), [VMEM] * 9)(
+    payload = kernel_call(
+        pack_body, shape((NX * NC, SENT_ROWS, CH), bf16), [VMEM] * 9, near=False
+    )(
         query_projection_weight,
         forget_gate_weight,
         recurrence_value_weight,
@@ -342,7 +355,7 @@
     )
     arrived = exchanged(payload, (X, C))
     copies = kernel_call(
-        norm_body, shape((NX * NY, OWN, width), bf16), [VMEM, VMEM]
+        norm_body, shape((NX * NY, OWN, width), bf16), [VMEM, VMEM], near=False
     )(tokens, input_norm_gain.reshape(1, width))
     own = exchanged(copies, (X, Y)).reshape(NX * HALF, width)
     other = lax.ppermute(own, C, [(0, 1), (1, 0)])

time: 200 us -> 183 us (0.915)
  Pallas kernels: 27.2 us -> 14.8 us
  blocking collectives: 119 us -> 115 us
  waiting for transfers between devices: 9.38 us -> 12.9 us
    pallas_call x11, Pallas kernels: 27.2 us -> 14.8 us  [the longest x9 10.8 us: kernel_call(): return lambda *args: call(*[in_vmem(a, s) for a, s in zip(args, specs)])]
    all_to_all x2, waiting for transfers between devices: 5.73 us -> 9.64 us  [exchanged(): return lax.all_to_all(x, axes, split_axis=0, concat_axis=0, tiled=True)]
    all_to_all x5, blocking collectives: 76.2 us -> 73.3 us  [exchanged(): return lax.all_to_all(x, axes, split_axis=0, concat_axis=0, tiled=True)]
  transfers between devices with their start and end apart: 6 -> 6, of which waited for: 4 -> 4; matrix products, arithmetic and copies ran while one was open for 1% -> 0% of each run, Pallas kernels for 11% -> 6%
where the time goes in v8:
time: 183 us; the launch traced here: 181 us
  blocking collectives  115 us (63%)
  starting transfers between devices  21.1 us (12%)
  Pallas kernels  14.8 us (8%)
  between operations  13.5 us (7%)
  waiting for transfers between devices  12.9 us (7%)
  local copies, waits for them, and re-layouts  1.97 us (1%)
    all_to_all x5, blocking collectives, exchanged(): return lax.all_to_all(x, axes, split_axis=0, concat_axis=0, tiled=True)  73.3 us
    all_gather x1, blocking collectives, per_device(): lax.all_gather(arrived[:, :COLUMN_ROWS], (ZH, ZL), axis=0, tiled=True)  42.1 us
    all_to_all x2, starting transfers between devices, exchanged(): return lax.all_to_all(x, axes, split_axis=0, concat_axis=0, tiled=True)  11.7 us
    pallas_call x9, Pallas kernels, kernel_call(): return lambda *args: call(*[in_vmem(a, s) for a, s in zip(args, specs)])  10.8 us
    all_to_all x2, waiting for transfers between devices, exchanged(): return lax.all_to_all(x, axes, split_axis=0, concat_axis=0, tiled=True)  9.64 us
    ppermute x1, starting transfers between devices, per_device(): lax.ppermute(tail, (ZH, ZL, X), [(k, k + 1) for k in range(blocks - 1)])  5.47 us
  transfers between devices with their start and end apart: 6, of which 4 were waited for; matrix products, arithmetic and copies ran while one was open for 0% of the time, Pallas kernels for 6%

profile of v8, /device:TPU:6, one launch (start us, length us, event | category | flops | bytes accessed | tf_op | source)
XLA Modules:
  0.0 180.6 jit_solution(7018260451928650532)
XLA Ops:
  6.5 2.5 %shard_map.154 = bf16[16,32,2048]{2,1,0:T(8,128)(2,1)} custom-call(bf16[32,2048]{1,0:T(8,128)(2,1)} %tokens.1, f32[1,2048]{1,0:T(1,128)} %bitcast.24), custom_call_target="tpu_custom_call" | custom-call | tf_op jit(solution)/shard_map/pallas_call | solution.py:357
  9.0 33.7 %all_to_all.35 = bf16[16,32,2048]{2,1,0:T(8,128)(2,1)S(1)} all-to-all(bf16[16,32,2048]{2,1,0:T(8,128)(2,1)} %shard_map.154), channel_id=1, replica_groups=mesh['sp_0'=4,'sp_1'=4,'sp_2'=4,'sp_3'=2,'tp'=4] {'sp_2','tp'}, dimensions={0} | all-to-all | bytes 4194304 | tf_op jit(solution)/shard_map/all_to_all | solution.py:319
  42.8 1.9 %collective-permute-start = (bf16[512,2048]{1,0:T(8,128)(2,1)S(1)}, bf16[512,2048]{1,0:T(8,128)(2,1)}, u32[]{:S(2)}, u32[]{:S(2)}) collective-permute-start(bf16[512,2048]{1,0:T(8,128)(2,1)S(1)} %bitcast.15), channel_id=1, source_target_pairs={{0,4},{4,0},{1,5},{5,1},{2,6},{6,2},{3,7},{7,3},{8,12},{12,8},{9,1... | collective-permute-start | bytes 6291464 | tf_op jit(solution)/shard_map/ppermute | solution.py:361
  44.7 1.6 shard_map.155
  46.2 9.4 %all_to_all.36.arrived = bf16[8,64,128]{2,1,0:T(8,128)(2,1)S(1)} all-to-all(bf16[8,64,128]{2,1,0:T(8,128)(2,1)} %shard_map.155), channel_id=1, replica_groups=mesh['sp_0'=4,'sp_1'=4,'sp_2'=4,'sp_3'=2,'tp'=4] {'sp_2','sp_3'}, dimensions={0} | all-to-all | bytes 262144 | tf_op jit(solution)/shard_map/all_to_all | solution.py:319
  56.4 42.1 %all_gather.9.columns = bf16[128,24,128]{2,1,0:T(8,128)(2,1)S(1)} all-gather(bf16[8,24,128]{2,1,0:T(8,128)(2,1)S(1)} %slice.8), channel_id=1, replica_groups=mesh['sp_0'=4,'sp_1'=4,'sp_2'=4,'sp_3'=2,'tp'=4] {'sp_0','sp_1'}, dimensions={0}, use_global_device_ids=true | all-gather | bytes 835584 | tf_op jit(solution)/shard_map/all_gather | solution.py:362
  99.4 2.4 %shard_map.157 = bf16[4,384,128]{2,1,0:T(8,128)(2,1)S(1)} custom-call(s32[5]{0:T(128)S(1)} %stack.23.place, bf16[512,2048]{1,0:T(8,128)(2,1)} %collective-permute-done.other, bf16[512,256]{1,0:T(8,128)(2,1)S(1)} %get-tuple-element.15.half, bf16[2048,256]{1,0:T(8,128)(2,1)S(1)} %get-tuple-element.16.weight), custom_call_target="tpu_custom_call" | custom-call | tf_op jit(solution)/shard_map/pallas_call | solution.py:55
  101.8 9.8 %all_to_all.37.pieces = bf16[4,384,128]{2,1,0:T(8,128)(2,1)S(1)} all-to-all(bf16[4,384,128]{2,1,0:T(8,128)(2,1)S(1)} %shard_map.157), channel_id=1, replica_groups=mesh['sp_0'=4,'sp_1'=4,'sp_2'=4,'sp_3'=2,'tp'=4] {'sp_2'}, dimensions={0} | all-to-all | bytes 786432 | tf_op jit(solution)/shard_map/all_to_all | solution.py:319
  111.6 1.0 shard_map.158
  112.6 7.8 %all_to_all.38.parts = bf16[4,40,128]{2,1,0:T(8,128)(2,1)S(1)} all-to-all(bf16[4,40,128]{2,1,0:T(8,128)(2,1)S(1)} %get-tuple-element.17), channel_id=1, replica_groups=mesh['sp_0'=4,'sp_1'=4,'sp_2'=4,'sp_3'=2,'tp'=4] {'sp_2'}, dimensions={0} | all-to-all | bytes 81920 | tf_op jit(solution)/shard_map/all_to_all | solution.py:319
  121.2 5.7 %all-to-all-start.4 = ((bf16[16,40,128]{2,1,0:T(8,128)(2,1)}), bf16[16,40,128]{2,1,0:T(8,128)(2,1)S(1)}, u32[]{:S(2)}, u32[]{:S(2)}) async-start(bf16[16,40,128]{2,1,0:T(8,128)(2,1)} %shard_map.159), calls=%async_computation.4 | async-start | bytes 327680 | tf_op jit(solution)/shard_map/all_to_all | solution.py:319
  126.9 5.5 %collective-permute-start.1 = (bf16[32,256]{1,0:T(8,128)(2,1)S(1)}, bf16[32,256]{1,0:T(8,128)(2,1)S(1)}, u32[]{:S(2)}, u32[]{:S(2)}) collective-permute-start(bf16[32,256]{1,0:T(8,128)(2,1)S(1)} %get-tuple-element.18), channel_id=1, source_target_pairs={{0,8},{8,16},{16,24},{24,32},{32,40},{40,48},{48,56},{56,64},{64,7... | collective-permute-start | bytes 49160 | tf_op jit(solution)/shard_map/ppermute | solution.py:393
  132.4 1.4 collective-permute-done.1.halo
  133.8 1.2 shard_map.160
  135.0 5.2 %all-to-all-done.4.slabs = bf16[16,40,128]{2,1,0:T(8,128)(2,1)S(1)} async-done(((bf16[16,40,128]{2,1,0:T(8,128)(2,1)}), bf16[16,40,128]{2,1,0:T(8,128)(2,1)S(1)}, u32[]{:S(2)}, u32[]{:S(2)}) %all-to-all-start.4) | async-done | bytes 163872 | tf_op jit(solution)/shard_map/all_to_all | solution.py:319
  140.3 1.3 shard_map.161
  141.6 6.0 %all-to-all-start.5 = ((bf16[32,32,128]{2,1,0:T(8,128)(2,1)}), bf16[32,32,128]{2,1,0:T(8,128)(2,1)S(1)}, u32[]{:S(2)}, u32[]{:S(2)}) async-start(bf16[32,32,128]{2,1,0:T(8,128)(2,1)} %shard_map.161), calls=%async_computation.5 | async-start | bytes 524288 | tf_op jit(solution)/shard_map/all_to_all | solution.py:319
  147.7 1.2 copy-done
  149.0 1.4 shard_map.162
  150.4 4.4 %all-to-all-done.5.joint = bf16[32,32,128]{2,1,0:T(8,128)(2,1)S(1)} async-done(((bf16[32,32,128]{2,1,0:T(8,128)(2,1)}), bf16[32,32,128]{2,1,0:T(8,128)(2,1)S(1)}, u32[]{:S(2)}, u32[]{:S(2)}) %all-to-all-start.5) | async-done | bytes 262176 | tf_op jit(solution)/shard_map/all_to_all | solution.py:319
  154.8 1.9 %shard_map.164 = (bf16[128,2048]{1,0:T(8,128)(2,1)S(1)}, bf16[128,2048]{1,0:T(8,128)(2,1)S(1)}) custom-call(s32[5]{0:T(128)S(1)} %stack.23.place, bf16[32,32,128]{2,1,0:T(8,128)(2,1)S(1)} %all-to-all-done.5.joint, f32[8,256]{1,0:T(8,128)S(1)} %get-tuple-element.19.sums, bf16[256,128]{1,0:T(8,128)(2,1)S(1)} %get-tuple-element.20.values, ...), custom_call_target="tpu_custom_call" | custom-call | tf_op jit(solution)/shard_map/pallas_call | solution.py:55
  156.6 2.0 %collective-permute-start.2 = (bf16[128,2048]{1,0:T(8,128)(2,1)S(1)}, bf16[128,2048]{1,0:T(8,128)(2,1)S(1)}, u32[]{:S(2)}, u32[]{:S(2)}) collective-permute-start(bf16[128,2048]{1,0:T(8,128)(2,1)S(1)} %get-tuple-element.24), channel_id=1, source_target_pairs={{0,4},{4,0},{1,5},{5,1},{2,6},{6,2},{3,7},{7,3},{8,12},{12,8},{9,1... | collective-permute-start | bytes 1572872 | tf_op jit(solution)/shard_map/ppermute | solution.py:425
  158.7 1.8 collective-permute-done.2
  160.6 12.5 %all_to_all.39 = bf16[4,32,2048]{2,1,0:T(8,128)(2,1)S(1)} all-to-all(bf16[4,32,2048]{2,1,0:T(8,128)(2,1)S(1)} %bitcast.23), channel_id=1, replica_groups=mesh['sp_0'=4,'sp_1'=4,'sp_2'=4,'sp_3'=2,'tp'=4] {'tp'}, dimensions={0} | all-to-all | bytes 1048576 | tf_op jit(solution)/shard_map/all_to_all | solution.py:319
  (23 shorter events, 3.3 us)
Async XLA Ops:
  6.5 141.1 %all-gather.3.cloned.1.call-start = ((), (), s32[]{:S(2)}) async-start(), calls=%async_computation.7 | async-start | bytes 1114112 | tf_op jit(solution)/shard_map/all_gather | solution.py:363
  42.8 56.6 %collective-permute-start = (bf16[512,2048]{1,0:T(8,128)(2,1)S(1)}, bf16[512,2048]{1,0:T(8,128)(2,1)}, u32[]{:S(2)}, u32[]{:S(2)}) collective-permute-start(bf16[512,2048]{1,0:T(8,128)(2,1)S(1)} %bitcast.15), channel_id=1, source_target_pairs={{0,4},{4,0},{1,5},{5,1},{2,6},{6,2},{3,7},{7,3},{8,12},{12,8},{9,1... | collective-permute-start | bytes 6291464 | tf_op jit(solution)/shard_map/ppermute | solution.py:361
  99.3 12.3 %copy-start.2 = (f32[256]{0:T(256)S(1)}, f32[256]{0:T(256)}, u32[]{:S(2)}) copy-start(f32[256]{0:T(256)} %param.27) | copy-start | bytes 3076
  99.4 34.5 %copy-start.1 = (f32[31,256]{1,0:T(8,128)S(1)}, f32[31,256]{1,0:T(8,128)}, u32[]{:S(2)}) copy-start(f32[31,256]{1,0:T(8,128)} %taps.1) | copy-start | bytes 95236
  121.2 19.1 %all-to-all-start.4 = ((bf16[16,40,128]{2,1,0:T(8,128)(2,1)}), bf16[16,40,128]{2,1,0:T(8,128)(2,1)S(1)}, u32[]{:S(2)}, u32[]{:S(2)}) async-start(bf16[16,40,128]{2,1,0:T(8,128)(2,1)} %shard_map.159), calls=%async_computation.4 | async-start | bytes 327680 | tf_op jit(solution)/shard_map/all_to_all | solution.py:319
  126.9 27.9 %copy-start.3 = (f32[256]{0:T(256)S(1)}, f32[256]{0:T(256)}, u32[]{:S(2)}) copy-start(f32[256]{0:T(256)} %param.21) | copy-start | bytes 3076
  126.9 27.8 %copy-start.4 = (f32[256]{0:T(256)S(1)}, f32[256]{0:T(256)}, u32[]{:S(2)}) copy-start(f32[256]{0:T(256)} %param.22) | copy-start | bytes 3076
  126.9 27.8 %copy-start.5 = (f32[256]{0:T(256)S(1)}, f32[256]{0:T(256)}, u32[]{:S(2)}) copy-start(f32[256]{0:T(256)} %param.29) | copy-start | bytes 3076
  126.9 6.9 %collective-permute-start.1 = (bf16[32,256]{1,0:T(8,128)(2,1)S(1)}, bf16[32,256]{1,0:T(8,128)(2,1)S(1)}, u32[]{:S(2)}, u32[]{:S(2)}) collective-permute-start(bf16[32,256]{1,0:T(8,128)(2,1)S(1)} %get-tuple-element.18), channel_id=1, source_target_pairs={{0,8},{8,16},{16,24},{24,32},{32,40},{40,48},{48,56},{56,64},{64,7... | collective-permute-start | bytes 49160 | tf_op jit(solution)/shard_map/ppermute | solution.py:393
  141.6 13.1 %all-to-all-start.5 = ((bf16[32,32,128]{2,1,0:T(8,128)(2,1)}), bf16[32,32,128]{2,1,0:T(8,128)(2,1)S(1)}, u32[]{:S(2)}, u32[]{:S(2)}) async-start(bf16[32,32,128]{2,1,0:T(8,128)(2,1)} %shard_map.161), calls=%async_computation.5 | async-start | bytes 524288 | tf_op jit(solution)/shard_map/all_to_all | solution.py:319
  147.6 1.2 copy-start
  156.6 3.8 %collective-permute-start.2 = (bf16[128,2048]{1,0:T(8,128)(2,1)S(1)}, bf16[128,2048]{1,0:T(8,128)(2,1)S(1)}, u32[]{:S(2)}, u32[]{:S(2)}) collective-permute-start(bf16[128,2048]{1,0:T(8,128)(2,1)S(1)} %get-tuple-element.24), channel_id=1, source_target_pairs={{0,4},{4,0},{1,5},{5,1},{2,6},{6,2},{3,7},{7,3},{8,12},{12,8},{9,1... | collective-permute-start | bytes 1572872 | tf_op jit(solution)/shard_map/ppermute | solution.py:425
Sparse Core Ops, SparseCore 0:
  56.4 73.3 all-gather.2

commit v9 on v8

--- a/solution.py
+++ b/solution.py
@@ -41,10 +41,12 @@
     return pltpu.with_memory_space_constraint(value, pltpu.VMEM)
 
 
-def kernel_call(body, out, specs, scratch=(), near=True):
+def kernel_call(body, out, specs, scratch=(), name=None, near=True):
     call = pl.pallas_call(
         body,
-        out_shape=jax.tree.map(lambda o: pltpu.VMEM(o.shape, o.dtype), out) if near else out,
+        out_shape=jax.tree.map(lambda o: pltpu.VMEM(o.shape, o.dtype), out)
+        if near or name == "pack"
+        else out,
         in_specs=specs,
         out_specs=jax.tree.map(lambda _: VMEM, out),
         scratch_shapes=scratch,
@@ -233,9 +235,10 @@
         total[z, OWN:] = tail
 
 
-def bridge_body(place, slabs, parts, sums, out):
+def bridge_body(place, slabs, parts, sums, paired, out):
     mine = NQ * place[0] + place[1]
-    own = NY * place[3] + place[4]
+    own = place[4]
+    total = sums[...] + paired[...]
     state = jnp.zeros((OWN, CH), f32)
     for z in range(NZ):
         step, add = unpacked(slabs[z])
@@ -243,15 +246,15 @@
     row = lax.broadcasted_iota(jnp.int32, (8, CH), 0)
     packed = []
     for k in range(2):
-        value = sums[:, k * CH : (k + 1) * CH]
+        value = total[:, k * CH : (k + 1) * CH]
         high = value.astype(bf16).astype(f32)
         middle = (value - high).astype(bf16).astype(f32)
         low = value - high - middle
         packed.append(jnp.where(row < 2, high, jnp.where(row < 4, middle, low)))
     packed = jnp.concatenate([*packed, jnp.zeros((16, CH), f32)], axis=0)
     for x in range(NX):
-        for k in range(NC * NY):
-            out[x * NC * NY + k] = jnp.where(k == own, state, packed).astype(bf16)
+        for k in range(NY):
+            out[x * NY + k] = jnp.where(k == own, state, packed).astype(bf16)
         step, add = unpacked(parts[x])
         state = state * jnp.exp(step) + add
 
@@ -286,18 +289,18 @@
 
 
 def tail_body(
-    place, joint, sums, values, gain, bias, inner, decayed, head_gain, pieces, weight, mine, theirs, both
+    place, joint, sums, paired, values, gain, bias, inner, decayed, head_gain, pieces, weight, theirs, both
 ):
     c = place[3]
-    group = NC * NY
-    own = NY * c + place[4]
+    group = NY
+    own = place[4]
     total = jnp.zeros((8, ROWS), f32)
     for k in range(group):
         piece = joint[group * place[2] + k].astype(f32)
         part = jnp.concatenate([piece[:8], piece[8:16]], axis=1)
         total = total + jnp.where(k == own, 0.0, part)
     row = lax.broadcasted_iota(jnp.int32, (8, ROWS), 0)
-    total = total + jnp.where(row < 2, sums[...], 0.0)
+    total = total + jnp.where(row < 2, sums[...] + paired[...], 0.0)
     row = lax.broadcasted_iota(jnp.int32, (8, CH), 0)
     pick_first = jnp.where((row < 6) & (row % 2 == 0), 1.0 / CONV_CH, 0.0)
     pick_second = jnp.where((row < 6) & (row % 2 == 1), 1.0 / CONV_CH, 0.0)
@@ -310,9 +313,13 @@
     scale = lax.rsqrt(jnp.mean(recurrent * recurrent, axis=1, keepdims=True) + norm_eps)
     gate = silu(pieces[3, :ROWS].astype(f32))
     both[:, CH:] = (recurrent * scale * own_half(head_gain[...], c) * gate).astype(bf16)
-    for core, out in ((c, mine), (1 - c, theirs)):
-        rows = pl.ds(pl.multiple_of(core * HALF, HALF), HALF)
-        out[...] = matmul(both[rows], weight[...], ((1,), (1,))).astype(bf16)
+    rows = pl.ds(pl.multiple_of((1 - c) * HALF, HALF), HALF)
+    theirs[...] = matmul(both[rows], weight[...], ((1,), (1,))).astype(bf16)
+
+
+def mine_body(place, both, weight, mine):
+    rows = pl.ds(pl.multiple_of(place[3] * HALF, HALF), HALF)
+    mine[...] = matmul(both[rows], weight[...], ((1,), (1,)))
 
 
 def exchanged(x, axes):
@@ -341,7 +348,7 @@
     width = tokens.shape[1]
 
     payload = kernel_call(
-        pack_body, shape((NX * NC, SENT_ROWS, CH), bf16), [VMEM] * 9, near=False
+        pack_body, shape((NX * NC, SENT_ROWS, CH), bf16), [VMEM] * 9, name="pack", near=False
     )(
         query_projection_weight,
         forget_gate_weight,
@@ -355,7 +362,7 @@
     )
     arrived = exchanged(payload, (X, C))
     copies = kernel_call(
-        norm_body, shape((NX * NY, OWN, width), bf16), [VMEM, VMEM], near=False
+        norm_body, shape((NX * NY, OWN, width), bf16), [VMEM, VMEM], name="norm", near=False
     )(tokens, input_norm_gain.reshape(1, width))
     own = exchanged(copies, (X, Y)).reshape(NX * HALF, width)
     other = lax.ppermute(own, C, [(0, 1), (1, 0)])
@@ -367,9 +374,13 @@
         weight_body,
         (shape((NX * HALF, 2 * CH), bf16), shape((width, 2 * CH), bf16)),
         [VMEM] * 2,
+        name="weight",
     )(own, columns)
     projected = kernel_call(
-        project_body, shape((NX, ROWS + HALF, CH), bf16), [SMEM] + [VMEM] * 3
+        project_body,
+        shape((NX, ROWS + HALF, CH), bf16),
+        [SMEM] + [VMEM] * 3,
+        name="project",
     )(place, other, half, weight)
     pieces = exchanged(projected, X)
 
@@ -378,15 +389,17 @@
         state_body,
         (shape((NX, STATE_ROWS, CH), bf16), shape((HALO, 2 * CH), bf16)),
         [SMEM] + [VMEM] * 3,
+        name="state",
     )(place, pieces, margin, arrived)
     inner, decayed = kernel_call(
         local_body,
         (shape((ROWS, CH), f32), shape((ROWS, CH), bf16)),
         [SMEM] + [VMEM] * 3,
+        name="local",
     )(place, pieces, margin, arrived)
     parts = exchanged(packed, X)
     slab_copies = kernel_call(
-        slab_body, shape((NZ, STATE_ROWS, CH), bf16), [VMEM]
+        slab_body, shape((NZ, STATE_ROWS, CH), bf16), [VMEM], name="slab"
     )(parts)
     slabs = exchanged(slab_copies, (ZH, ZL))
     blocks = NZ * NX
@@ -396,23 +409,26 @@
         (shape((ROWS, CH), bf16), shape((8, ROWS), f32)),
         [SMEM, VMEM, VMEM, VMEM],
         [pltpu.VMEM((HALO + ROWS, CH), f32)],
+        name="conv",
     )(place, pieces, halo, depthwise_filter_taps)
+    paired = lax.ppermute(sums, C, [(0, 1), (1, 0)])
     bridge = kernel_call(
-        bridge_body, shape((NX * NC * NY, OWN, CH), bf16), [SMEM] + [VMEM] * 3
-    )(place, slabs, parts, sums)
-    joint = exchanged(bridge, (X, C, Y))
-    out_weight = kernel_call(order_body, shape((width, 2 * CH), bf16), [VMEM])(
+        bridge_body, shape((NX * NY, OWN, CH), bf16), [SMEM] + [VMEM] * 4, name="bridge"
+    )(place, slabs, parts, sums, paired)
+    joint = exchanged(bridge, (X, Y))
+    out_weight = kernel_call(order_body, shape((width, 2 * CH), bf16), [VMEM], name="order")(
         out_pieces
     )
-    mine, theirs = kernel_call(
+    theirs, both = kernel_call(
         tail_body,
-        (shape((HALF, width), bf16), shape((HALF, width), bf16)),
-        [SMEM] + [VMEM] * 10,
-        [pltpu.VMEM((ROWS, 2 * CH), bf16)],
+        (shape((HALF, width), bf16), shape((ROWS, 2 * CH), bf16)),
+        [SMEM] + [VMEM] * 11,
+        name="tail",
     )(
         place,
         joint,
         sums,
+        paired,
         convolved,
         channel_norm_gain.reshape(1, 2 * CH),
         channel_norm_bias.reshape(1, 2 * CH),
@@ -423,7 +439,10 @@
         out_weight,
     )
     given = lax.ppermute(theirs, C, [(0, 1), (1, 0)])
-    pair_sum = (mine.astype(f32) + given.astype(f32)).astype(bf16)
+    mine = kernel_call(mine_body, shape((HALF, width), f32), [SMEM] + [VMEM] * 2, name="mine")(
+        place, both, out_weight
+    )
+    pair_sum = (mine + given.astype(f32)).astype(bf16)
     pieces = exchanged(pair_sum.reshape(NY, OWN, width), Y)
     return pieces.astype(f32).sum(axis=0).astype(bf16)
 

time: 183 us -> 180 us (0.984)
  waiting for transfers between devices: 12.9 us -> 8.86 us
    all_to_all x2, waiting for transfers between devices: 9.64 us -> 5.42 us  [exchanged(): return lax.all_to_all(x, axes, split_axis=0, concat_axis=0, tiled=True)]
    ppermute x0 -> x1, starting transfers between devices: none -> 1.94 us  [per_device(): paired = lax.ppermute(sums, C, [(0, 1), (1, 0)])]
    pallas_call x9 -> x10, Pallas kernels: 10.8 us -> 11.4 us  [kernel_call(): return lambda *args: call(*[in_vmem(a, s) for a, s in zip(args, specs)])]
  transfers between devices with their start and end apart: 6 -> 7, of which waited for: 4 -> 5; matrix products, arithmetic and copies ran while one was open for 0% -> 0% of each run, Pallas kernels for 6% -> 6%
where the time goes in v9:
time: 180 us; the launch traced here: 177 us
  blocking collectives  115 us (64%)
  starting transfers between devices  22.4 us (12%)
  Pallas kernels  14.8 us (8%)
  between operations  13.5 us (8%)
  waiting for transfers between devices  8.86 us (5%)
  local copies, waits for them, and re-layouts  1.95 us (1%)
    all_to_all x5, blocking collectives, exchanged(): return lax.all_to_all(x, axes, split_axis=0, concat_axis=0, tiled=True)  72.6 us
    all_gather x1, blocking collectives, per_device(): lax.all_gather(arrived[:, :COLUMN_ROWS], (ZH, ZL), axis=0, tiled=True)  42.3 us
    pallas_call x10, Pallas kernels, kernel_call(): return lambda *args: call(*[in_vmem(a, s) for a, s in zip(args, specs)])  11.4 us
    all_to_all x2, starting transfers between devices, exchanged(): return lax.all_to_all(x, axes, split_axis=0, concat_axis=0, tiled=True)  11.3 us
    all_to_all x2, waiting for transfers between devices, exchanged(): return lax.all_to_all(x, axes, split_axis=0, concat_axis=0, tiled=True)  5.42 us
    ppermute x1, starting transfers between devices, per_device(): lax.ppermute(tail, (ZH, ZL, X), [(k, k + 1) for k in range(blocks - 1)])  5.33 us
  transfers between devices with their start and end apart: 7, of which 5 were waited for; matrix products, arithmetic and copies ran while one was open for 0% of the time, Pallas kernels for 6%

profile of v9, /device:TPU:6, one launch (start us, length us, event | category | flops | bytes accessed | tf_op | source)
XLA Modules:
  0.0 177.4 jit_solution(2256295690084470874)
XLA Ops:
  6.5 2.5 %shard_map.154 = bf16[16,32,2048]{2,1,0:T(8,128)(2,1)} custom-call(bf16[32,2048]{1,0:T(8,128)(2,1)} %tokens.1, f32[1,2048]{1,0:T(1,128)} %bitcast.24), custom_call_target="tpu_custom_call" | custom-call | tf_op jit(solution)/shard_map/pallas_call | solution.py:364
  9.0 33.7 %all_to_all.35 = bf16[16,32,2048]{2,1,0:T(8,128)(2,1)S(1)} all-to-all(bf16[16,32,2048]{2,1,0:T(8,128)(2,1)} %shard_map.154), channel_id=1, replica_groups=mesh['sp_0'=4,'sp_1'=4,'sp_2'=4,'sp_3'=2,'tp'=4] {'sp_2','tp'}, dimensions={0} | all-to-all | bytes 4194304 | tf_op jit(solution)/shard_map/all_to_all | solution.py:326
  42.8 1.9 %collective-permute-start = (bf16[512,2048]{1,0:T(8,128)(2,1)S(1)}, bf16[512,2048]{1,0:T(8,128)(2,1)}, u32[]{:S(2)}, u32[]{:S(2)}) collective-permute-start(bf16[512,2048]{1,0:T(8,128)(2,1)S(1)} %bitcast.15), channel_id=1, source_target_pairs={{0,4},{4,0},{1,5},{5,1},{2,6},{6,2},{3,7},{7,3},{8,12},{12,8},{9,1... | collective-permute-start | bytes 6291464 | tf_op jit(solution)/shard_map/ppermute | solution.py:368
  45.6 8.5 %all_to_all.36.arrived = bf16[8,64,128]{2,1,0:T(8,128)(2,1)S(1)} all-to-all(bf16[8,64,128]{2,1,0:T(8,128)(2,1)S(1)} %shard_map.155), channel_id=1, replica_groups=mesh['sp_0'=4,'sp_1'=4,'sp_2'=4,'sp_3'=2,'tp'=4] {'sp_2','sp_3'}, dimensions={0} | all-to-all | bytes 262144 | tf_op jit(solution)/shard_map/all_to_all | solution.py:326
  54.9 42.3 %all_gather.9.columns = bf16[128,24,128]{2,1,0:T(8,128)(2,1)S(1)} all-gather(bf16[8,24,128]{2,1,0:T(8,128)(2,1)S(1)} %slice.8), channel_id=1, replica_groups=mesh['sp_0'=4,'sp_1'=4,'sp_2'=4,'sp_3'=2,'tp'=4] {'sp_0','sp_1'}, dimensions={0}, use_global_device_ids=true | all-gather | bytes 835584 | tf_op jit(solution)/shard_map/all_gather | solution.py:369
  98.0 2.4 %shard_map.157 = bf16[4,384,128]{2,1,0:T(8,128)(2,1)S(1)} custom-call(s32[5]{0:T(128)S(1)} %stack.23.place, bf16[512,2048]{1,0:T(8,128)(2,1)} %collective-permute-done.other, bf16[512,256]{1,0:T(8,128)(2,1)S(1)} %get-tuple-element.15.half, bf16[2048,256]{1,0:T(8,128)(2,1)S(1)} %get-tuple-element.16.weight), custom_call_target="tpu_custom_call" | custom-call | tf_op jit(solution)/shard_map/pallas_call | solution.py:57
  100.4 10.1 %all_to_all.37.pieces = bf16[4,384,128]{2,1,0:T(8,128)(2,1)S(1)} all-to-all(bf16[4,384,128]{2,1,0:T(8,128)(2,1)S(1)} %shard_map.157), channel_id=1, replica_groups=mesh['sp_0'=4,'sp_1'=4,'sp_2'=4,'sp_3'=2,'tp'=4] {'sp_2'}, dimensions={0} | all-to-all | bytes 786432 | tf_op jit(solution)/shard_map/all_to_all | solution.py:326
  111.5 7.8 %all_to_all.38.parts = bf16[4,40,128]{2,1,0:T(8,128)(2,1)S(1)} all-to-all(bf16[4,40,128]{2,1,0:T(8,128)(2,1)S(1)} %get-tuple-element.17), channel_id=1, replica_groups=mesh['sp_0'=4,'sp_1'=4,'sp_2'=4,'sp_3'=2,'tp'=4] {'sp_2'}, dimensions={0} | all-to-all | bytes 81920 | tf_op jit(solution)/shard_map/all_to_all | solution.py:326
  120.1 5.9 %all-to-all-start.4 = ((bf16[16,40,128]{2,1,0:T(8,128)(2,1)}), bf16[16,40,128]{2,1,0:T(8,128)(2,1)S(1)}, u32[]{:S(2)}, u32[]{:S(2)}) async-start(bf16[16,40,128]{2,1,0:T(8,128)(2,1)} %shard_map.159), calls=%async_computation.4 | async-start | bytes 327680 | tf_op jit(solution)/shard_map/all_to_all | solution.py:326
  126.0 5.3 %collective-permute-start.1 = (bf16[32,256]{1,0:T(8,128)(2,1)S(1)}, bf16[32,256]{1,0:T(8,128)(2,1)S(1)}, u32[]{:S(2)}, u32[]{:S(2)}) collective-permute-start(bf16[32,256]{1,0:T(8,128)(2,1)S(1)} %get-tuple-element.18), channel_id=1, source_target_pairs={{0,8},{8,16},{16,24},{24,32},{32,40},{40,48},{48,56},{56,64},{64,7... | collective-permute-start | bytes 49160 | tf_op jit(solution)/shard_map/ppermute | solution.py:406
  131.3 1.4 collective-permute-done.1.halo
  132.7 1.2 shard_map.160
  133.9 1.9 %collective-permute-start.2 = (f32[8,256]{1,0:T(8,128)S(1)}, f32[8,256]{1,0:T(8,128)S(1)}, u32[]{:S(2)}, u32[]{:S(2)}) collective-permute-start(f32[8,256]{1,0:T(8,128)S(1)} %get-tuple-element.19.sums), channel_id=1, source_target_pairs={{0,4},{4,0},{1,5},{5,1},{2,6},{6,2},{3,7},{7,3},{8,12},{12,8},{9,1... | collective-permute-start | bytes 24584 | tf_op jit(solution)/shard_map/ppermute | solution.py:414
  135.9 1.1 collective-permute-done.2.paired
  137.0 2.3 %all-to-all-done.4.slabs = bf16[16,40,128]{2,1,0:T(8,128)(2,1)S(1)} async-done(((bf16[16,40,128]{2,1,0:T(8,128)(2,1)}), bf16[16,40,128]{2,1,0:T(8,128)(2,1)S(1)}, u32[]{:S(2)}, u32[]{:S(2)}) %all-to-all-start.4) | async-done | bytes 163872 | tf_op jit(solution)/shard_map/all_to_all | solution.py:326
  139.3 1.3 shard_map.161
  140.6 5.4 %all-to-all-start.5 = ((bf16[16,32,128]{2,1,0:T(8,128)(2,1)}), bf16[16,32,128]{2,1,0:T(8,128)(2,1)S(1)}, u32[]{:S(2)}, u32[]{:S(2)}) async-start(bf16[16,32,128]{2,1,0:T(8,128)(2,1)} %shard_map.161), calls=%async_computation.5 | async-start | bytes 262144 | tf_op jit(solution)/shard_map/all_to_all | solution.py:326
  146.1 1.2 copy-done
  147.4 1.4 shard_map.162
  148.8 3.1 %all-to-all-done.5.joint = bf16[16,32,128]{2,1,0:T(8,128)(2,1)S(1)} async-done(((bf16[16,32,128]{2,1,0:T(8,128)(2,1)}), bf16[16,32,128]{2,1,0:T(8,128)(2,1)S(1)}, u32[]{:S(2)}, u32[]{:S(2)}) %all-to-all-start.5) | async-done | bytes 131104 | tf_op jit(solution)/shard_map/all_to_all | solution.py:326
  151.9 1.5 shard_map.164
  153.4 1.9 %collective-permute-start.3 = (bf16[128,2048]{1,0:T(8,128)(2,1)S(1)}, bf16[128,2048]{1,0:T(8,128)(2,1)S(1)}, u32[]{:S(2)}, u32[]{:S(2)}) collective-permute-start(bf16[128,2048]{1,0:T(8,128)(2,1)S(1)} %get-tuple-element.24), channel_id=1, source_target_pairs={{0,4},{4,0},{1,5},{5,1},{2,6},{6,2},{3,7},{7,3},{8,12},{12,8},{9,1... | collective-permute-start | bytes 1572872 | tf_op jit(solution)/shard_map/ppermute | solution.py:441
  155.3 1.0 shard_map.165
  157.3 12.5 %all_to_all.39 = bf16[4,32,2048]{2,1,0:T(8,128)(2,1)S(1)} all-to-all(bf16[4,32,2048]{2,1,0:T(8,128)(2,1)S(1)} %bitcast.23), channel_id=1, replica_groups=mesh['sp_0'=4,'sp_1'=4,'sp_2'=4,'sp_3'=2,'tp'=4] {'tp'}, dimensions={0} | all-to-all | bytes 1048576 | tf_op jit(solution)/shard_map/all_to_all | solution.py:326
  (26 shorter events, 6.0 us)
Async XLA Ops:
  6.5 139.5 %all-gather.3.cloned.1.call-start = ((), (), s32[]{:S(2)}) async-start(), calls=%async_computation.7 | async-start | bytes 1114112 | tf_op jit(solution)/shard_map/all_gather | solution.py:370
  42.8 55.3 %collective-permute-start = (bf16[512,2048]{1,0:T(8,128)(2,1)S(1)}, bf16[512,2048]{1,0:T(8,128)(2,1)}, u32[]{:S(2)}, u32[]{:S(2)}) collective-permute-start(bf16[512,2048]{1,0:T(8,128)(2,1)S(1)} %bitcast.15), channel_id=1, source_target_pairs={{0,4},{4,0},{1,5},{5,1},{2,6},{6,2},{3,7},{7,3},{8,12},{12,8},{9,1... | collective-permute-start | bytes 6291464 | tf_op jit(solution)/shard_map/ppermute | solution.py:368
  98.0 12.5 %copy-start.2 = (f32[256]{0:T(256)S(1)}, f32[256]{0:T(256)}, u32[]{:S(2)}) copy-start(f32[256]{0:T(256)} %param.27) | copy-start | bytes 3076
  98.0 34.7 %copy-start.1 = (f32[31,256]{1,0:T(8,128)S(1)}, f32[31,256]{1,0:T(8,128)}, u32[]{:S(2)}) copy-start(f32[31,256]{1,0:T(8,128)} %taps.1) | copy-start | bytes 95236
  119.4 32.5 %copy-start.3 = (f32[256]{0:T(256)S(1)}, f32[256]{0:T(256)}, u32[]{:S(2)}) copy-start(f32[256]{0:T(256)} %param.21) | copy-start | bytes 3076
  119.4 32.5 %copy-start.4 = (f32[256]{0:T(256)S(1)}, f32[256]{0:T(256)}, u32[]{:S(2)}) copy-start(f32[256]{0:T(256)} %param.22) | copy-start | bytes 3076
  119.4 32.5 %copy-start.5 = (f32[256]{0:T(256)S(1)}, f32[256]{0:T(256)}, u32[]{:S(2)}) copy-start(f32[256]{0:T(256)} %param.29) | copy-start | bytes 3076
  120.1 19.3 %all-to-all-start.4 = ((bf16[16,40,128]{2,1,0:T(8,128)(2,1)}), bf16[16,40,128]{2,1,0:T(8,128)(2,1)S(1)}, u32[]{:S(2)}, u32[]{:S(2)}) async-start(bf16[16,40,128]{2,1,0:T(8,128)(2,1)} %shard_map.159), calls=%async_computation.4 | async-start | bytes 327680 | tf_op jit(solution)/shard_map/all_to_all | solution.py:326
  126.0 6.8 %collective-permute-start.1 = (bf16[32,256]{1,0:T(8,128)(2,1)S(1)}, bf16[32,256]{1,0:T(8,128)(2,1)S(1)}, u32[]{:S(2)}, u32[]{:S(2)}) collective-permute-start(bf16[32,256]{1,0:T(8,128)(2,1)S(1)} %get-tuple-element.18), channel_id=1, source_target_pairs={{0,8},{8,16},{16,24},{24,32},{32,40},{40,48},{48,56},{56,64},{64,7... | collective-permute-start | bytes 49160 | tf_op jit(solution)/shard_map/ppermute | solution.py:406
  133.9 3.1 %collective-permute-start.2 = (f32[8,256]{1,0:T(8,128)S(1)}, f32[8,256]{1,0:T(8,128)S(1)}, u32[]{:S(2)}, u32[]{:S(2)}) collective-permute-start(f32[8,256]{1,0:T(8,128)S(1)} %get-tuple-element.19.sums), channel_id=1, source_target_pairs={{0,4},{4,0},{1,5},{5,1},{2,6},{6,2},{3,7},{7,3},{8,12},{12,8},{9,1... | collective-permute-start | bytes 24584 | tf_op jit(solution)/shard_map/ppermute | solution.py:414
  140.6 11.3 %all-to-all-start.5 = ((bf16[16,32,128]{2,1,0:T(8,128)(2,1)}), bf16[16,32,128]{2,1,0:T(8,128)(2,1)S(1)}, u32[]{:S(2)}, u32[]{:S(2)}) async-start(bf16[16,32,128]{2,1,0:T(8,128)(2,1)} %shard_map.161), calls=%async_computation.5 | async-start | bytes 262144 | tf_op jit(solution)/shard_map/all_to_all | solution.py:326
  146.1 1.2 copy-start
  153.4 3.8 %collective-permute-start.3 = (bf16[128,2048]{1,0:T(8,128)(2,1)S(1)}, bf16[128,2048]{1,0:T(8,128)(2,1)S(1)}, u32[]{:S(2)}, u32[]{:S(2)}) collective-permute-start(bf16[128,2048]{1,0:T(8,128)(2,1)S(1)} %get-tuple-element.24), channel_id=1, source_target_pairs={{0,4},{4,0},{1,5},{5,1},{2,6},{6,2},{3,7},{7,3},{8,12},{12,8},{9,1... | collective-permute-start | bytes 1572872 | tf_op jit(solution)/shard_map/ppermute | solution.py:441
Sparse Core Ops, SparseCore 0:
  54.9 73.6 all-gather.2
